TPU v7x, 256 devices: a 4x2x16 block of a 4x16x16 slice. The times are simulated.
256 devices in a mesh: grp: 2 (over y), st: 32 (over z, core), tp: 4 (over x).
Axes of the slice: x: 4, y: 2, z: 16, core: 2. Of those that a mesh axis runs over, the one named last changes fastest.
The devices are a block of a 4x16x16 slice.
Arguments:
- tokens: bfloat16 [32768, 2048], P(('grp', 'st')), parts along dimension 0, may hold values from -6 to 6
- owners: int32 [512, 4], P(('grp', 'st')), parts along dimension 0, may hold values from 0 to 31, all different within a row; in each aligned block of 8 rows (0 to 7, 8 to 15, ...) at most 2 rows name the same one
- entries: int32 [512, 4], P(('grp', 'st')), parts along dimension 0, may hold values from 0 to 15
- store: bfloat16 [1024, 64, 2048], P(('grp', 'st')), parts along dimension 0, may hold values from -600 to 600
- mixer_query_weight: bfloat16 [2048, 1024], P(None, 'tp'), may hold values from -0.125 to 0.125
- mixer_key_weight: bfloat16 [2048, 1024], P(None, 'tp'), may hold values from -0.125 to 0.125
- mixer_value_weight: bfloat16 [2048, 1024], P(None, 'tp'), may hold values from -0.125 to 0.125
- strength_weight: bfloat16 [2048, 8], P(None, 'tp'), may hold values from -0.125 to 0.125
- decay_weight: bfloat16 [2048, 8], P(None, 'tp'), may hold values from -0.125 to 0.125
- head_decay_rate: float32 [8], P('tp'), may hold values from 0.003 to 0.15
- extra_forgetting_exponent: float32 [32768, 8], P(('grp', 'st'), 'tp'), parts along dimension 0, may hold values from -0.7 to 0
- output_norm_gain: float32 [128], replicated, may hold values from 0.1 to 1.9
- retrieval_query_weight: bfloat16 [2048, 1024], P(None, 'tp'), may hold values from -0.125 to 0.125
- passage_key_weight: bfloat16 [2048, 1024], P(None, 'tp'), may hold values from -0.125 to 0.125
- passage_value_weight: bfloat16 [2048, 1024], P(None, 'tp'), may hold values from -0.125 to 0.125
- retrieval_gate_weight: bfloat16 [2048, 8], P(None, 'tp'), may hold values from -0.125 to 0.125
Outputs:
- mixed: bfloat16 [32768, 1024], P(('grp', 'st'), 'tp'), parts along dimension 0
There are 2 independent parts, one for each index of `grp`. A program takes and returns all parts, laid end to end along the dimension named above; an argument that names none is the same for every part. Nothing has to cross between parts.
Inputs may be any that keep to these rules, and one draw needn't show every extreme that they name: `owners`: each row names 4 different values; the rows of one device name no value more than 2 times, a bound that some device reaches; every value is named by some row.
All inputs are finite; a program needn't handle non-finite values.
Results may differ from a plain program's by a relative error of at most 0.015.
The roundings to bfloat16 on the way count: a program that leaves them out, or rounds other values in their place, can miss the bound.
Values may be sent and summed in bfloat16 or wider, within the bound.
No kernel may reach another device: no remote copies, remote signals or barrier semaphores. Data moves between devices by JAX's collectives and lax.ppermute only.
A program may use at most 128 MiB of HBM per device.

v0:
```python
import functools

import jax
import jax.numpy as jnp
from jax import lax
from jax.experimental import pallas as pl
from jax.experimental.pallas import tpu as pltpu
from jax.sharding import PartitionSpec as P


BLOCK = 64
SLOTS = 4
EPS = 1e-06
NONE = -1e30
MIB = 1024 * 1024
BIG = 52
F32 = jnp.float32
BF16 = jnp.bfloat16
VMEM = pltpu.VMEM


def nt(left, right):
    return lax.dot_general(left, right, (((1,), (1,)), ((), ())), preferred_element_type=F32)


def nn(left, right):
    return jnp.dot(left, right, preferred_element_type=F32)


def tn(left, right):
    return lax.dot_general(left, right, (((0,), (0,)), ((), ())), preferred_element_type=F32)


def params(limit, **more):
    return pltpu.CompilerParams(vmem_limit_bytes=limit * MIB, **more)


def cost(flops, size, trans=0):
    return pl.CostEstimate(flops=flops, bytes_accessed=size, transcendentals=trans)


def pieces(src, dst, sems, first, count):
    rows = dst.shape[0] // count
    return [
        pltpu.make_async_copy(
            src.at[pl.ds(i * rows, rows)], dst.at[pl.ds(i * rows, rows)], sems.at[first + i]
        )
        for i in range(count)
    ]


def query_body(x_hbm, w_hbm, owners_hbm, entries_hbm, out_ref, x_buf, w_buf, owners_ref, entries_ref, sems):
    tiles, rows, _ = x_buf.shape
    loads = pieces(w_hbm, w_buf, sems, 0, 4)
    x_loads = [
        pieces(x_hbm.at[pl.ds(i * rows, rows)], x_buf.at[i], sems, 4 + i * 4, 4)
        for i in range(tiles)
    ]
    tables = [
        pltpu.make_async_copy(owners_hbm, owners_ref, sems.at[tiles * 4 + 4]),
        pltpu.make_async_copy(entries_hbm, entries_ref, sems.at[tiles * 4 + 5]),
    ]
    for copies in [loads] + x_loads + [tables]:
        for copy in copies:
            copy.start()
    per, count = owners_ref.shape
    blocks = tiles * rows // BLOCK
    for table in tables:
        table.wait()
    names = jnp.concatenate([owners_ref[...] + 1, entries_ref[...]], axis=0).astype(F32)
    out_ref[blocks * 128 :, :] = jnp.zeros((2 * per, 128), BF16)
    out_ref[blocks * 128 :, 0:count] = names.astype(BF16)
    for copy in loads:
        copy.wait()
    for i in range(tiles):
        for copy in x_loads[i]:
            copy.wait()
        q = nn(x_buf[i], w_buf[...]).astype(BF16)
        for n in range(rows // BLOCK):
            at = (i * rows // BLOCK + n) * 128
            for h in range(2):
                out_ref[at + h * BLOCK : at + (h + 1) * BLOCK, :] = q[
                    n * BLOCK : (n + 1) * BLOCK, h * 128 : (h + 1) * 128
                ]


def query_message(x, w, owners, entries, tiles=2):
    rows, depth = x.shape
    hbm = pl.BlockSpec(memory_space=pltpu.HBM)
    whole = pl.BlockSpec(memory_space=VMEM)
    return pl.pallas_call(
        query_body,
        in_specs=[hbm] * 4,
        out_specs=whole,
        out_shape=jax.ShapeDtypeStruct((rows * 2 + 8, 128), BF16),
        scratch_shapes=[
            VMEM((tiles, rows // tiles, depth), BF16),
            VMEM(w.shape, BF16),
            VMEM(owners.shape, jnp.int32),
            VMEM(entries.shape, jnp.int32),
            pltpu.SemaphoreType.DMA((tiles * 4 + 6,)),
        ],
        compiler_params=params(BIG + 1),
        cost_estimate=cost(2 * rows * depth * 256, 2 * (rows * depth + depth * 256)),
        name="query",
    )(x, w, owners, entries)


def mixed_body(
    x_hbm, wq_hbm, wk_hbm, wv_hbm, ga_ref, gb_ref, gc_ref, after_ref, out_ref, lg_ref, x_buf, w_buf, sems
):
    tiles, tall, depth = x_buf.shape

    x_loads = [
        pieces(x_hbm.at[pl.ds(t * tall, tall)], x_buf.at[t], sems, t * 4, 4) for t in range(tiles)
    ]
    w_loads = [
        pieces(w, w_buf.at[i], sems, (tiles + i) * 4, 4)
        for i, w in enumerate((wq_hbm, wk_hbm, wv_hbm))
    ]
    for copies in x_loads + w_loads:
        for copy in copies:
            copy.start()
    none = jnp.zeros((2, depth), BF16)
    gates = jnp.concatenate([ga_ref[...], gb_ref[...], gc_ref[...], none], axis=0)
    for t in range(tiles):
        for copy in x_loads[t]:
            copy.wait()
        lg_ref[t * tall : (t + 1) * tall, :] = nt(x_buf[t], gates)
    for copy in w_loads[0]:
        copy.wait()

    def piece(step, _):
        i, t = step // tiles, step % tiles
        rows = nn(x_buf[t], w_buf[i]).astype(BF16)
        for n in range(tall // BLOCK):
            for h in range(2):
                out_ref[i, t * (tall // BLOCK) + n, h * BLOCK : (h + 1) * BLOCK, :] = rows[
                    n * BLOCK : (n + 1) * BLOCK, h * 128 : (h + 1) * 128
                ]
        return 0

    lax.fori_loop(0, tiles, piece, 0)
    for copy in w_loads[1] + w_loads[2]:
        copy.wait()
    lax.fori_loop(tiles, 3 * tiles, piece, 0)


def mixer_inputs(x, wq, wk, wv, ga, gb, gc, after, tiles=2):
    rows, depth = x.shape
    hbm = pl.BlockSpec(memory_space=pltpu.HBM)
    whole = pl.BlockSpec(memory_space=VMEM)
    return pl.pallas_call(
        mixed_body,
        in_specs=[hbm] * 4 + [whole] * 3 + [pl.BlockSpec(memory_space=pl.ANY)],
        out_specs=[whole] * 2,
        out_shape=[
            jax.ShapeDtypeStruct((3, rows // BLOCK, 128, 128), BF16),
            jax.ShapeDtypeStruct((rows, 8), F32),
        ],
        scratch_shapes=[
            VMEM((tiles, rows // tiles, depth), BF16),
            VMEM((3,) + wq.shape, BF16),
            pltpu.SemaphoreType.DMA((tiles * 4 + 12,)),
        ],
        compiler_params=params(BIG),
        cost_estimate=cost(2 * rows * depth * 768, 2 * (rows * depth + depth * 768)),
        name="mixer_inputs",
    )(x, wq, wk, wv, ga, gb, gc, after)


def passages_body(store_hbm, wk_hbm, wv_hbm, after_ref, out_ref, x_buf, w_buf, sems):
    chunks, tall, _ = x_buf.shape
    rows = out_ref.shape[1] // 4
    count = tall // rows

    def load(i):
        return pieces(store_hbm.at[pl.ds(i * tall, tall)], x_buf.at[i], sems, i * 4, 4)

    weights = pieces(wk_hbm, w_buf.at[0], sems, chunks * 4, 4)
    weights += pieces(wv_hbm, w_buf.at[1], sems, chunks * 4 + 4, 4)
    for copy in load(0) + weights:
        copy.start()
    for i in range(1, chunks):
        for copy in load(i):
            copy.start()
    for copy in weights:
        copy.wait()

    def chunk(i, _):
        for copy in load(i):
            copy.wait()
        keys = nn(x_buf[i], w_buf[0]).astype(BF16)
        values = nn(x_buf[i], w_buf[1]).astype(BF16).astype(F32)
        for p in range(count):
            span = slice(p * rows, (p + 1) * rows)
            at = i * count + p
            for h in range(2):
                out_ref[at, h * rows : (h + 1) * rows, :] = keys[span, h * 128 : (h + 1) * 128]
            stacked = jnp.concatenate([values[span, :128], values[span, 128:]], axis=0)
            out_ref[at, 128:256, :] = stacked.T.astype(BF16)
        return 0

    lax.fori_loop(0, chunks, chunk, 0)


def project_passages(store, wk, wv, after, chunks=4):
    number, rows, depth = store.shape
    hbm = pl.BlockSpec(memory_space=pltpu.HBM)
    return pl.pallas_call(
        passages_body,
        in_specs=[hbm, hbm, hbm, pl.BlockSpec(memory_space=pl.ANY)],
        out_specs=pl.BlockSpec(memory_space=VMEM),
        out_shape=jax.ShapeDtypeStruct((number, 256, 128), BF16),
        scratch_shapes=[
            VMEM((chunks, number * rows // chunks, depth), BF16),
            VMEM((2,) + wk.shape, BF16),
            pltpu.SemaphoreType.DMA((chunks * 4 + 8,)),
        ],
        compiler_params=params(BIG),
        cost_estimate=cost(2 * number * rows * depth * 512, 2 * number * rows * depth),
        name="passages",
    )(store.reshape(number * rows, depth), wk, wv, after)


def mixer_body(
    first, qkv_ref, lg_ref, ex_ref, rate_ref, gain_ref, s_ref, after_ref, out_ref, s_out_ref
):
    ri = lax.broadcasted_iota(jnp.int32, (128, 128), 0)
    ci = lax.broadcasted_iota(jnp.int32, (128, 128), 1)
    same = (ri >= BLOCK) == (ci >= BLOCK)
    lower = same & (ri >= ci)
    strict = same & (ri > ci)
    upper = same & (ri <= ci)
    diag = ri == ci
    top = lax.broadcasted_iota(jnp.int32, (128, 1), 0) < BLOCK
    rate = jnp.where(top, rate_ref[0], rate_ref[1])
    pieces = []
    for n in range(qkv_ref.shape[1]):
        lg = lg_ref[n * BLOCK : (n + 1) * BLOCK, :]
        at = (first + n) * BLOCK
        ex = jnp.concatenate([ex_ref[0:1, at : at + BLOCK], ex_ref[1:2, at : at + BLOCK]], axis=1)
        beta = jax.nn.sigmoid(jnp.concatenate([lg[:, 0:1], lg[:, 1:2]], axis=0))
        pre = jnp.concatenate([lg[:, 2:3], lg[:, 3:4]], axis=0)
        extra = jnp.sum(jnp.where(diag, ex, 0.0), axis=1, keepdims=True)
        soft = jnp.maximum(pre, 0.0) + jnp.log1p(jnp.exp(-jnp.abs(pre)))
        g = extra - rate * soft
        g_row = jnp.sum(jnp.where(diag, g, 0.0), axis=0, keepdims=True)
        c = jnp.sum(jnp.where(lower, g_row, 0.0), axis=1, keepdims=True)
        total = jnp.sum(jnp.where(same, g_row, 0.0), axis=1, keepdims=True)
        c_row = jnp.sum(jnp.where(upper, g, 0.0), axis=0, keepdims=True)
        damping = jnp.where(lower, jnp.exp(jnp.where(lower, c - c_row, 0.0)), 0.0)
        q = qkv_ref[0, n].astype(F32)
        k = qkv_ref[1, n].astype(F32)
        v = qkv_ref[2, n].astype(F32)
        q = q * (lax.rsqrt(jnp.sum(q * q, axis=1, keepdims=True) + EPS) * 128**-0.5)
        k = k * lax.rsqrt(jnp.sum(k * k, axis=1, keepdims=True) + EPS)
        kb = k * beta
        decay = jnp.exp(c)
        k16 = k.astype(BF16)
        power = jnp.where(strict, nt(kb.astype(BF16), k16) * damping, 0.0)
        within = (nt(q.astype(BF16), k16) * damping).astype(BF16)
        inverse = jnp.where(diag, 1.0, 0.0) - power
        p16 = power.astype(BF16)
        for _ in range(5):
            p16 = nn(p16, p16).astype(BF16)
            inverse = inverse + nn(inverse.astype(BF16), p16)
        inv16 = inverse.astype(BF16)
        mix = nn(inv16, (kb * decay).astype(BF16)).astype(BF16)
        base = nn(inv16, (v * beta).astype(BF16))
        q_dec = (q * decay).astype(BF16)
        k_tail = (k * jnp.exp(total - c)).astype(BF16)
        pieces.append((mix, base, within, q_dec, k_tail, jnp.exp(total)))
    state = [s_ref[0], s_ref[1]]
    for n, (mix, base, within, q_dec, k_tail, keep) in enumerate(pieces):
        fresh, far = [], []
        for h in range(2):
            rows = slice(h * BLOCK, (h + 1) * BLOCK)
            both = nn(jnp.concatenate([mix[rows], q_dec[rows]], axis=0), state[h].astype(BF16))
            fresh.append(base[rows] - both[:BLOCK])
            far.append(both[BLOCK:])
        f16 = jnp.concatenate(fresh, axis=0).astype(BF16)
        recur = jnp.concatenate(far, axis=0) + nn(within, f16)
        for h in range(2):
            rows = slice(h * BLOCK, (h + 1) * BLOCK)
            state[h] = state[h] * keep[h * BLOCK : h * BLOCK + 1] + tn(k_tail[rows], f16[rows])
        scale = lax.rsqrt(jnp.mean(recur * recur, axis=1, keepdims=True) + EPS)
        out_ref[n] = recur * scale * gain_ref[...]
    s_out_ref[0] = state[0]
    s_out_ref[1] = state[1]


def mixer(qkv, logits, extra, rate, gain, state, after, first, number):
    at = first // number
    return pl.pallas_call(
        functools.partial(mixer_body, first),
        grid=(1,),
        in_specs=[
            pl.BlockSpec((3, number, 128, 128), lambda i: (0, at, 0, 0)),
            pl.BlockSpec((number * BLOCK, logits.shape[1]), lambda i: (at, 0)),
            pl.BlockSpec(extra.shape, lambda i: (0, 0)),
            pl.BlockSpec(memory_space=pltpu.SMEM),
            pl.BlockSpec((1, 128), lambda i: (0, 0)),
            pl.BlockSpec((2, 128, 128), lambda i: (0, 0, 0)),
            pl.BlockSpec(memory_space=pl.ANY),
        ],
        out_specs=[
            pl.BlockSpec((number, 128, 128), lambda i: (0, 0, 0)),
            pl.BlockSpec((2, 128, 128), lambda i: (0, 0, 0)),
        ],
        out_shape=[
            jax.ShapeDtypeStruct((number, 128, 128), F32),
            jax.ShapeDtypeStruct((2, 128, 128), F32),
        ],
        compiler_params=params(16),
        cost_estimate=cost(number * 1000 * MIB // 2, number * 300 * 1024),
        name="mixer",
    )(qkv, logits, extra, rate, gain, state, after)


def find_parts(count, own_ref, *refs):
    messages, refs = refs[:count], refs[count:]
    (kv_ref, mate_ref, _, sums_ref, stats_ref, codes_ref) = refs
    chip, core = own_ref[0], own_ref[1]
    rows = messages[0].shape[0]
    row = lax.broadcasted_iota(jnp.int32, (8, 128), 0)
    lane = lax.broadcasted_iota(jnp.int32, (8, 128), 1)
    before = (
        lax.broadcasted_iota(jnp.int32, (128, 128), 0) < lax.broadcasted_iota(jnp.int32, (128, 128), 1)
    )
    before = jnp.where(before, 1.0, 0.0).astype(BF16)
    blocks = (rows - 8) // 128
    left = lax.broadcasted_iota(jnp.int32, (BLOCK, 128), 1) < BLOCK
    spots = []
    for n in range(count):
        table = messages[n][rows - 8 :, :].astype(F32)
        entry = jnp.concatenate([table[4:8], table[4:8]], axis=0)
        name = table.astype(jnp.int32) - 1
        hit = ((name >> 1) == chip) & (row < 4) & (lane < blocks)
        ones = jnp.where(hit, 1.0, 0.0)
        rank = nn(ones.astype(BF16), before)
        sums = jnp.sum(ones, axis=1, keepdims=True)
        first, second, third = sums[0:1], sums[1:2], sums[2:3]
        rank = rank + jnp.where(row > 0, first, 0.0)
        rank = rank + jnp.where(row > 1, second, 0.0)
        rank = rank + jnp.where(row > 2, third, 0.0)
        far = jnp.where((name & 1) == core, 0.0, 16.0)
        code = lane.astype(F32) * 32.0 + far + entry + 1.0
        for r in range(SLOTS):
            value = jnp.where(hit & (rank == float(r)), code, 0.0)
            spots.append(jnp.sum(value).astype(jnp.int32))
    for i, spot in enumerate(spots):
        codes_ref[i] = spot

    def some(step, _):
        found = []
        for n in range(count):
            for r in range(2):
                i = n * SLOTS + step * 2 + r
                spot = jnp.maximum(codes_ref[i] - 1, 0)
                at = pl.multiple_of((spot >> 5) * 128, 128)
                q = messages[n][pl.ds(at, 128), :]
                kv = jnp.where((spot & 16) != 0, mate_ref[spot & 15], kv_ref[spot & 15])
                both = nt(kv[0:128], q)
                scores = jnp.where(left, both[:BLOCK], both[BLOCK:]) * 128**-0.5
                found.append((i, scores, kv[128:256]))
        weighed = []
        for i, scores, values in found:
            peak = jnp.max(scores, axis=0, keepdims=True)
            expo = jnp.exp(scores - peak)
            denom = jnp.sum(expo, axis=0, keepdims=True)
            split = jnp.concatenate(
                [jnp.where(left, expo, 0.0), jnp.where(left, 0.0, expo)], axis=0
            ).astype(BF16)
            weighed.append((i, nn(values, split), jnp.where(row == 0, peak, denom)))
        for i, sums, stats in weighed:
            sums_ref[i], stats_ref[i] = sums, stats
        return 0

    lax.fori_loop(0, SLOTS // 2, some, 0)


def parts(own, messages, kv, kv_mate, after):
    count = len(messages)
    total = count * SLOTS
    whole = pl.BlockSpec(memory_space=VMEM)
    scalars = pl.BlockSpec(memory_space=pltpu.SMEM)
    return pl.pallas_call(
        functools.partial(find_parts, count),
        in_specs=[scalars] + [whole] * (count + 2) + [pl.BlockSpec(memory_space=pl.ANY)],
        out_specs=[whole, whole, scalars],
        out_shape=[
            jax.ShapeDtypeStruct((total, 128, 128), F32),
            jax.ShapeDtypeStruct((total, 8, 128), F32),
            jax.ShapeDtypeStruct((total,), jnp.int32),
        ],
        compiler_params=params(12),
        cost_estimate=cost(count * 400 * MIB, count * 500 * 1024),
        name="parts",
    )(own, *messages, kv, kv_mate, after)


def split3(x):
    high = x.astype(BF16)
    rest = x - high.astype(F32)
    mid = rest.astype(BF16)
    low = (rest - mid.astype(F32)).astype(BF16)
    return high.astype(F32), mid.astype(F32), low.astype(F32)


def begin(out_ref):
    pad = lax.broadcasted_iota(jnp.int32, (8, 128), 0)
    none = jnp.where(pad == 0, NONE, 0.0).astype(BF16)
    for b in range(out_ref.shape[0]):
        out_ref[b, 0:128, :] = jnp.zeros((128, 128), BF16)
        out_ref[b, 128:136, :] = none


def merge_into(first, codes_ref, sums_ref, stats_ref, out_ref):
    for r in range(SLOTS):
        code = codes_ref[first + r]

        @pl.when(code > 0)
        def _():
            b = (code - 1) >> 5
            peak, denom = stats_ref[first + r, 0:1, :], stats_ref[first + r, 1:2, :]
            stats = out_ref[b, 128:136, :].astype(F32)
            m_old = stats[0:1] + stats[1:2] + stats[2:3]
            l_old = stats[3:4] + stats[4:5] + stats[5:6]
            m_new = jnp.maximum(m_old, peak)
            keep = jnp.exp(m_old - m_new)
            gain = jnp.exp(peak - m_new)
            l_new = l_old * keep + denom * gain
            zero = jnp.zeros((2, 128), F32)
            fresh = jnp.concatenate(split3(m_new) + split3(l_new) + (zero,), axis=0)
            out_ref[b, 128:136, :] = fresh.astype(BF16)
            mixed = out_ref[b, 0:128, :].astype(F32) * keep + sums_ref[first + r] * gain
            out_ref[b, 0:128, :] = mixed.astype(BF16)


def merge_body(first, start, own_ref, codes_ref, sums_ref, stats_ref, after_ref, *refs):
    out_ref = refs[-1]
    if start == "all":
        begin(out_ref)
    elif start == "core_0":
        pl.when(own_ref[1] == 0)(lambda: begin(out_ref))
    merge_into(first, codes_ref, sums_ref, stats_ref, out_ref)


def far_body(own_ref, q_ref, kv_ref, mate_ref, after_ref, out_ref, sums_ref, stats_ref, codes_ref):
    @pl.when(own_ref[1] != 0)
    def _():
        find_parts(1, own_ref, q_ref, kv_ref, mate_ref, after_ref, sums_ref, stats_ref, codes_ref)
        begin(out_ref)
        merge_into(0, codes_ref, sums_ref, stats_ref, out_ref)


def far_message(own, q, kv, kv_mate, blocks, after):
    whole = pl.BlockSpec(memory_space=VMEM)
    return pl.pallas_call(
        far_body,
        in_specs=[pl.BlockSpec(memory_space=pltpu.SMEM), whole, whole, whole]
        + [pl.BlockSpec(memory_space=pl.ANY)],
        out_specs=whole,
        out_shape=jax.ShapeDtypeStruct((blocks, 136, 128), BF16),
        scratch_shapes=[
            VMEM((SLOTS, 128, 128), F32),
            VMEM((SLOTS, 8, 128), F32),
            pltpu.SMEM((SLOTS,), jnp.int32),
        ],
        compiler_params=params(10),
        cost_estimate=cost(500 * MIB, 500 * 1024),
        name="far",
    )(own, q, kv, kv_mate, after)


def merge(own, part, blocks, after, msg=None, start="none"):
    (sums, stats, codes), n = part
    whole = pl.BlockSpec(memory_space=VMEM)
    scalars = pl.BlockSpec(memory_space=pltpu.SMEM)
    more = () if msg is None else (msg,)
    return pl.pallas_call(
        functools.partial(merge_body, n * SLOTS, start),
        in_specs=[scalars, scalars, whole, whole, pl.BlockSpec(memory_space=pl.ANY)]
        + [whole] * len(more),
        out_specs=whole,
        out_shape=jax.ShapeDtypeStruct((blocks, 136, 128), BF16),
        input_output_aliases={5: 0} if more else {},
        compiler_params=params(8),
        cost_estimate=cost(100 * MIB, 900 * 1024),
        name="merge",
    )(own, codes, sums, stats, after, *more)


def finish_body(count, lg_ref, *refs):
    messages, normed, out_ref = refs[:count], refs[count:-1], refs[-1]
    for b in range(messages[0].shape[0]):
        peaks, denoms = [], []
        for message in messages:
            s = message[b, 128:136, :].astype(F32)
            peaks.append(s[0:1] + s[1:2] + s[2:3])
            denoms.append(s[3:4] + s[4:5] + s[5:6])
        peak = functools.reduce(jnp.maximum, peaks)
        gains = [jnp.exp(p - peak) for p in peaks]
        denom = sum(d * g for d, g in zip(denoms, gains))
        sums = sum(m[b, 0:128, :].astype(F32) * g for m, g in zip(messages, gains))
        retrieved = (sums / denom).T
        lg = lg_ref[b * BLOCK : (b + 1) * BLOCK, :]
        gate = jax.nn.sigmoid(jnp.concatenate([lg[:, 4:5], lg[:, 5:6]], axis=0))
        mixed = (normed[b][0] + gate * retrieved).astype(BF16)
        for h in range(2):
            out_ref[b * BLOCK : (b + 1) * BLOCK, h * 128 : (h + 1) * 128] = mixed[
                h * BLOCK : (h + 1) * BLOCK
            ]


def finish(messages, logits, normed):
    rows = logits.shape[0]
    return pl.pallas_call(
        functools.partial(finish_body, len(messages)),
        out_shape=jax.ShapeDtypeStruct((rows, 256), BF16),
        compiler_params=params(16),
        cost_estimate=cost(100 * MIB, 2 * MIB),
        name="finish",
    )(logits, *messages, *normed)


def per_device(
    tokens,
    owners,
    entries,
    store,
    mixer_query_weight,
    mixer_key_weight,
    mixer_value_weight,
    strength_weight,
    decay_weight,
    head_decay_rate,
    extra_forgetting_exponent,
    output_norm_gain,
    retrieval_query_weight,
    passage_key_weight,
    passage_value_weight,
    retrieval_gate_weight,
):
    devices = lax.axis_size("st")
    me = lax.axis_index("st")
    core = lax.rem(me, 2)
    reach = devices // 4
    blocks = owners.shape[0]

    step = [2 if i % 2 == 0 else -2 for i in range(devices)]

    def hops(lane, chips=1, ends=False):
        pairs = [(i, (i + chips * step[i]) % devices) for i in range(devices)]
        if lane == "other" and ends:
            pairs = [(i ^ 1, j) for i, j in pairs]
        return pairs

    def send(x, pairs):
        return lax.ppermute(x, "st", pairs)

    def second(pairs):
        return [(i, j) for i, j in pairs if i % 2 == 1]

    def reverse(pairs):
        return [(j, i) for i, j in pairs]

    query = query_message(tokens, retrieval_query_weight, owners.T, entries.T)
    own = {0: query}
    other = {}
    gain = output_norm_gain.reshape(1, 128)
    extra = extra_forgetting_exponent.T
    where_own = jnp.stack([me >> 1, me & 1])
    part = {}

    def compute_parts(names, after):
        messages = [(own if lane == "own" else other)[h] for lane, h in names]
        result = parts(where_own, messages, kv_own, kv_mate, after)
        for n, name in enumerate(names):
            part[name] = (result, n)
        return result[1]

    lanes = {"own": own, "other": other}
    for name, lane in lanes.items():
        lane[2] = send(query, hops(name, 2, True))
    kv_own = project_passages(store, passage_key_weight, passage_value_weight, query)
    kv_mate = send(kv_own, [(i, i ^ 1) for i in range(devices)])
    for name, lane in lanes.items():
        lane[1] = send(query, hops(name, 1, True))
    for h in range(3, reach + 1):
        for name, lane in lanes.items():
            pairs = hops(name)
            lane[h] = send(lane[h - 1], second(pairs) if h == reach else pairs)
    qkv, logits = mixer_inputs(
        tokens,
        mixer_query_weight,
        mixer_key_weight,
        mixer_value_weight,
        strength_weight.T,
        decay_weight.T,
        retrieval_gate_weight.T,
        own[2],
    )
    last = compute_parts([("own", 0)], logits)
    for h in ORDER:
        last = compute_parts([("own", h), ("other", h)], last)

    normed = []
    state = jnp.zeros((2, 128, 128), F32)

    def mixer_step(after):
        nonlocal state
        result, state = mixer(
            qkv, logits, extra, head_decay_rate, gain, state, after, len(normed), 1
        )
        normed.append(result)
        return state

    came = {}
    near = {}
    for h in range(reach, 1, -1):
        for name, lane in lanes.items():
            if h == reach:
                last = far_message(where_own, lane[h], kv_own, kv_mate, blocks, last)
            else:
                start = "core_0" if h == reach - 1 else "none"
                last = merge(where_own, part[(name, h)], blocks, last, came[name], start)
            pairs = hops(name, 2, True) if h == 2 else hops(name)
            pairs = second(pairs) if h == reach else pairs
            came[name] = send(last, reverse(pairs))
        last = mixer_step(last)
        if h in NEAR:
            name = NEAR[h]
            last = merge(where_own, part[(name, 1)], blocks, last, None, "all")
            near[name] = send(last, reverse(hops(name, 1, True)))
    while len(normed) < blocks:
        last = mixer_step(last)
    came["own"] = merge(where_own, part[("own", 0)], blocks, last, came["own"])
    messages = (came["own"], came["other"], near["own"], near["other"])
    return finish(messages, logits, normed)


ORDER = (2, 3, 1, 4, 5, 6, 7)
NEAR = {5: "own", 4: "other"}


def solution(mesh):
    return jax.shard_map(
        per_device,
        mesh=mesh,
        in_specs=(
            P(("grp", "st"), None),
            P(("grp", "st"), None),
            P(("grp", "st"), None),
            P(("grp", "st"), None, None),
            P(None, "tp"),
            P(None, "tp"),
            P(None, "tp"),
            P(None, "tp"),
            P(None, "tp"),
            P("tp"),
            P(("grp", "st"), "tp"),
            P(),
            P(None, "tp"),
            P(None, "tp"),
            P(None, "tp"),
            P(None, "tp"),
        ),
        out_specs=P(("grp", "st"), "tp"),
        check_vma=False,
    )
```

profile of v0, /device:TPU:38, one launch (start us, length us, event | category | flops | bytes accessed | tf_op | source)
XLA Modules:
  0.0 171.3 jit_solution(9575820037887384127)
XLA Ops:
  1.4 3.0 %query.1.after_ref.refs_0_ = bf16[1032,128]{1,0:T(8,128)(2,1)S(1)} custom-call(bf16[512,2048]{1,0:T(8,128)(2,1)} %x_hbm.3, bf16[2048,256]{1,0:T(8,128)(2,1)} %w_hbm.1, s32[4,8]{1,0:T(4,128)S(1)} %bitcast.10, s32[4,8]{1,0:T(4,128)S(1)} %bitcast.11), custom_call_target="tpu_custom_call" | custom-call | flops 536870912 | bytes 3145728 | tf_op jit(solution)/shard_map/query/pallas_call | solution.py:91
  4.4 5.1 %collective-permute-start = (bf16[1032,128]{1,0:T(8,128)(2,1)S(1)}, bf16[1032,128]{1,0:T(8,128)(2,1)S(1)}, u32[]{:S(2)}, u32[]{:S(2)}) collective-permute-start(bf16[1032,128]{1,0:T(8,128)(2,1)S(1)} %query.1.after_ref.refs_0_), channel_id=1, source_target_pairs={{0,16},{4,116},{8,24},{12,124},{16,32},{20,4},{24,40},{28,12},{32,... | collective-permute-start | bytes 792584 | tf_op jit(solution)/shard_map/ppermute | solution.py:561
  9.5 16.6 %collective-permute-start.2 = (bf16[1032,128]{1,0:T(8,128)(2,1)S(1)}, bf16[1032,128]{1,0:T(8,128)(2,1)S(1)}, u32[]{:S(2)}, u32[]{:S(2)}) collective-permute-start(bf16[1032,128]{1,0:T(8,128)(2,1)S(1)} %query.1.after_ref.refs_0_), channel_id=1, source_target_pairs={{4,16},{0,116},{12,24},{8,124},{20,32},{16,4},{28,40},{24,12},{36,... | collective-permute-start | bytes 792584 | tf_op jit(solution)/shard_map/ppermute | solution.py:561
  26.1 11.8 %collective-permute-done.after_ref.refs_0_ = bf16[1032,128]{1,0:T(8,128)(2,1)S(1)} collective-permute-done((bf16[1032,128]{1,0:T(8,128)(2,1)S(1)}, bf16[1032,128]{1,0:T(8,128)(2,1)S(1)}, u32[]{:S(2)}, u32[]{:S(2)}) %collective-permute-start) | collective-permute-done | bytes 264224 | tf_op jit(solution)/shard_map/ppermute | solution.py:561
  38.0 2.2 %collective-permute-start.9 = (bf16[1032,128]{1,0:T(8,128)(2,1)S(1)}, bf16[1032,128]{1,0:T(8,128)(2,1)S(1)}, u32[]{:S(2)}, u32[]{:S(2)}) collective-permute-start(bf16[1032,128]{1,0:T(8,128)(2,1)S(1)} %collective-permute-done.after_ref.refs_0_), channel_id=1, source_target_pairs={{0,8},{4,124},{8,16},{12,4},{16,24},{20,12},{24,32},{28,20},{32,40... | collective-permute-start | bytes 792584 | tf_op jit(solution)/shard_map/ppermute | solution.py:561
  40.2 5.2 %passages.1.refs_1_.refs_2_.kv_ref = bf16[16,256,128]{2,1,0:T(8,128)(2,1)S(1)} custom-call(bf16[1024,2048]{1,0:T(8,128)(2,1)} %bitcast.31, bf16[2048,256]{1,0:T(8,128)(2,1)} %wk_hbm.3, bf16[2048,256]{1,0:T(8,128)(2,1)} %wv_hbm.3, bf16[1032,128]{1,0:T(8,128)(2,1)S(1)} %query.1.after_ref.refs_0_), custom_call_target="tpu_custom_call" | custom-call | flops 2147483648 | bytes 4194304 | tf_op jit(solution)/shard_map/passages/pallas_call | solution.py:210
  45.5 1.4 collective-permute-start.1
  47.6 1.5 collective-permute-done.3.refs_1_
  50.2 4.3 %collective-permute-done.10.refs_0_ = bf16[1032,128]{1,0:T(8,128)(2,1)S(1)} collective-permute-done((bf16[1032,128]{1,0:T(8,128)(2,1)S(1)}, bf16[1032,128]{1,0:T(8,128)(2,1)S(1)}, u32[]{:S(2)}, u32[]{:S(2)}) %collective-permute-start.10) | collective-permute-done | bytes 264224 | tf_op jit(solution)/shard_map/ppermute | solution.py:561
  54.5 2.9 %collective-permute-done.4.refs_1_ = bf16[1032,128]{1,0:T(8,128)(2,1)} collective-permute-done((bf16[1032,128]{1,0:T(8,128)(2,1)S(1)}, bf16[1032,128]{1,0:T(8,128)(2,1)}, u32[]{:S(2)}, u32[]{:S(2)}) %collective-permute-start.4) | collective-permute-done | bytes 264224 | tf_op jit(solution)/shard_map/ppermute | solution.py:561
  57.4 4.7 %collective-permute-done.11.refs_0_ = bf16[1032,128]{1,0:T(8,128)(2,1)S(1)} collective-permute-done((bf16[1032,128]{1,0:T(8,128)(2,1)S(1)}, bf16[1032,128]{1,0:T(8,128)(2,1)S(1)}, u32[]{:S(2)}, u32[]{:S(2)}) %collective-permute-start.11) | collective-permute-done | bytes 264224 | tf_op jit(solution)/shard_map/ppermute | solution.py:561
  62.1 3.2 %collective-permute-done.5.refs_1_ = bf16[1032,128]{1,0:T(8,128)(2,1)} collective-permute-done((bf16[1032,128]{1,0:T(8,128)(2,1)}, bf16[1032,128]{1,0:T(8,128)(2,1)}, u32[]{:S(2)}, u32[]{:S(2)}) %collective-permute-start.5) | collective-permute-done | bytes 264224 | tf_op jit(solution)/shard_map/ppermute | solution.py:561
  65.4 5.4 %mixer_inputs.1 = (bf16[3,8,128,128]{3,2,1,0:T(8,128)(2,1)S(1)}, f32[512,8]{1,0:T(8,128)S(1)}) custom-call(bf16[512,2048]{1,0:T(8,128)(2,1)} %x_hbm.3, bf16[2048,256]{1,0:T(8,128)(2,1)} %wq_hbm.1, bf16[2048,256]{1,0:T(8,128)(2,1)} %wk_hbm.2, bf16[2048,256]{1,0:T(8,128)(2,1)} %wv_hbm.2, bf16[2,2048]{1,0:T(2,128)(2,1)S(1)} %bitcast.12, ...), custom_call_target="tpu_custom_call" | custom-call | flops 1610612736 | bytes 5242880 | tf_op jit(solution)/shard_map/mixer_inputs/pallas_call | solution.py:153
  70.8 1.2 collective-permute-done.12.refs_0_
  72.1 1.8 %parts.8 = (f32[4,128,128]{2,1,0:T(8,128)S(1)}, f32[4,8,128]{2,1,0:T(8,128)S(1)}, s32[4]{0:T(128)S(1)}) custom-call(s32[2]{0:T(128)S(1)} %pad_add_fusion.own_ref, bf16[1032,128]{1,0:T(8,128)(2,1)S(1)} %query.1.after_ref.refs_0_, bf16[16,256,128]{2,1,0:T(8,128)(2,1)S(1)} %passages.1.refs_1_.refs_2_.kv_ref, ...), custom_call_target="tpu_custom_call" | custom-call | flops 419430400 | bytes 512000 | tf_op jit(solution)/shard_map/parts/pallas_call | solution.py:388
  73.8 3.8 %collective-permute-done.6.refs_1_ = bf16[1032,128]{1,0:T(8,128)(2,1)S(1)} collective-permute-done((bf16[1032,128]{1,0:T(8,128)(2,1)}, bf16[1032,128]{1,0:T(8,128)(2,1)S(1)}, u32[]{:S(2)}, u32[]{:S(2)}) %collective-permute-start.6) | collective-permute-done | bytes 264224 | tf_op jit(solution)/shard_map/ppermute | solution.py:561
  77.6 2.0 %parts.9 = (f32[8,128,128]{2,1,0:T(8,128)S(1)}, f32[8,8,128]{2,1,0:T(8,128)S(1)}, s32[8]{0:T(128)S(1)}) custom-call(s32[2]{0:T(128)S(1)} %pad_add_fusion.own_ref, bf16[1032,128]{1,0:T(8,128)(2,1)S(1)} %collective-permute-done.after_ref.refs_0_, bf16[1032,128]{1,0:T(8,128)(2,1)S(1)} %collective-permute-done.2.refs_1_, ...), custom_call_target="tpu_custom_call" | custom-call | flops 838860800 | bytes 1024000 | tf_op jit(solution)/shard_map/parts/pallas_call | solution.py:388
  79.7 2.0 %parts.10 = (f32[8,128,128]{2,1,0:T(8,128)S(1)}, f32[8,8,128]{2,1,0:T(8,128)S(1)}, s32[8]{0:T(128)S(1)}) custom-call(s32[2]{0:T(128)S(1)} %pad_add_fusion.own_ref, bf16[1032,128]{1,0:T(8,128)(2,1)S(1)} %copy-done.3, bf16[1032,128]{1,0:T(8,128)(2,1)S(1)} %copy-done.5, bf16[16,256,128]{2,1,0:T(8,128)(2,1)S(1)} %passages.1.refs_1_.refs_2_.kv_ref, ...), custom_call_target="tpu_custom_call" | custom-call | flops 838860800 | bytes 1024000 | tf_op jit(solution)/shard_map/parts/pallas_call | solution.py:388
  81.8 2.5 %parts.11 = (f32[8,128,128]{2,1,0:T(8,128)S(1)}, f32[8,8,128]{2,1,0:T(8,128)S(1)}, s32[8]{0:T(128)S(1)}) custom-call(s32[2]{0:T(128)S(1)} %pad_add_fusion.own_ref, bf16[1032,128]{1,0:T(8,128)(2,1)} %collective-permute-done.15.refs_0_, bf16[1032,128]{1,0:T(8,128)(2,1)} %collective-permute-done.16.refs_1_, ...), custom_call_target="tpu_custom_call" | custom-call | flops 838860800 | bytes 1024000 | tf_op jit(solution)/shard_map/parts/pallas_call | solution.py:388
  85.0 2.5 %parts.12 = (f32[8,128,128]{2,1,0:T(8,128)S(1)}, f32[8,8,128]{2,1,0:T(8,128)S(1)}, s32[8]{0:T(128)S(1)}) custom-call(s32[2]{0:T(128)S(1)} %pad_add_fusion.own_ref, bf16[1032,128]{1,0:T(8,128)(2,1)S(1)} %collective-permute-done.10.refs_0_, bf16[1032,128]{1,0:T(8,128)(2,1)} %collective-permute-done.4.refs_1_, ...), custom_call_target="tpu_custom_call" | custom-call | flops 838860800 | bytes 1024000 | tf_op jit(solution)/shard_map/parts/pallas_call | solution.py:388
  88.2 2.5 %parts.13 = (f32[8,128,128]{2,1,0:T(8,128)S(1)}, f32[8,8,128]{2,1,0:T(8,128)S(1)}, s32[8]{0:T(128)S(1)}) custom-call(s32[2]{0:T(128)S(1)} %pad_add_fusion.own_ref, bf16[1032,128]{1,0:T(8,128)(2,1)S(1)} %collective-permute-done.11.refs_0_, bf16[1032,128]{1,0:T(8,128)(2,1)} %collective-permute-done.5.refs_1_, ...), custom_call_target="tpu_custom_call" | custom-call | flops 838860800 | bytes 1024000 | tf_op jit(solution)/shard_map/parts/pallas_call | solution.py:388
  90.7 2.5 %parts.14 = (f32[8,128,128]{2,1,0:T(8,128)S(1)}, f32[8,8,128]{2,1,0:T(8,128)S(1)}, s32[8]{0:T(128)S(1)}) custom-call(s32[2]{0:T(128)S(1)} %pad_add_fusion.own_ref, bf16[1032,128]{1,0:T(8,128)(2,1)} %collective-permute-done.12.refs_0_, bf16[1032,128]{1,0:T(8,128)(2,1)S(1)} %collective-permute-done.6.refs_1_, ...), custom_call_target="tpu_custom_call" | custom-call | flops 838860800 | bytes 1024000 | tf_op jit(solution)/shard_map/parts/pallas_call | solution.py:388
  93.2 2.0 %parts.15 = (f32[8,128,128]{2,1,0:T(8,128)S(1)}, f32[8,8,128]{2,1,0:T(8,128)S(1)}, s32[8]{0:T(128)S(1)}) custom-call(s32[2]{0:T(128)S(1)} %pad_add_fusion.own_ref, bf16[1032,128]{1,0:T(8,128)(2,1)S(1)} %collective-permute-done.13.refs_0_, bf16[1032,128]{1,0:T(8,128)(2,1)S(1)} %collective-permute-done.7.refs_1_, ...), custom_call_target="tpu_custom_call" | custom-call | flops 838860800 | bytes 1024000 | tf_op jit(solution)/shard_map/parts/pallas_call | solution.py:388
  97.8 2.3 %mixer.8 = (f32[1,128,128]{2,1,0:T(8,128)S(1)}, f32[2,128,128]{2,1,0:T(8,128)S(1)}) custom-call(bf16[3,8,128,128]{3,2,1,0:T(8,128)(2,1)S(1)} %get-tuple-element.51.qkv_ref, f32[512,8]{1,0:T(8,128)S(1)} %get-tuple-element.47.refs_3_.lg_ref, f32[2,512]{1,0:T(2,128)S(1)} %bitcast.15, f32[2]{0:T(128)S(1)} %copy-done.10, f32[1,128]{1,0:T(1,128)S(1)} %bitcast.23, ...), custom_call_target="tpu_custom_call" | custom-call | flops 524288000 | bytes 307200 | tf_op jit(solution)/shard_map/mixer/pallas_call | solution.py:295
  100.8 3.3 %collective-permute-start.19 = (bf16[8,136,128]{2,1,0:T(8,128)(2,1)S(1)}, bf16[8,136,128]{2,1,0:T(8,128)(2,1)S(1)}, u32[]{:S(2)}, u32[]{:S(2)}) collective-permute-start(bf16[8,136,128]{2,1,0:T(8,128)(2,1)S(1)} %merge.15.after_ref), channel_id=1, source_target_pairs={{8,0},{124,4},{16,8},{4,12},{24,16},{12,20},{32,24},{20,28},{40,32... | collective-permute-start | bytes 835592 | tf_op jit(solution)/shard_map/ppermute | solution.py:561
  105.0 2.3 %mixer.9 = (f32[1,128,128]{2,1,0:T(8,128)S(1)}, f32[2,128,128]{2,1,0:T(8,128)S(1)}) custom-call(bf16[3,8,128,128]{3,2,1,0:T(8,128)(2,1)S(1)} %get-tuple-element.51.qkv_ref, f32[512,8]{1,0:T(8,128)S(1)} %get-tuple-element.47.refs_3_.lg_ref, f32[2,512]{1,0:T(2,128)S(1)} %bitcast.16, f32[2]{0:T(128)S(1)} %copy-done.10, f32[1,128]{1,0:T(1,128)S(1)} %bitcast.24, ...), custom_call_target="tpu_custom_call" | custom-call | flops 524288000 | bytes 307200 | tf_op jit(solution)/shard_map/mixer/pallas_call | solution.py:295
  107.3 0.9 collective-permute-done.19.refs_0_
  108.9 3.8 %collective-permute-start.21 = (bf16[8,136,128]{2,1,0:T(8,128)(2,1)S(1)}, bf16[8,136,128]{2,1,0:T(8,128)(2,1)S(1)}, u32[]{:S(2)}, u32[]{:S(2)}) collective-permute-start(bf16[8,136,128]{2,1,0:T(8,128)(2,1)S(1)} %merge.17.after_ref), channel_id=1, source_target_pairs={{8,0},{124,4},{16,8},{4,12},{24,16},{12,20},{32,24},{20,28},{40,32... | collective-permute-start | bytes 835592 | tf_op jit(solution)/shard_map/ppermute | solution.py:561
  113.3 2.3 %collective-permute-start.22 = (bf16[8,136,128]{2,1,0:T(8,128)(2,1)S(1)}, bf16[8,136,128]{2,1,0:T(8,128)(2,1)S(1)}, u32[]{:S(2)}, u32[]{:S(2)}) collective-permute-start(bf16[8,136,128]{2,1,0:T(8,128)(2,1)S(1)} %merge.18.after_ref), channel_id=1, source_target_pairs={{8,0},{124,4},{16,8},{4,12},{24,16},{12,20},{32,24},{20,28},{40,32... | collective-permute-start | bytes 835592 | tf_op jit(solution)/shard_map/ppermute | solution.py:561
  115.7 2.3 %mixer.10 = (f32[1,128,128]{2,1,0:T(8,128)S(1)}, f32[2,128,128]{2,1,0:T(8,128)S(1)}) custom-call(bf16[3,8,128,128]{3,2,1,0:T(8,128)(2,1)S(1)} %get-tuple-element.51.qkv_ref, f32[512,8]{1,0:T(8,128)S(1)} %get-tuple-element.47.refs_3_.lg_ref, f32[2,512]{1,0:T(2,128)S(1)} %bitcast.17, f32[2]{0:T(128)S(1)} %copy-done.10, f32[1,128]{1,0:T(1,128)S(1)} %bitcast.25, ...), custom_call_target="tpu_custom_call" | custom-call | flops 524288000 | bytes 307200 | tf_op jit(solution)/shard_map/mixer/pallas_call | solution.py:295
  118.7 2.8 %collective-permute-start.23 = (bf16[8,136,128]{2,1,0:T(8,128)(2,1)S(1)}, bf16[8,136,128]{2,1,0:T(8,128)(2,1)S(1)}, u32[]{:S(2)}, u32[]{:S(2)}) collective-permute-start(bf16[8,136,128]{2,1,0:T(8,128)(2,1)S(1)} %merge.19.after_ref), channel_id=1, source_target_pairs={{8,0},{124,4},{16,8},{4,12},{24,16},{12,20},{32,24},{20,28},{40,32... | collective-permute-start | bytes 835592 | tf_op jit(solution)/shard_map/ppermute | solution.py:561
  122.1 2.1 %collective-permute-start.24 = (bf16[8,136,128]{2,1,0:T(8,128)(2,1)S(1)}, bf16[8,136,128]{2,1,0:T(8,128)(2,1)S(1)}, u32[]{:S(2)}, u32[]{:S(2)}) collective-permute-start(bf16[8,136,128]{2,1,0:T(8,128)(2,1)S(1)} %merge.20.after_ref), channel_id=1, source_target_pairs={{8,0},{124,4},{16,8},{4,12},{24,16},{12,20},{32,24},{20,28},{40,32... | collective-permute-start | bytes 835592 | tf_op jit(solution)/shard_map/ppermute | solution.py:561
  124.2 2.3 %mixer.11 = (f32[1,128,128]{2,1,0:T(8,128)S(1)}, f32[2,128,128]{2,1,0:T(8,128)S(1)}) custom-call(bf16[3,8,128,128]{3,2,1,0:T(8,128)(2,1)S(1)} %get-tuple-element.51.qkv_ref, f32[512,8]{1,0:T(8,128)S(1)} %get-tuple-element.47.refs_3_.lg_ref, f32[2,512]{1,0:T(2,128)S(1)} %bitcast.18, f32[2]{0:T(128)S(1)} %copy-done.10, f32[1,128]{1,0:T(1,128)S(1)} %bitcast.26, ...), custom_call_target="tpu_custom_call" | custom-call | flops 524288000 | bytes 307200 | tf_op jit(solution)/shard_map/mixer/pallas_call | solution.py:295
  127.9 2.1 %collective-permute-start.25 = (bf16[8,136,128]{2,1,0:T(8,128)(2,1)S(1)}, bf16[8,136,128]{2,1,0:T(8,128)(2,1)S(1)}, u32[]{:S(2)}, u32[]{:S(2)}) collective-permute-start(bf16[8,136,128]{2,1,0:T(8,128)(2,1)S(1)} %merge.22.after_ref), channel_id=1, source_target_pairs={{8,0},{124,4},{16,8},{4,12},{24,16},{12,20},{32,24},{20,28},{40,32... | collective-permute-start | bytes 835592 | tf_op jit(solution)/shard_map/ppermute | solution.py:561
  130.6 2.3 %collective-permute-start.26 = (bf16[8,136,128]{2,1,0:T(8,128)(2,1)S(1)}, bf16[8,136,128]{2,1,0:T(8,128)(2,1)S(1)}, u32[]{:S(2)}, u32[]{:S(2)}) collective-permute-start(bf16[8,136,128]{2,1,0:T(8,128)(2,1)S(1)} %merge.23.after_ref), channel_id=1, source_target_pairs={{8,0},{124,4},{16,8},{4,12},{24,16},{12,20},{32,24},{20,28},{40,32... | collective-permute-start | bytes 835592 | tf_op jit(solution)/shard_map/ppermute | solution.py:561
  132.9 2.3 %mixer.12 = (f32[1,128,128]{2,1,0:T(8,128)S(1)}, f32[2,128,128]{2,1,0:T(8,128)S(1)}) custom-call(bf16[3,8,128,128]{3,2,1,0:T(8,128)(2,1)S(1)} %get-tuple-element.51.qkv_ref, f32[512,8]{1,0:T(8,128)S(1)} %get-tuple-element.47.refs_3_.lg_ref, f32[2,512]{1,0:T(2,128)S(1)} %bitcast.19, f32[2]{0:T(128)S(1)} %copy-done.10, f32[1,128]{1,0:T(1,128)S(1)} %bitcast.27, ...), custom_call_target="tpu_custom_call" | custom-call | flops 524288000 | bytes 307200 | tf_op jit(solution)/shard_map/mixer/pallas_call | solution.py:295
  136.6 1.8 %collective-permute-start.27 = (bf16[8,136,128]{2,1,0:T(8,128)(2,1)S(1)}, bf16[8,136,128]{2,1,0:T(8,128)(2,1)S(1)}, u32[]{:S(2)}, u32[]{:S(2)}) collective-permute-start(bf16[8,136,128]{2,1,0:T(8,128)(2,1)S(1)} %merge.25.after_ref), channel_id=1, source_target_pairs={{8,0},{124,4},{16,8},{4,12},{24,16},{12,20},{32,24},{20,28},{40,32... | collective-permute-start | bytes 835592 | tf_op jit(solution)/shard_map/ppermute | solution.py:561
  139.1 2.3 %collective-permute-start.28 = (bf16[8,136,128]{2,1,0:T(8,128)(2,1)S(1)}, bf16[8,136,128]{2,1,0:T(8,128)(2,1)S(1)}, u32[]{:S(2)}, u32[]{:S(2)}) collective-permute-start(bf16[8,136,128]{2,1,0:T(8,128)(2,1)S(1)} %merge.26.after_ref), channel_id=1, source_target_pairs={{8,0},{124,4},{16,8},{4,12},{24,16},{12,20},{32,24},{20,28},{40,32... | collective-permute-start | bytes 835592 | tf_op jit(solution)/shard_map/ppermute | solution.py:561
  141.4 2.3 %mixer.13 = (f32[1,128,128]{2,1,0:T(8,128)S(1)}, f32[2,128,128]{2,1,0:T(8,128)S(1)}) custom-call(bf16[3,8,128,128]{3,2,1,0:T(8,128)(2,1)S(1)} %get-tuple-element.51.qkv_ref, f32[512,8]{1,0:T(8,128)S(1)} %get-tuple-element.47.refs_3_.lg_ref, f32[2,512]{1,0:T(2,128)S(1)} %bitcast.20, f32[2]{0:T(128)S(1)} %copy-done.10, f32[1,128]{1,0:T(1,128)S(1)} %bitcast.28, ...), custom_call_target="tpu_custom_call" | custom-call | flops 524288000 | bytes 307200 | tf_op jit(solution)/shard_map/mixer/pallas_call | solution.py:295
  145.2 1.9 %collective-permute-start.31 = (bf16[8,136,128]{2,1,0:T(8,128)(2,1)S(1)}, bf16[8,136,128]{2,1,0:T(8,128)(2,1)S(1)}, u32[]{:S(2)}, u32[]{:S(2)}) collective-permute-start(bf16[8,136,128]{2,1,0:T(8,128)(2,1)S(1)} %merge.21.after_ref), channel_id=1, source_target_pairs={{8,0},{124,4},{16,8},{4,12},{24,16},{12,20},{32,24},{20,28},{40,32... | collective-permute-start | bytes 835592 | tf_op jit(solution)/shard_map/ppermute | solution.py:561
  147.1 2.8 %collective-permute-start.32 = (bf16[8,136,128]{2,1,0:T(8,128)(2,1)S(1)}, bf16[8,136,128]{2,1,0:T(8,128)(2,1)S(1)}, u32[]{:S(2)}, u32[]{:S(2)}) collective-permute-start(bf16[8,136,128]{2,1,0:T(8,128)(2,1)S(1)} %merge.24.after_ref), channel_id=1, source_target_pairs={{8,4},{124,0},{16,12},{4,8},{24,20},{12,16},{32,28},{20,24},{40,36... | collective-permute-start | bytes 835592 | tf_op jit(solution)/shard_map/ppermute | solution.py:561
  150.6 0.9 collective-permute-start.30
  151.5 2.3 %mixer.14 = (f32[1,128,128]{2,1,0:T(8,128)S(1)}, f32[2,128,128]{2,1,0:T(8,128)S(1)}) custom-call(bf16[3,8,128,128]{3,2,1,0:T(8,128)(2,1)S(1)} %get-tuple-element.51.qkv_ref, f32[512,8]{1,0:T(8,128)S(1)} %get-tuple-element.47.refs_3_.lg_ref, f32[2,512]{1,0:T(2,128)S(1)} %bitcast.21, f32[2]{0:T(128)S(1)} %copy-done.10, f32[1,128]{1,0:T(1,128)S(1)} %bitcast.29, ...), custom_call_target="tpu_custom_call" | custom-call | flops 524288000 | bytes 307200 | tf_op jit(solution)/shard_map/mixer/pallas_call | solution.py:295
  153.8 2.3 %mixer.15 = (f32[1,128,128]{2,1,0:T(8,128)S(1)}, f32[2,128,128]{2,1,0:T(8,128)S(1)}) custom-call(bf16[3,8,128,128]{3,2,1,0:T(8,128)(2,1)S(1)} %get-tuple-element.51.qkv_ref, f32[512,8]{1,0:T(8,128)S(1)} %get-tuple-element.47.refs_3_.lg_ref, f32[2,512]{1,0:T(2,128)S(1)} %bitcast.22, f32[2]{0:T(128)S(1)} %copy-done.10, f32[1,128]{1,0:T(1,128)S(1)} %bitcast.30, ...), custom_call_target="tpu_custom_call" | custom-call | flops 524288000 | bytes 307200 | tf_op jit(solution)/shard_map/mixer/pallas_call | solution.py:295
  156.8 2.0 %collective-permute-done.31.refs_2_ = bf16[8,136,128]{2,1,0:T(8,128)(2,1)S(1)} collective-permute-done((bf16[8,136,128]{2,1,0:T(8,128)(2,1)S(1)}, bf16[8,136,128]{2,1,0:T(8,128)(2,1)S(1)}, u32[]{:S(2)}, u32[]{:S(2)}) %collective-permute-start.31) | collective-permute-done | bytes 278560 | tf_op jit(solution)/shard_map/ppermute | solution.py:561
  158.9 2.9 %collective-permute-done.32.refs_3_ = bf16[8,136,128]{2,1,0:T(8,128)(2,1)S(1)} collective-permute-done((bf16[8,136,128]{2,1,0:T(8,128)(2,1)S(1)}, bf16[8,136,128]{2,1,0:T(8,128)(2,1)S(1)}, u32[]{:S(2)}, u32[]{:S(2)}) %collective-permute-start.32) | collective-permute-done | bytes 278560 | tf_op jit(solution)/shard_map/ppermute | solution.py:561
  161.8 8.1 %collective-permute-done.30.refs_1_ = bf16[8,136,128]{2,1,0:T(8,128)(2,1)S(1)} collective-permute-done((bf16[8,136,128]{2,1,0:T(8,128)(2,1)S(1)}, bf16[8,136,128]{2,1,0:T(8,128)(2,1)S(1)}, u32[]{:S(2)}, u32[]{:S(2)}) %collective-permute-start.30) | collective-permute-done | bytes 278560 | tf_op jit(solution)/shard_map/ppermute | solution.py:561
  169.9 1.4 finish.1
  (81 shorter events, 17.8 us)
Async XLA Ops:
  0.0 0.7 copy-start
  0.7 0.7 copy-start.1
  4.4 61.1 %copy-start.6 = (bf16[2048,2]{0,1:T(2,128)(2,1)S(1)}, bf16[2048,2]{0,1:T(2,128)(2,1)}, u32[]{:S(2)}) copy-start(bf16[2048,2]{0,1:T(2,128)(2,1)} %param.23) | copy-start | bytes 24580
  4.4 61.0 %copy-start.7 = (bf16[2048,2]{0,1:T(2,128)(2,1)S(1)}, bf16[2048,2]{0,1:T(2,128)(2,1)}, u32[]{:S(2)}) copy-start(bf16[2048,2]{0,1:T(2,128)(2,1)} %param.24) | copy-start | bytes 24580
  4.4 61.0 %copy-start.8 = (bf16[2048,2]{0,1:T(2,128)(2,1)S(1)}, bf16[2048,2]{0,1:T(2,128)(2,1)}, u32[]{:S(2)}) copy-start(bf16[2048,2]{0,1:T(2,128)(2,1)} %param.31) | copy-start | bytes 24580
  4.4 33.6 %collective-permute-start = (bf16[1032,128]{1,0:T(8,128)(2,1)S(1)}, bf16[1032,128]{1,0:T(8,128)(2,1)S(1)}, u32[]{:S(2)}, u32[]{:S(2)}) collective-permute-start(bf16[1032,128]{1,0:T(8,128)(2,1)S(1)} %query.1.after_ref.refs_0_), channel_id=1, source_target_pairs={{0,16},{4,116},{8,24},{12,124},{16,32},{20,4},{24,40},{28,12},{32,... | collective-permute-start | bytes 792584 | tf_op jit(solution)/shard_map/ppermute | solution.py:561
  9.5 30.7 %collective-permute-start.2 = (bf16[1032,128]{1,0:T(8,128)(2,1)S(1)}, bf16[1032,128]{1,0:T(8,128)(2,1)S(1)}, u32[]{:S(2)}, u32[]{:S(2)}) collective-permute-start(bf16[1032,128]{1,0:T(8,128)(2,1)S(1)} %query.1.after_ref.refs_0_), channel_id=1, source_target_pairs={{4,16},{0,116},{12,24},{8,124},{20,32},{16,4},{28,40},{24,12},{36,... | collective-permute-start | bytes 792584 | tf_op jit(solution)/shard_map/ppermute | solution.py:561
  38.0 8.9 %collective-permute-start.9 = (bf16[1032,128]{1,0:T(8,128)(2,1)S(1)}, bf16[1032,128]{1,0:T(8,128)(2,1)S(1)}, u32[]{:S(2)}, u32[]{:S(2)}) collective-permute-start(bf16[1032,128]{1,0:T(8,128)(2,1)S(1)} %collective-permute-done.after_ref.refs_0_), channel_id=1, source_target_pairs={{0,8},{4,124},{8,16},{12,4},{16,24},{20,12},{24,32},{28,20},{32,40... | collective-permute-start | bytes 792584 | tf_op jit(solution)/shard_map/ppermute | solution.py:561
  40.2 8.9 %collective-permute-start.3 = (bf16[1032,128]{1,0:T(8,128)(2,1)S(1)}, bf16[1032,128]{1,0:T(8,128)(2,1)S(1)}, u32[]{:S(2)}, u32[]{:S(2)}) collective-permute-start(bf16[1032,128]{1,0:T(8,128)(2,1)S(1)} %collective-permute-done.2.refs_1_), channel_id=1, source_target_pairs={{0,8},{4,124},{8,16},{12,4},{16,24},{20,12},{24,32},{28,20},{32,40... | collective-permute-start | bytes 792584 | tf_op jit(solution)/shard_map/ppermute | solution.py:561
  45.5 26.6 %collective-permute-start.1 = (bf16[16,256,128]{2,1,0:T(8,128)(2,1)S(1)}, bf16[16,256,128]{2,1,0:T(8,128)(2,1)S(1)}, u32[]{:S(2)}, u32[]{:S(2)}) collective-permute-start(bf16[16,256,128]{2,1,0:T(8,128)(2,1)S(1)} %passages.1.refs_1_.refs_2_.kv_ref), channel_id=1, source_target_pairs={{0,4},{4,0},{8,12},{12,8},{16,20},{20,16},{24,28},{28,24},{32,36},... | collective-permute-start | bytes 3145736 | tf_op jit(solution)/shard_map/ppermute | solution.py:561
  46.9 7.6 %collective-permute-start.10 = (bf16[1032,128]{1,0:T(8,128)(2,1)S(1)}, bf16[1032,128]{1,0:T(8,128)(2,1)S(1)}, u32[]{:S(2)}, u32[]{:S(2)}) collective-permute-start(bf16[1032,128]{1,0:T(8,128)(2,1)S(1)} %collective-permute-done.9.refs_0_), channel_id=1, source_target_pairs={{0,8},{4,124},{8,16},{12,4},{16,24},{20,12},{24,32},{28,20},{32,40... | collective-permute-start | bytes 792584 | tf_op jit(solution)/shard_map/ppermute | solution.py:561
  46.9 0.7 copy-start.2
  49.1 8.3 %collective-permute-start.4 = (bf16[1032,128]{1,0:T(8,128)(2,1)S(1)}, bf16[1032,128]{1,0:T(8,128)(2,1)}, u32[]{:S(2)}, u32[]{:S(2)}) collective-permute-start(bf16[1032,128]{1,0:T(8,128)(2,1)S(1)} %collective-permute-done.3.refs_1_), channel_id=1, source_target_pairs={{0,8},{4,124},{8,16},{12,4},{16,24},{20,12},{24,32},{28,20},{32,40... | collective-permute-start | bytes 792584 | tf_op jit(solution)/shard_map/ppermute | solution.py:561
  49.4 0.7 copy-start.4
  54.5 7.6 %collective-permute-start.11 = (bf16[1032,128]{1,0:T(8,128)(2,1)S(1)}, bf16[1032,128]{1,0:T(8,128)(2,1)S(1)}, u32[]{:S(2)}, u32[]{:S(2)}) collective-permute-start(bf16[1032,128]{1,0:T(8,128)(2,1)S(1)} %collective-permute-done.10.refs_0_), channel_id=1, source_target_pairs={{0,8},{4,124},{8,16},{12,4},{16,24},{20,12},{24,32},{28,20},{32,40... | collective-permute-start | bytes 792584 | tf_op jit(solution)/shard_map/ppermute | solution.py:561
  57.4 7.9 %collective-permute-start.5 = (bf16[1032,128]{1,0:T(8,128)(2,1)}, bf16[1032,128]{1,0:T(8,128)(2,1)}, u32[]{:S(2)}, u32[]{:S(2)}) collective-permute-start(bf16[1032,128]{1,0:T(8,128)(2,1)} %collective-permute-done.4.refs_1_), channel_id=1, source_target_pairs={{0,8},{4,124},{8,16},{12,4},{16,24},{20,12},{24,32},{28,20},{32,40... | collective-permute-start | bytes 792584 | tf_op jit(solution)/shard_map/ppermute | solution.py:561
  62.1 10.0 %collective-permute-start.12 = (bf16[1032,128]{1,0:T(8,128)(2,1)S(1)}, bf16[1032,128]{1,0:T(8,128)(2,1)}, u32[]{:S(2)}, u32[]{:S(2)}) collective-permute-start(bf16[1032,128]{1,0:T(8,128)(2,1)S(1)} %collective-permute-done.11.refs_0_), channel_id=1, source_target_pairs={{0,8},{4,124},{8,16},{12,4},{16,24},{20,12},{24,32},{28,20},{32,40... | collective-permute-start | bytes 792584 | tf_op jit(solution)/shard_map/ppermute | solution.py:561
  62.1 19.7 %collective-permute-start.15 = (bf16[1032,128]{1,0:T(8,128)(2,1)S(1)}, bf16[1032,128]{1,0:T(8,128)(2,1)}, u32[]{:S(2)}, u32[]{:S(2)}) collective-permute-start(bf16[1032,128]{1,0:T(8,128)(2,1)S(1)} %query.1.after_ref.refs_0_), channel_id=1, source_target_pairs={{0,8},{4,124},{8,16},{12,4},{16,24},{20,12},{24,32},{28,20},{32,40... | collective-permute-start | bytes 792584 | tf_op jit(solution)/shard_map/ppermute | solution.py:561
  62.1 19.7 %collective-permute-start.16 = (bf16[1032,128]{1,0:T(8,128)(2,1)S(1)}, bf16[1032,128]{1,0:T(8,128)(2,1)}, u32[]{:S(2)}, u32[]{:S(2)}) collective-permute-start(bf16[1032,128]{1,0:T(8,128)(2,1)S(1)} %query.1.after_ref.refs_0_), channel_id=1, source_target_pairs={{4,8},{0,124},{12,16},{8,4},{20,24},{16,12},{28,32},{24,20},{36,40... | collective-permute-start | bytes 792584 | tf_op jit(solution)/shard_map/ppermute | solution.py:561
  65.4 12.3 %collective-permute-start.6 = (bf16[1032,128]{1,0:T(8,128)(2,1)}, bf16[1032,128]{1,0:T(8,128)(2,1)S(1)}, u32[]{:S(2)}, u32[]{:S(2)}) collective-permute-start(bf16[1032,128]{1,0:T(8,128)(2,1)} %collective-permute-done.5.refs_1_), channel_id=1, source_target_pairs={{0,8},{4,124},{8,16},{12,4},{16,24},{20,12},{24,32},{28,20},{32,40... | collective-permute-start | bytes 792584 | tf_op jit(solution)/shard_map/ppermute | solution.py:561
  70.8 8.9 %copy-start.3 = (bf16[1032,128]{1,0:T(8,128)(2,1)S(1)}, bf16[1032,128]{1,0:T(8,128)(2,1)}, u32[]{:S(2)}) copy-start(bf16[1032,128]{1,0:T(8,128)(2,1)} %copy-done.2) | copy-start | bytes 792580
  70.8 8.9 %copy-start.5 = (bf16[1032,128]{1,0:T(8,128)(2,1)S(1)}, bf16[1032,128]{1,0:T(8,128)(2,1)}, u32[]{:S(2)}) copy-start(bf16[1032,128]{1,0:T(8,128)(2,1)} %copy-done.4) | copy-start | bytes 792580
  72.1 12.3 %collective-permute-start.13 = (bf16[1032,128]{1,0:T(8,128)(2,1)}, bf16[1032,128]{1,0:T(8,128)(2,1)S(1)}, u32[]{:S(2)}, u32[]{:S(2)}) collective-permute-start(bf16[1032,128]{1,0:T(8,128)(2,1)} %collective-permute-done.12.refs_0_), channel_id=1, source_target_pairs={{0,8},{4,124},{8,16},{12,4},{16,24},{20,12},{24,32},{28,20},{32,40... | collective-permute-start | bytes 792584 | tf_op jit(solution)/shard_map/ppermute | solution.py:561
  77.6 9.9 %collective-permute-start.7 = (bf16[1032,128]{1,0:T(8,128)(2,1)S(1)}, bf16[1032,128]{1,0:T(8,128)(2,1)S(1)}, u32[]{:S(2)}, u32[]{:S(2)}) collective-permute-start(bf16[1032,128]{1,0:T(8,128)(2,1)S(1)} %collective-permute-done.6.refs_1_), channel_id=1, source_target_pairs={{0,8},{4,124},{8,16},{12,4},{16,24},{20,12},{24,32},{28,20},{32,40... | collective-permute-start | bytes 792584 | tf_op jit(solution)/shard_map/ppermute | solution.py:561
  84.3 10.9 %collective-permute-start.14 = (bf16[1032,128]{1,0:T(8,128)(2,1)S(1)}, bf16[1032,128]{1,0:T(8,128)(2,1)S(1)}, u32[]{:S(2)}, u32[]{:S(2)}) collective-permute-start(bf16[1032,128]{1,0:T(8,128)(2,1)S(1)} %collective-permute-done.13.refs_0_), channel_id=1, source_target_pairs={{4,124},{12,4},{20,12},{28,20},{36,28},{44,36},{52,44},{60,52},{68... | collective-permute-start | bytes 792584 | tf_op jit(solution)/shard_map/ppermute | solution.py:561
  87.5 9.0 %collective-permute-start.8 = (bf16[1032,128]{1,0:T(8,128)(2,1)S(1)}, bf16[1032,128]{1,0:T(8,128)(2,1)S(1)}, u32[]{:S(2)}, u32[]{:S(2)}) collective-permute-start(bf16[1032,128]{1,0:T(8,128)(2,1)S(1)} %collective-permute-done.7.refs_1_), channel_id=1, source_target_pairs={{4,124},{12,4},{20,12},{28,20},{36,28},{44,36},{52,44},{60,52},{68... | collective-permute-start | bytes 792584 | tf_op jit(solution)/shard_map/ppermute | solution.py:561
  93.1 4.6 %copy-start.9 = (f32[512,2]{0,1:T(2,128)S(1)}, f32[512,2]{0,1:T(2,128)}, u32[]{:S(2)}) copy-start(f32[512,2]{0,1:T(2,128)} %param.26) | copy-start | bytes 12292
  93.1 4.6 %copy-start.10 = (f32[2]{0:T(128)S(1)}, f32[2]{0:T(128)}, u32[]{:S(2)}) copy-start(f32[2]{0:T(128)} %rate_ref.15) | copy-start | bytes 28
  93.1 4.6 %copy-start.11 = (f32[128]{0:T(128)S(1)}, f32[128]{0:T(128)}, u32[]{:S(2)}) copy-start(f32[128]{0:T(128)} %param.27) | copy-start | bytes 1540
  95.8 4.3 %collective-permute-start.17 = (bf16[8,136,128]{2,1,0:T(8,128)(2,1)S(1)}, bf16[8,136,128]{2,1,0:T(8,128)(2,1)S(1)}, u32[]{:S(2)}, u32[]{:S(2)}) collective-permute-start(bf16[8,136,128]{2,1,0:T(8,128)(2,1)S(1)} %far.2.after_ref), channel_id=1, source_target_pairs={{124,4},{4,12},{12,20},{20,28},{28,36},{36,44},{44,52},{52,60},{60... | collective-permute-start | bytes 835592 | tf_op jit(solution)/shard_map/ppermute | solution.py:561
  97.0 7.1 %collective-permute-start.18 = (bf16[8,136,128]{2,1,0:T(8,128)(2,1)S(1)}, bf16[8,136,128]{2,1,0:T(8,128)(2,1)S(1)}, u32[]{:S(2)}, u32[]{:S(2)}) collective-permute-start(bf16[8,136,128]{2,1,0:T(8,128)(2,1)S(1)} %far.3.after_ref), channel_id=1, source_target_pairs={{124,4},{4,12},{12,20},{20,28},{28,36},{36,44},{44,52},{52,60},{60... | collective-permute-start | bytes 835592 | tf_op jit(solution)/shard_map/ppermute | solution.py:561
  100.8 7.4 %collective-permute-start.19 = (bf16[8,136,128]{2,1,0:T(8,128)(2,1)S(1)}, bf16[8,136,128]{2,1,0:T(8,128)(2,1)S(1)}, u32[]{:S(2)}, u32[]{:S(2)}) collective-permute-start(bf16[8,136,128]{2,1,0:T(8,128)(2,1)S(1)} %merge.15.after_ref), channel_id=1, source_target_pairs={{8,0},{124,4},{16,8},{4,12},{24,16},{12,20},{32,24},{20,28},{40,32... | collective-permute-start | bytes 835592 | tf_op jit(solution)/shard_map/ppermute | solution.py:561
  104.8 7.8 %collective-permute-start.20 = (bf16[8,136,128]{2,1,0:T(8,128)(2,1)S(1)}, bf16[8,136,128]{2,1,0:T(8,128)(2,1)S(1)}, u32[]{:S(2)}, u32[]{:S(2)}) collective-permute-start(bf16[8,136,128]{2,1,0:T(8,128)(2,1)S(1)} %merge.16.after_ref), channel_id=1, source_target_pairs={{8,0},{124,4},{16,8},{4,12},{24,16},{12,20},{32,24},{20,28},{40,32... | collective-permute-start | bytes 835592 | tf_op jit(solution)/shard_map/ppermute | solution.py:561
  108.9 9.1 %collective-permute-start.21 = (bf16[8,136,128]{2,1,0:T(8,128)(2,1)S(1)}, bf16[8,136,128]{2,1,0:T(8,128)(2,1)S(1)}, u32[]{:S(2)}, u32[]{:S(2)}) collective-permute-start(bf16[8,136,128]{2,1,0:T(8,128)(2,1)S(1)} %merge.17.after_ref), channel_id=1, source_target_pairs={{8,0},{124,4},{16,8},{4,12},{24,16},{12,20},{32,24},{20,28},{40,32... | collective-permute-start | bytes 835592 | tf_op jit(solution)/shard_map/ppermute | solution.py:561
  113.3 8.1 %collective-permute-start.22 = (bf16[8,136,128]{2,1,0:T(8,128)(2,1)S(1)}, bf16[8,136,128]{2,1,0:T(8,128)(2,1)S(1)}, u32[]{:S(2)}, u32[]{:S(2)}) collective-permute-start(bf16[8,136,128]{2,1,0:T(8,128)(2,1)S(1)} %merge.18.after_ref), channel_id=1, source_target_pairs={{8,0},{124,4},{16,8},{4,12},{24,16},{12,20},{32,24},{20,28},{40,32... | collective-permute-start | bytes 835592 | tf_op jit(solution)/shard_map/ppermute | solution.py:561
  118.7 8.5 %collective-permute-start.23 = (bf16[8,136,128]{2,1,0:T(8,128)(2,1)S(1)}, bf16[8,136,128]{2,1,0:T(8,128)(2,1)S(1)}, u32[]{:S(2)}, u32[]{:S(2)}) collective-permute-start(bf16[8,136,128]{2,1,0:T(8,128)(2,1)S(1)} %merge.19.after_ref), channel_id=1, source_target_pairs={{8,0},{124,4},{16,8},{4,12},{24,16},{12,20},{32,24},{20,28},{40,32... | collective-permute-start | bytes 835592 | tf_op jit(solution)/shard_map/ppermute | solution.py:561
  122.1 7.9 %collective-permute-start.24 = (bf16[8,136,128]{2,1,0:T(8,128)(2,1)S(1)}, bf16[8,136,128]{2,1,0:T(8,128)(2,1)S(1)}, u32[]{:S(2)}, u32[]{:S(2)}) collective-permute-start(bf16[8,136,128]{2,1,0:T(8,128)(2,1)S(1)} %merge.20.after_ref), channel_id=1, source_target_pairs={{8,0},{124,4},{16,8},{4,12},{24,16},{12,20},{32,24},{20,28},{40,32... | collective-permute-start | bytes 835592 | tf_op jit(solution)/shard_map/ppermute | solution.py:561
  127.9 8.1 %collective-permute-start.25 = (bf16[8,136,128]{2,1,0:T(8,128)(2,1)S(1)}, bf16[8,136,128]{2,1,0:T(8,128)(2,1)S(1)}, u32[]{:S(2)}, u32[]{:S(2)}) collective-permute-start(bf16[8,136,128]{2,1,0:T(8,128)(2,1)S(1)} %merge.22.after_ref), channel_id=1, source_target_pairs={{8,0},{124,4},{16,8},{4,12},{24,16},{12,20},{32,24},{20,28},{40,32... | collective-permute-start | bytes 835592 | tf_op jit(solution)/shard_map/ppermute | solution.py:561
  130.6 7.9 %collective-permute-start.26 = (bf16[8,136,128]{2,1,0:T(8,128)(2,1)S(1)}, bf16[8,136,128]{2,1,0:T(8,128)(2,1)S(1)}, u32[]{:S(2)}, u32[]{:S(2)}) collective-permute-start(bf16[8,136,128]{2,1,0:T(8,128)(2,1)S(1)} %merge.23.after_ref), channel_id=1, source_target_pairs={{8,0},{124,4},{16,8},{4,12},{24,16},{12,20},{32,24},{20,28},{40,32... | collective-permute-start | bytes 835592 | tf_op jit(solution)/shard_map/ppermute | solution.py:561
  136.6 7.2 %collective-permute-start.27 = (bf16[8,136,128]{2,1,0:T(8,128)(2,1)S(1)}, bf16[8,136,128]{2,1,0:T(8,128)(2,1)S(1)}, u32[]{:S(2)}, u32[]{:S(2)}) collective-permute-start(bf16[8,136,128]{2,1,0:T(8,128)(2,1)S(1)} %merge.25.after_ref), channel_id=1, source_target_pairs={{8,0},{124,4},{16,8},{4,12},{24,16},{12,20},{32,24},{20,28},{40,32... | collective-permute-start | bytes 835592 | tf_op jit(solution)/shard_map/ppermute | solution.py:561
  139.1 10.9 %collective-permute-start.28 = (bf16[8,136,128]{2,1,0:T(8,128)(2,1)S(1)}, bf16[8,136,128]{2,1,0:T(8,128)(2,1)S(1)}, u32[]{:S(2)}, u32[]{:S(2)}) collective-permute-start(bf16[8,136,128]{2,1,0:T(8,128)(2,1)S(1)} %merge.26.after_ref), channel_id=1, source_target_pairs={{8,0},{124,4},{16,8},{4,12},{24,16},{12,20},{32,24},{20,28},{40,32... | collective-permute-start | bytes 835592 | tf_op jit(solution)/shard_map/ppermute | solution.py:561
  144.4 11.8 %collective-permute-start.29 = (bf16[8,136,128]{2,1,0:T(8,128)(2,1)S(1)}, bf16[8,136,128]{2,1,0:T(8,128)(2,1)S(1)}, u32[]{:S(2)}, u32[]{:S(2)}) collective-permute-start(bf16[8,136,128]{2,1,0:T(8,128)(2,1)S(1)} %merge.27.after_ref), channel_id=1, source_target_pairs={{16,0},{116,4},{24,8},{124,12},{32,16},{4,20},{40,24},{12,28},{48,... | collective-permute-start | bytes 835592 | tf_op jit(solution)/shard_map/ppermute | solution.py:561
  145.2 13.7 %collective-permute-start.31 = (bf16[8,136,128]{2,1,0:T(8,128)(2,1)S(1)}, bf16[8,136,128]{2,1,0:T(8,128)(2,1)S(1)}, u32[]{:S(2)}, u32[]{:S(2)}) collective-permute-start(bf16[8,136,128]{2,1,0:T(8,128)(2,1)S(1)} %merge.21.after_ref), channel_id=1, source_target_pairs={{8,0},{124,4},{16,8},{4,12},{24,16},{12,20},{32,24},{20,28},{40,32... | collective-permute-start | bytes 835592 | tf_op jit(solution)/shard_map/ppermute | solution.py:561
  147.1 14.7 %collective-permute-start.32 = (bf16[8,136,128]{2,1,0:T(8,128)(2,1)S(1)}, bf16[8,136,128]{2,1,0:T(8,128)(2,1)S(1)}, u32[]{:S(2)}, u32[]{:S(2)}) collective-permute-start(bf16[8,136,128]{2,1,0:T(8,128)(2,1)S(1)} %merge.24.after_ref), channel_id=1, source_target_pairs={{8,4},{124,0},{16,12},{4,8},{24,20},{12,16},{32,28},{20,24},{40,36... | collective-permute-start | bytes 835592 | tf_op jit(solution)/shard_map/ppermute | solution.py:561
  150.6 19.3 %collective-permute-start.30 = (bf16[8,136,128]{2,1,0:T(8,128)(2,1)S(1)}, bf16[8,136,128]{2,1,0:T(8,128)(2,1)S(1)}, u32[]{:S(2)}, u32[]{:S(2)}) collective-permute-start(bf16[8,136,128]{2,1,0:T(8,128)(2,1)S(1)} %merge.28.after_ref), channel_id=1, source_target_pairs={{16,4},{116,0},{24,12},{124,8},{32,20},{4,16},{40,28},{12,24},{48,... | collective-permute-start | bytes 835592 | tf_op jit(solution)/shard_map/ppermute | solution.py:561
where the time goes:
time: 172 us; the launch traced here: 171 us
  Pallas kernels  62.3 us (36%)
  starting transfers between devices  57.9 us (34%)
  waiting for transfers between devices  47.6 us (28%)
  local copies, waits for them, and re-layouts  2.86 us (2%)
    ppermute x33, starting transfers between devices, send(): return lax.ppermute(x, 'st', pairs)  57.9 us
    ppermute x33, waiting for transfers between devices, send(): return lax.ppermute(x, 'st', pairs)  47.6 us
    pallas_call x8, Pallas kernels, mixer(): pl.pallas_call(functools.partial(mixer_body, first), grid=(1,), in_specs=...  18.7 us
    pallas_call x8, Pallas kernels, parts(): pl.pallas_call(functools.partial(find_parts, count), in_specs=[scalars] +...  17.8 us
    pallas_call x15, Pallas kernels, merge(): pl.pallas_call(functools.partial(merge_body, n * SLOTS, start), in_specs=...  9.76 us
    pallas_call x1, Pallas kernels, mixer_inputs(): pl.pallas_call(mixed_body, in_specs=[hbm] * 4 + [whole] * 3 + [pl.BlockSp...  5.38 us
    pallas_call x1, Pallas kernels, project_passages(): pl.pallas_call(passages_body, in_specs=[hbm, hbm, hbm, pl.BlockSpec(memor...  5.23 us
  transfers between devices with their start and end apart: 33, of which 12 were waited for; matrix products, arithmetic and copies ran while one was open for 0% of the time, Pallas kernels for 34%

commit v1 on v0

--- a/solution.py
+++ b/solution.py
@@ -551,11 +551,9 @@
 
     step = [2 if i % 2 == 0 else -2 for i in range(devices)]
 
-    def hops(lane, chips=1, ends=False):
-        pairs = [(i, (i + chips * step[i]) % devices) for i in range(devices)]
-        if lane == "other" and ends:
-            pairs = [(i ^ 1, j) for i, j in pairs]
-        return pairs
+    def hops(lane, end):
+        ring = [(i, (i + step[i]) % devices) for i in range(devices)]
+        return [(i ^ 1, j) for i, j in ring] if lane == "other" and end else ring
 
     def send(x, pairs):
         return lax.ppermute(x, "st", pairs)
@@ -582,16 +580,17 @@
         return result[1]
 
     lanes = {"own": own, "other": other}
-    for name, lane in lanes.items():
-        lane[2] = send(query, hops(name, 2, True))
-    kv_own = project_passages(store, passage_key_weight, passage_value_weight, query)
-    kv_mate = send(kv_own, [(i, i ^ 1) for i in range(devices)])
-    for name, lane in lanes.items():
-        lane[1] = send(query, hops(name, 1, True))
-    for h in range(3, reach + 1):
+
+    def pairs(name, h):
+        hop = hops(name, h == 1)
+        return second(hop) if h == reach else hop
+
+    for h in range(1, reach + 1):
         for name, lane in lanes.items():
-            pairs = hops(name)
-            lane[h] = send(lane[h - 1], second(pairs) if h == reach else pairs)
+            lane[h] = send(lane[h - 1] if h > 1 else query, pairs(name, h))
+        if h == 1:
+            kv_own = project_passages(store, passage_key_weight, passage_value_weight, query)
+            kv_mate = send(kv_own, [(i, i ^ 1) for i in range(devices)])
     qkv, logits = mixer_inputs(
         tokens,
         mixer_query_weight,
@@ -600,10 +599,10 @@
         strength_weight.T,
         decay_weight.T,
         retrieval_gate_weight.T,
-        own[2],
+        other[1],
     )
     last = compute_parts([("own", 0)], logits)
-    for h in ORDER:
+    for h in range(1, reach):
         last = compute_parts([("own", h), ("other", h)], last)
 
     normed = []
@@ -618,31 +617,20 @@
         return state
 
     came = {}
-    near = {}
-    for h in range(reach, 1, -1):
+    for h in range(reach, 0, -1):
         for name, lane in lanes.items():
             if h == reach:
                 last = far_message(where_own, lane[h], kv_own, kv_mate, blocks, last)
             else:
                 start = "core_0" if h == reach - 1 else "none"
                 last = merge(where_own, part[(name, h)], blocks, last, came[name], start)
-            pairs = hops(name, 2, True) if h == 2 else hops(name)
-            pairs = second(pairs) if h == reach else pairs
-            came[name] = send(last, reverse(pairs))
-        last = mixer_step(last)
-        if h in NEAR:
-            name = NEAR[h]
-            last = merge(where_own, part[(name, 1)], blocks, last, None, "all")
-            near[name] = send(last, reverse(hops(name, 1, True)))
+            came[name] = send(last, reverse(pairs(name, h)))
+        if len(normed) < blocks:
+            last = mixer_step(last)
     while len(normed) < blocks:
         last = mixer_step(last)
     came["own"] = merge(where_own, part[("own", 0)], blocks, last, came["own"])
-    messages = (came["own"], came["other"], near["own"], near["other"])
-    return finish(messages, logits, normed)
-
-
-ORDER = (2, 3, 1, 4, 5, 6, 7)
-NEAR = {5: "own", 4: "other"}
+    return finish((came["own"], came["other"]), logits, normed)
 
 
 def solution(mesh):

time: 172 us -> 165 us (0.959)
  the two profiles are of different devices: /device:TPU:38 before, /device:TPU:33 now
where the time goes in v1:
time: 165 us
  starting transfers between devices  69.2 us (42%)
  Pallas kernels  63.9 us (39%)
  waiting for transfers between devices  27.8 us (17%)
  local copies, waits for them, and re-layouts  3.52 us (2%)
    ppermute x33, starting transfers between devices, send(): return lax.ppermute(x, 'st', pairs)  69.2 us
    ppermute x33, waiting for transfers between devices, send(): return lax.ppermute(x, 'st', pairs)  27.8 us
    pallas_call x8, Pallas kernels, mixer(): pl.pallas_call(functools.partial(mixer_body, first), grid=(1,), in_specs=...  18.7 us
    pallas_call x8, Pallas kernels, parts(): pl.pallas_call(functools.partial(find_parts, count), in_specs=[scalars] +...  17.4 us
    pallas_call x15, Pallas kernels, merge(): pl.pallas_call(functools.partial(merge_body, n * SLOTS, start), in_specs=...  9.61 us
    pallas_call x1, Pallas kernels, mixer_inputs(): pl.pallas_call(mixed_body, in_specs=[hbm] * 4 + [whole] * 3 + [pl.BlockSp...  5.37 us
    pallas_call x1, Pallas kernels, project_passages(): pl.pallas_call(passages_body, in_specs=[hbm, hbm, hbm, pl.BlockSpec(memor...  5.23 us
    unnamed x28, local copies, waits for them, and re-layouts  3.51 us
  transfers between devices with their start and end apart: 33, of which 19 were waited for; matrix products, arithmetic and copies ran while one was open for 0% of the time, Pallas kernels for 36%

profile of v1, /device:TPU:33, one launch (start us, length us, event | category | flops | bytes accessed | tf_op | source)
XLA Modules:
  0.0 165.1 jit_solution(14213359068738734537)
XLA Ops:
  1.4 3.0 %query.1.after_ref.refs_0_ = bf16[1032,128]{1,0:T(8,128)(2,1)S(1)} custom-call(bf16[512,2048]{1,0:T(8,128)(2,1)} %x_hbm.3, bf16[2048,256]{1,0:T(8,128)(2,1)} %w_hbm.1, s32[4,8]{1,0:T(4,128)S(1)} %bitcast.10, s32[4,8]{1,0:T(4,128)S(1)} %bitcast.11), custom_call_target="tpu_custom_call" | custom-call | flops 536870912 | bytes 3145728 | tf_op jit(solution)/shard_map/query/pallas_call | solution.py:91
  4.4 3.9 %collective-permute-start = (bf16[1032,128]{1,0:T(8,128)(2,1)S(1)}, bf16[1032,128]{1,0:T(8,128)(2,1)S(1)}, u32[]{:S(2)}, u32[]{:S(2)}) collective-permute-start(bf16[1032,128]{1,0:T(8,128)(2,1)S(1)} %query.1.after_ref.refs_0_), channel_id=1, source_target_pairs={{4,8},{0,124},{12,16},{8,4},{20,24},{16,12},{28,32},{24,20},{36,40... | collective-permute-start | bytes 792584 | tf_op jit(solution)/shard_map/ppermute | solution.py:559
  8.3 19.2 %collective-permute-start.9 = (bf16[1032,128]{1,0:T(8,128)(2,1)S(1)}, bf16[1032,128]{1,0:T(8,128)(2,1)S(1)}, u32[]{:S(2)}, u32[]{:S(2)}) collective-permute-start(bf16[1032,128]{1,0:T(8,128)(2,1)S(1)} %query.1.after_ref.refs_0_), channel_id=1, source_target_pairs={{0,8},{4,124},{8,16},{12,4},{16,24},{20,12},{24,32},{28,20},{32,40... | collective-permute-start | bytes 792584 | tf_op jit(solution)/shard_map/ppermute | solution.py:559
  27.6 9.3 %collective-permute-start.2 = (bf16[1032,128]{1,0:T(8,128)(2,1)S(1)}, bf16[1032,128]{1,0:T(8,128)(2,1)S(1)}, u32[]{:S(2)}, u32[]{:S(2)}) collective-permute-start(bf16[1032,128]{1,0:T(8,128)(2,1)S(1)} %collective-permute-done.after_ref.refs_1_), channel_id=1, source_target_pairs={{0,8},{4,124},{8,16},{12,4},{16,24},{20,12},{24,32},{28,20},{32,40... | collective-permute-start | bytes 792584 | tf_op jit(solution)/shard_map/ppermute | solution.py:559
  36.9 3.3 %collective-permute-done.2.refs_1_ = bf16[1032,128]{1,0:T(8,128)(2,1)S(1)} collective-permute-done((bf16[1032,128]{1,0:T(8,128)(2,1)S(1)}, bf16[1032,128]{1,0:T(8,128)(2,1)S(1)}, u32[]{:S(2)}, u32[]{:S(2)}) %collective-permute-start.2) | collective-permute-done | bytes 264224 | tf_op jit(solution)/shard_map/ppermute | solution.py:559
  40.2 3.1 %collective-permute-start.3 = (bf16[1032,128]{1,0:T(8,128)(2,1)S(1)}, bf16[1032,128]{1,0:T(8,128)(2,1)S(1)}, u32[]{:S(2)}, u32[]{:S(2)}) collective-permute-start(bf16[1032,128]{1,0:T(8,128)(2,1)S(1)} %collective-permute-done.2.refs_1_), channel_id=1, source_target_pairs={{0,8},{4,124},{8,16},{12,4},{16,24},{20,12},{24,32},{28,20},{32,40... | collective-permute-start | bytes 792584 | tf_op jit(solution)/shard_map/ppermute | solution.py:559
  43.3 2.8 %collective-permute-start.11 = (bf16[1032,128]{1,0:T(8,128)(2,1)S(1)}, bf16[1032,128]{1,0:T(8,128)(2,1)S(1)}, u32[]{:S(2)}, u32[]{:S(2)}) collective-permute-start(bf16[1032,128]{1,0:T(8,128)(2,1)S(1)} %collective-permute-done.10.refs_0_), channel_id=1, source_target_pairs={{0,8},{4,124},{8,16},{12,4},{16,24},{20,12},{24,32},{28,20},{32,40... | collective-permute-start | bytes 792584 | tf_op jit(solution)/shard_map/ppermute | solution.py:559
  46.2 5.2 %passages.1.refs_1_.refs_2_.kv_ref = bf16[16,256,128]{2,1,0:T(8,128)(2,1)S(1)} custom-call(bf16[1024,2048]{1,0:T(8,128)(2,1)} %bitcast.31, bf16[2048,256]{1,0:T(8,128)(2,1)} %wk_hbm.3, bf16[2048,256]{1,0:T(8,128)(2,1)} %wv_hbm.3, bf16[1032,128]{1,0:T(8,128)(2,1)S(1)} %query.1.after_ref.refs_0_), custom_call_target="tpu_custom_call" | custom-call | flops 2147483648 | bytes 4194304 | tf_op jit(solution)/shard_map/passages/pallas_call | solution.py:210
  51.6 1.4 collective-permute-start.12
  54.3 2.9 %collective-permute-done.12.refs_0_ = bf16[1032,128]{1,0:T(8,128)(2,1)S(1)} collective-permute-done((bf16[1032,128]{1,0:T(8,128)(2,1)S(1)}, bf16[1032,128]{1,0:T(8,128)(2,1)S(1)}, u32[]{:S(2)}, u32[]{:S(2)}) %collective-permute-start.12) | collective-permute-done | bytes 264224 | tf_op jit(solution)/shard_map/ppermute | solution.py:559
  57.2 2.2 %collective-permute-start.13 = (bf16[1032,128]{1,0:T(8,128)(2,1)S(1)}, bf16[1032,128]{1,0:T(8,128)(2,1)}, u32[]{:S(2)}, u32[]{:S(2)}) collective-permute-start(bf16[1032,128]{1,0:T(8,128)(2,1)S(1)} %collective-permute-done.12.refs_0_), channel_id=1, source_target_pairs={{0,8},{4,124},{8,16},{12,4},{16,24},{20,12},{24,32},{28,20},{32,40... | collective-permute-start | bytes 792584 | tf_op jit(solution)/shard_map/ppermute | solution.py:559
  60.2 2.2 %collective-permute-start.5 = (bf16[1032,128]{1,0:T(8,128)(2,1)}, bf16[1032,128]{1,0:T(8,128)(2,1)}, u32[]{:S(2)}, u32[]{:S(2)}) collective-permute-start(bf16[1032,128]{1,0:T(8,128)(2,1)} %collective-permute-done.4.refs_1_), channel_id=1, source_target_pairs={{0,8},{4,124},{8,16},{12,4},{16,24},{20,12},{24,32},{28,20},{32,40... | collective-permute-start | bytes 792584 | tf_op jit(solution)/shard_map/ppermute | solution.py:559
  62.7 3.2 %collective-permute-start.14 = (bf16[1032,128]{1,0:T(8,128)(2,1)}, bf16[1032,128]{1,0:T(8,128)(2,1)}, u32[]{:S(2)}, u32[]{:S(2)}) collective-permute-start(bf16[1032,128]{1,0:T(8,128)(2,1)} %collective-permute-done.13.refs_0_), channel_id=1, source_target_pairs={{0,8},{4,124},{8,16},{12,4},{16,24},{20,12},{24,32},{28,20},{32,40... | collective-permute-start | bytes 792584 | tf_op jit(solution)/shard_map/ppermute | solution.py:559
  66.0 3.1 %collective-permute-start.6 = (bf16[1032,128]{1,0:T(8,128)(2,1)}, bf16[1032,128]{1,0:T(8,128)(2,1)S(1)}, u32[]{:S(2)}, u32[]{:S(2)}) collective-permute-start(bf16[1032,128]{1,0:T(8,128)(2,1)} %collective-permute-done.5.refs_1_), channel_id=1, source_target_pairs={{0,8},{4,124},{8,16},{12,4},{16,24},{20,12},{24,32},{28,20},{32,40... | collective-permute-start | bytes 792584 | tf_op jit(solution)/shard_map/ppermute | solution.py:559
  69.2 5.4 %mixer_inputs.1 = (bf16[3,8,128,128]{3,2,1,0:T(8,128)(2,1)S(1)}, f32[512,8]{1,0:T(8,128)S(1)}) custom-call(bf16[512,2048]{1,0:T(8,128)(2,1)} %x_hbm.3, bf16[2048,256]{1,0:T(8,128)(2,1)} %wq_hbm.1, bf16[2048,256]{1,0:T(8,128)(2,1)} %wk_hbm.2, bf16[2048,256]{1,0:T(8,128)(2,1)} %wv_hbm.2, bf16[2,2048]{1,0:T(2,128)(2,1)S(1)} %bitcast.12, ...), custom_call_target="tpu_custom_call" | custom-call | flops 1610612736 | bytes 5242880 | tf_op jit(solution)/shard_map/mixer_inputs/pallas_call | solution.py:153
  74.7 1.8 %parts.8 = (f32[4,128,128]{2,1,0:T(8,128)S(1)}, f32[4,8,128]{2,1,0:T(8,128)S(1)}, s32[4]{0:T(128)S(1)}) custom-call(s32[2]{0:T(128)S(1)} %pad_add_fusion.own_ref, bf16[1032,128]{1,0:T(8,128)(2,1)S(1)} %query.1.after_ref.refs_0_, bf16[16,256,128]{2,1,0:T(8,128)(2,1)S(1)} %passages.1.refs_1_.refs_2_.kv_ref, ...), custom_call_target="tpu_custom_call" | custom-call | flops 419430400 | bytes 512000 | tf_op jit(solution)/shard_map/parts/pallas_call | solution.py:388
  76.6 2.0 %parts.9 = (f32[8,128,128]{2,1,0:T(8,128)S(1)}, f32[8,8,128]{2,1,0:T(8,128)S(1)}, s32[8]{0:T(128)S(1)}) custom-call(s32[2]{0:T(128)S(1)} %pad_add_fusion.own_ref, bf16[1032,128]{1,0:T(8,128)(2,1)S(1)} %collective-permute-done.9.refs_0_, bf16[1032,128]{1,0:T(8,128)(2,1)S(1)} %collective-permute-done.after_ref.refs_1_, ...), custom_call_target="tpu_custom_call" | custom-call | flops 838860800 | bytes 1024000 | tf_op jit(solution)/shard_map/parts/pallas_call | solution.py:388
  78.7 2.0 %parts.10 = (f32[8,128,128]{2,1,0:T(8,128)S(1)}, f32[8,8,128]{2,1,0:T(8,128)S(1)}, s32[8]{0:T(128)S(1)}) custom-call(s32[2]{0:T(128)S(1)} %pad_add_fusion.own_ref, bf16[1032,128]{1,0:T(8,128)(2,1)S(1)} %collective-permute-done.10.refs_0_, bf16[1032,128]{1,0:T(8,128)(2,1)S(1)} %collective-permute-done.2.refs_1_, ...), custom_call_target="tpu_custom_call" | custom-call | flops 838860800 | bytes 1024000 | tf_op jit(solution)/shard_map/parts/pallas_call | solution.py:388
  80.8 2.0 %parts.11 = (f32[8,128,128]{2,1,0:T(8,128)S(1)}, f32[8,8,128]{2,1,0:T(8,128)S(1)}, s32[8]{0:T(128)S(1)}) custom-call(s32[2]{0:T(128)S(1)} %pad_add_fusion.own_ref, bf16[1032,128]{1,0:T(8,128)(2,1)S(1)} %copy-done.5, bf16[1032,128]{1,0:T(8,128)(2,1)S(1)} %copy-done.3, bf16[16,256,128]{2,1,0:T(8,128)(2,1)S(1)} %passages.1.refs_1_.refs_2_.kv_ref, ...), custom_call_target="tpu_custom_call" | custom-call | flops 838860800 | bytes 1024000 | tf_op jit(solution)/shard_map/parts/pallas_call | solution.py:388
  82.8 2.0 %collective-permute-start.16 = (bf16[1032,128]{1,0:T(8,128)(2,1)S(1)}, bf16[1032,128]{1,0:T(8,128)(2,1)S(1)}, u32[]{:S(2)}, u32[]{:S(2)}) collective-permute-start(bf16[1032,128]{1,0:T(8,128)(2,1)S(1)} %collective-permute-done.15.refs_0_), channel_id=1, source_target_pairs={{4,124},{12,4},{20,12},{28,20},{36,28},{44,36},{52,44},{60,52},{68... | collective-permute-start | bytes 792584 | tf_op jit(solution)/shard_map/ppermute | solution.py:559
  84.8 2.5 %parts.12 = (f32[8,128,128]{2,1,0:T(8,128)S(1)}, f32[8,8,128]{2,1,0:T(8,128)S(1)}, s32[8]{0:T(128)S(1)}) custom-call(s32[2]{0:T(128)S(1)} %pad_add_fusion.own_ref, bf16[1032,128]{1,0:T(8,128)(2,1)S(1)} %copy-done.7, bf16[1032,128]{1,0:T(8,128)(2,1)} %collective-permute-done.4.refs_1_, bf16[16,256,128]{2,1,0:T(8,128)(2,1)S(1)} %passages.1.refs_1_.refs_2_.kv_ref, ...), custom_call_target="tpu_custom_call" | custom-call | flops 838860800 | bytes 1024000 | tf_op jit(solution)/shard_map/parts/pallas_call | solution.py:388
  87.3 3.8 %collective-permute-start.8 = (bf16[1032,128]{1,0:T(8,128)(2,1)S(1)}, bf16[1032,128]{1,0:T(8,128)(2,1)S(1)}, u32[]{:S(2)}, u32[]{:S(2)}) collective-permute-start(bf16[1032,128]{1,0:T(8,128)(2,1)S(1)} %collective-permute-done.7.refs_1_), channel_id=1, source_target_pairs={{4,124},{12,4},{20,12},{28,20},{36,28},{44,36},{52,44},{60,52},{68... | collective-permute-start | bytes 792584 | tf_op jit(solution)/shard_map/ppermute | solution.py:559
  91.1 2.5 %parts.13 = (f32[8,128,128]{2,1,0:T(8,128)S(1)}, f32[8,8,128]{2,1,0:T(8,128)S(1)}, s32[8]{0:T(128)S(1)}) custom-call(s32[2]{0:T(128)S(1)} %pad_add_fusion.own_ref, bf16[1032,128]{1,0:T(8,128)(2,1)} %collective-permute-done.13.refs_0_, bf16[1032,128]{1,0:T(8,128)(2,1)} %collective-permute-done.5.refs_1_, ...), custom_call_target="tpu_custom_call" | custom-call | flops 838860800 | bytes 1024000 | tf_op jit(solution)/shard_map/parts/pallas_call | solution.py:388
  93.6 2.5 %parts.14 = (f32[8,128,128]{2,1,0:T(8,128)S(1)}, f32[8,8,128]{2,1,0:T(8,128)S(1)}, s32[8]{0:T(128)S(1)}) custom-call(s32[2]{0:T(128)S(1)} %pad_add_fusion.own_ref, bf16[1032,128]{1,0:T(8,128)(2,1)} %collective-permute-done.14.refs_0_, bf16[1032,128]{1,0:T(8,128)(2,1)S(1)} %collective-permute-done.6.refs_1_, ...), custom_call_target="tpu_custom_call" | custom-call | flops 838860800 | bytes 1024000 | tf_op jit(solution)/shard_map/parts/pallas_call | solution.py:388
  96.1 2.0 %parts.15 = (f32[8,128,128]{2,1,0:T(8,128)S(1)}, f32[8,8,128]{2,1,0:T(8,128)S(1)}, s32[8]{0:T(128)S(1)}) custom-call(s32[2]{0:T(128)S(1)} %pad_add_fusion.own_ref, bf16[1032,128]{1,0:T(8,128)(2,1)S(1)} %collective-permute-done.15.refs_0_, bf16[1032,128]{1,0:T(8,128)(2,1)S(1)} %collective-permute-done.7.refs_1_, ...), custom_call_target="tpu_custom_call" | custom-call | flops 838860800 | bytes 1024000 | tf_op jit(solution)/shard_map/parts/pallas_call | solution.py:388
  98.2 1.6 far.2.after_ref
  99.8 2.0 %collective-permute-start.17 = (bf16[8,136,128]{2,1,0:T(8,128)(2,1)S(1)}, bf16[8,136,128]{2,1,0:T(8,128)(2,1)S(1)}, u32[]{:S(2)}, u32[]{:S(2)}) collective-permute-start(bf16[8,136,128]{2,1,0:T(8,128)(2,1)S(1)} %far.2.after_ref), channel_id=1, source_target_pairs={{124,4},{4,12},{12,20},{20,28},{28,36},{36,44},{44,52},{52,60},{60... | collective-permute-start | bytes 835592 | tf_op jit(solution)/shard_map/ppermute | solution.py:559
  101.8 1.6 far.3.after_ref
  103.4 3.0 %collective-permute-start.18 = (bf16[8,136,128]{2,1,0:T(8,128)(2,1)S(1)}, bf16[8,136,128]{2,1,0:T(8,128)(2,1)S(1)}, u32[]{:S(2)}, u32[]{:S(2)}) collective-permute-start(bf16[8,136,128]{2,1,0:T(8,128)(2,1)S(1)} %far.3.after_ref), channel_id=1, source_target_pairs={{124,4},{4,12},{12,20},{20,28},{28,36},{36,44},{44,52},{52,60},{60... | collective-permute-start | bytes 835592 | tf_op jit(solution)/shard_map/ppermute | solution.py:559
  106.4 2.3 %mixer.8 = (f32[1,128,128]{2,1,0:T(8,128)S(1)}, f32[2,128,128]{2,1,0:T(8,128)S(1)}) custom-call(bf16[3,8,128,128]{3,2,1,0:T(8,128)(2,1)S(1)} %get-tuple-element.51.qkv_ref, f32[512,8]{1,0:T(8,128)S(1)} %get-tuple-element.47.refs_3_.lg_ref, f32[2,512]{1,0:T(2,128)S(1)} %bitcast.15, f32[2]{0:T(128)S(1)} %copy-done.12, f32[1,128]{1,0:T(1,128)S(1)} %bitcast.23, ...), custom_call_target="tpu_custom_call" | custom-call | flops 524288000 | bytes 307200 | tf_op jit(solution)/shard_map/mixer/pallas_call | solution.py:295
  109.4 1.5 collective-permute-start.19
  112.6 1.7 %collective-permute-start.20 = (bf16[8,136,128]{2,1,0:T(8,128)(2,1)S(1)}, bf16[8,136,128]{2,1,0:T(8,128)(2,1)S(1)}, u32[]{:S(2)}, u32[]{:S(2)}) collective-permute-start(bf16[8,136,128]{2,1,0:T(8,128)(2,1)S(1)} %merge.16.after_ref), channel_id=1, source_target_pairs={{8,0},{124,4},{16,8},{4,12},{24,16},{12,20},{32,24},{20,28},{40,32... | collective-permute-start | bytes 835592 | tf_op jit(solution)/shard_map/ppermute | solution.py:559
  114.3 2.3 %mixer.9 = (f32[1,128,128]{2,1,0:T(8,128)S(1)}, f32[2,128,128]{2,1,0:T(8,128)S(1)}) custom-call(bf16[3,8,128,128]{3,2,1,0:T(8,128)(2,1)S(1)} %get-tuple-element.51.qkv_ref, f32[512,8]{1,0:T(8,128)S(1)} %get-tuple-element.47.refs_3_.lg_ref, f32[2,512]{1,0:T(2,128)S(1)} %bitcast.16, f32[2]{0:T(128)S(1)} %copy-done.12, f32[1,128]{1,0:T(1,128)S(1)} %bitcast.24, ...), custom_call_target="tpu_custom_call" | custom-call | flops 524288000 | bytes 307200 | tf_op jit(solution)/shard_map/mixer/pallas_call | solution.py:295
  117.7 1.5 collective-permute-done.20.refs_0_
  120.7 2.3 %mixer.10 = (f32[1,128,128]{2,1,0:T(8,128)S(1)}, f32[2,128,128]{2,1,0:T(8,128)S(1)}) custom-call(bf16[3,8,128,128]{3,2,1,0:T(8,128)(2,1)S(1)} %get-tuple-element.51.qkv_ref, f32[512,8]{1,0:T(8,128)S(1)} %get-tuple-element.47.refs_3_.lg_ref, f32[2,512]{1,0:T(2,128)S(1)} %bitcast.17, f32[2]{0:T(128)S(1)} %copy-done.12, f32[1,128]{1,0:T(1,128)S(1)} %bitcast.25, ...), custom_call_target="tpu_custom_call" | custom-call | flops 524288000 | bytes 307200 | tf_op jit(solution)/shard_map/mixer/pallas_call | solution.py:295
  124.6 1.6 collective-permute-start.23
  127.8 2.3 %mixer.11 = (f32[1,128,128]{2,1,0:T(8,128)S(1)}, f32[2,128,128]{2,1,0:T(8,128)S(1)}) custom-call(bf16[3,8,128,128]{3,2,1,0:T(8,128)(2,1)S(1)} %get-tuple-element.51.qkv_ref, f32[512,8]{1,0:T(8,128)S(1)} %get-tuple-element.47.refs_3_.lg_ref, f32[2,512]{1,0:T(2,128)S(1)} %bitcast.18, f32[2]{0:T(128)S(1)} %copy-done.12, f32[1,128]{1,0:T(1,128)S(1)} %bitcast.26, ...), custom_call_target="tpu_custom_call" | custom-call | flops 524288000 | bytes 307200 | tf_op jit(solution)/shard_map/mixer/pallas_call | solution.py:295
  130.1 1.5 collective-permute-done.23.refs_0_
  132.6 1.9 %collective-permute-done.24.refs_0_ = bf16[8,136,128]{2,1,0:T(8,128)(2,1)S(1)} collective-permute-done((bf16[8,136,128]{2,1,0:T(8,128)(2,1)S(1)}, bf16[8,136,128]{2,1,0:T(8,128)(2,1)S(1)}, u32[]{:S(2)}, u32[]{:S(2)}) %collective-permute-start.24) | collective-permute-done | bytes 278560 | tf_op jit(solution)/shard_map/ppermute | solution.py:559
  135.6 2.3 %mixer.12 = (f32[1,128,128]{2,1,0:T(8,128)S(1)}, f32[2,128,128]{2,1,0:T(8,128)S(1)}) custom-call(bf16[3,8,128,128]{3,2,1,0:T(8,128)(2,1)S(1)} %get-tuple-element.51.qkv_ref, f32[512,8]{1,0:T(8,128)S(1)} %get-tuple-element.47.refs_3_.lg_ref, f32[2,512]{1,0:T(2,128)S(1)} %bitcast.19, f32[2]{0:T(128)S(1)} %copy-done.12, f32[1,128]{1,0:T(1,128)S(1)} %bitcast.27, ...), custom_call_target="tpu_custom_call" | custom-call | flops 524288000 | bytes 307200 | tf_op jit(solution)/shard_map/mixer/pallas_call | solution.py:295
  139.7 2.2 %collective-permute-done.26.refs_0_ = bf16[8,136,128]{2,1,0:T(8,128)(2,1)S(1)} collective-permute-done((bf16[8,136,128]{2,1,0:T(8,128)(2,1)S(1)}, bf16[8,136,128]{2,1,0:T(8,128)(2,1)S(1)}, u32[]{:S(2)}, u32[]{:S(2)}) %collective-permute-start.26) | collective-permute-done | bytes 278560 | tf_op jit(solution)/shard_map/ppermute | solution.py:559
  142.7 2.3 %mixer.13 = (f32[1,128,128]{2,1,0:T(8,128)S(1)}, f32[2,128,128]{2,1,0:T(8,128)S(1)}) custom-call(bf16[3,8,128,128]{3,2,1,0:T(8,128)(2,1)S(1)} %get-tuple-element.51.qkv_ref, f32[512,8]{1,0:T(8,128)S(1)} %get-tuple-element.47.refs_3_.lg_ref, f32[2,512]{1,0:T(2,128)S(1)} %bitcast.20, f32[2]{0:T(128)S(1)} %copy-done.12, f32[1,128]{1,0:T(1,128)S(1)} %bitcast.28, ...), custom_call_target="tpu_custom_call" | custom-call | flops 524288000 | bytes 307200 | tf_op jit(solution)/shard_map/mixer/pallas_call | solution.py:295
  147.1 2.2 %collective-permute-done.28.refs_0_ = bf16[8,136,128]{2,1,0:T(8,128)(2,1)S(1)} collective-permute-done((bf16[8,136,128]{2,1,0:T(8,128)(2,1)S(1)}, bf16[8,136,128]{2,1,0:T(8,128)(2,1)S(1)}, u32[]{:S(2)}, u32[]{:S(2)}) %collective-permute-start.28) | collective-permute-done | bytes 278560 | tf_op jit(solution)/shard_map/ppermute | solution.py:559
  150.1 2.3 %mixer.14 = (f32[1,128,128]{2,1,0:T(8,128)S(1)}, f32[2,128,128]{2,1,0:T(8,128)S(1)}) custom-call(bf16[3,8,128,128]{3,2,1,0:T(8,128)(2,1)S(1)} %get-tuple-element.51.qkv_ref, f32[512,8]{1,0:T(8,128)S(1)} %get-tuple-element.47.refs_3_.lg_ref, f32[2,512]{1,0:T(2,128)S(1)} %bitcast.21, f32[2]{0:T(128)S(1)} %copy-done.12, f32[1,128]{1,0:T(1,128)S(1)} %bitcast.29, ...), custom_call_target="tpu_custom_call" | custom-call | flops 524288000 | bytes 307200 | tf_op jit(solution)/shard_map/mixer/pallas_call | solution.py:295
  154.5 2.2 %collective-permute-done.30.refs_0_ = bf16[8,136,128]{2,1,0:T(8,128)(2,1)S(1)} collective-permute-done((bf16[8,136,128]{2,1,0:T(8,128)(2,1)S(1)}, bf16[8,136,128]{2,1,0:T(8,128)(2,1)S(1)}, u32[]{:S(2)}, u32[]{:S(2)}) %collective-permute-start.30) | collective-permute-done | bytes 278560 | tf_op jit(solution)/shard_map/ppermute | solution.py:559
  157.5 2.3 %mixer.15 = (f32[1,128,128]{2,1,0:T(8,128)S(1)}, f32[2,128,128]{2,1,0:T(8,128)S(1)}) custom-call(bf16[3,8,128,128]{3,2,1,0:T(8,128)(2,1)S(1)} %get-tuple-element.51.qkv_ref, f32[512,8]{1,0:T(8,128)S(1)} %get-tuple-element.47.refs_3_.lg_ref, f32[2,512]{1,0:T(2,128)S(1)} %bitcast.22, f32[2]{0:T(128)S(1)} %copy-done.12, f32[1,128]{1,0:T(1,128)S(1)} %bitcast.30, ...), custom_call_target="tpu_custom_call" | custom-call | flops 524288000 | bytes 307200 | tf_op jit(solution)/shard_map/mixer/pallas_call | solution.py:295
  161.7 2.0 %collective-permute-done.32.refs_1_ = bf16[8,136,128]{2,1,0:T(8,128)(2,1)S(1)} collective-permute-done((bf16[8,136,128]{2,1,0:T(8,128)(2,1)S(1)}, bf16[8,136,128]{2,1,0:T(8,128)(2,1)S(1)}, u32[]{:S(2)}, u32[]{:S(2)}) %collective-permute-start.32) | collective-permute-done | bytes 278560 | tf_op jit(solution)/shard_map/ppermute | solution.py:559
  163.7 1.4 finish.1
  (85 shorter events, 24.7 us)
Async XLA Ops:
  0.0 0.7 copy-start
  0.7 0.7 copy-start.1
  4.4 64.8 %copy-start.8 = (bf16[2048,2]{0,1:T(2,128)(2,1)S(1)}, bf16[2048,2]{0,1:T(2,128)(2,1)}, u32[]{:S(2)}) copy-start(bf16[2048,2]{0,1:T(2,128)(2,1)} %param.23) | copy-start | bytes 24580
  4.4 64.8 %copy-start.9 = (bf16[2048,2]{0,1:T(2,128)(2,1)S(1)}, bf16[2048,2]{0,1:T(2,128)(2,1)}, u32[]{:S(2)}) copy-start(bf16[2048,2]{0,1:T(2,128)(2,1)} %param.24) | copy-start | bytes 24580
  4.4 64.8 %copy-start.10 = (bf16[2048,2]{0,1:T(2,128)(2,1)S(1)}, bf16[2048,2]{0,1:T(2,128)(2,1)}, u32[]{:S(2)}) copy-start(bf16[2048,2]{0,1:T(2,128)(2,1)} %param.31) | copy-start | bytes 24580
  4.4 23.2 %collective-permute-start = (bf16[1032,128]{1,0:T(8,128)(2,1)S(1)}, bf16[1032,128]{1,0:T(8,128)(2,1)S(1)}, u32[]{:S(2)}, u32[]{:S(2)}) collective-permute-start(bf16[1032,128]{1,0:T(8,128)(2,1)S(1)} %query.1.after_ref.refs_0_), channel_id=1, source_target_pairs={{4,8},{0,124},{12,16},{8,4},{20,24},{16,12},{28,32},{24,20},{36,40... | collective-permute-start | bytes 792584 | tf_op jit(solution)/shard_map/ppermute | solution.py:559
  8.3 28.5 %collective-permute-start.9 = (bf16[1032,128]{1,0:T(8,128)(2,1)S(1)}, bf16[1032,128]{1,0:T(8,128)(2,1)S(1)}, u32[]{:S(2)}, u32[]{:S(2)}) collective-permute-start(bf16[1032,128]{1,0:T(8,128)(2,1)S(1)} %query.1.after_ref.refs_0_), channel_id=1, source_target_pairs={{0,8},{4,124},{8,16},{12,4},{16,24},{20,12},{24,32},{28,20},{32,40... | collective-permute-start | bytes 792584 | tf_op jit(solution)/shard_map/ppermute | solution.py:559
  27.6 12.6 %collective-permute-start.2 = (bf16[1032,128]{1,0:T(8,128)(2,1)S(1)}, bf16[1032,128]{1,0:T(8,128)(2,1)S(1)}, u32[]{:S(2)}, u32[]{:S(2)}) collective-permute-start(bf16[1032,128]{1,0:T(8,128)(2,1)S(1)} %collective-permute-done.after_ref.refs_1_), channel_id=1, source_target_pairs={{0,8},{4,124},{8,16},{12,4},{16,24},{20,12},{24,32},{28,20},{32,40... | collective-permute-start | bytes 792584 | tf_op jit(solution)/shard_map/ppermute | solution.py:559
  36.9 6.5 %collective-permute-start.10 = (bf16[1032,128]{1,0:T(8,128)(2,1)S(1)}, bf16[1032,128]{1,0:T(8,128)(2,1)S(1)}, u32[]{:S(2)}, u32[]{:S(2)}) collective-permute-start(bf16[1032,128]{1,0:T(8,128)(2,1)S(1)} %collective-permute-done.9.refs_0_), channel_id=1, source_target_pairs={{0,8},{4,124},{8,16},{12,4},{16,24},{20,12},{24,32},{28,20},{32,40... | collective-permute-start | bytes 792584 | tf_op jit(solution)/shard_map/ppermute | solution.py:559
  40.2 13.4 %collective-permute-start.3 = (bf16[1032,128]{1,0:T(8,128)(2,1)S(1)}, bf16[1032,128]{1,0:T(8,128)(2,1)S(1)}, u32[]{:S(2)}, u32[]{:S(2)}) collective-permute-start(bf16[1032,128]{1,0:T(8,128)(2,1)S(1)} %collective-permute-done.2.refs_1_), channel_id=1, source_target_pairs={{0,8},{4,124},{8,16},{12,4},{16,24},{20,12},{24,32},{28,20},{32,40... | collective-permute-start | bytes 792584 | tf_op jit(solution)/shard_map/ppermute | solution.py:559
  43.3 8.2 %collective-permute-start.11 = (bf16[1032,128]{1,0:T(8,128)(2,1)S(1)}, bf16[1032,128]{1,0:T(8,128)(2,1)S(1)}, u32[]{:S(2)}, u32[]{:S(2)}) collective-permute-start(bf16[1032,128]{1,0:T(8,128)(2,1)S(1)} %collective-permute-done.10.refs_0_), channel_id=1, source_target_pairs={{0,8},{4,124},{8,16},{12,4},{16,24},{20,12},{24,32},{28,20},{32,40... | collective-permute-start | bytes 792584 | tf_op jit(solution)/shard_map/ppermute | solution.py:559
  51.4 23.3 %collective-permute-start.1 = (bf16[16,256,128]{2,1,0:T(8,128)(2,1)S(1)}, bf16[16,256,128]{2,1,0:T(8,128)(2,1)S(1)}, u32[]{:S(2)}, u32[]{:S(2)}) collective-permute-start(bf16[16,256,128]{2,1,0:T(8,128)(2,1)S(1)} %passages.1.refs_1_.refs_2_.kv_ref), channel_id=1, source_target_pairs={{0,4},{4,0},{8,12},{12,8},{16,20},{20,16},{24,28},{28,24},{32,36},... | collective-permute-start | bytes 3145736 | tf_op jit(solution)/shard_map/ppermute | solution.py:559
  51.6 5.7 %collective-permute-start.12 = (bf16[1032,128]{1,0:T(8,128)(2,1)S(1)}, bf16[1032,128]{1,0:T(8,128)(2,1)S(1)}, u32[]{:S(2)}, u32[]{:S(2)}) collective-permute-start(bf16[1032,128]{1,0:T(8,128)(2,1)S(1)} %collective-permute-done.11.refs_0_), channel_id=1, source_target_pairs={{0,8},{4,124},{8,16},{12,4},{16,24},{20,12},{24,32},{28,20},{32,40... | collective-permute-start | bytes 792584 | tf_op jit(solution)/shard_map/ppermute | solution.py:559
  52.9 0.7 copy-start.4
  53.6 6.5 %collective-permute-start.4 = (bf16[1032,128]{1,0:T(8,128)(2,1)S(1)}, bf16[1032,128]{1,0:T(8,128)(2,1)}, u32[]{:S(2)}, u32[]{:S(2)}) collective-permute-start(bf16[1032,128]{1,0:T(8,128)(2,1)S(1)} %collective-permute-done.3.refs_1_), channel_id=1, source_target_pairs={{0,8},{4,124},{8,16},{12,4},{16,24},{20,12},{24,32},{28,20},{32,40... | collective-permute-start | bytes 792584 | tf_op jit(solution)/shard_map/ppermute | solution.py:559
  53.6 0.7 copy-start.2
  57.2 5.5 %collective-permute-start.13 = (bf16[1032,128]{1,0:T(8,128)(2,1)S(1)}, bf16[1032,128]{1,0:T(8,128)(2,1)}, u32[]{:S(2)}, u32[]{:S(2)}) collective-permute-start(bf16[1032,128]{1,0:T(8,128)(2,1)S(1)} %collective-permute-done.12.refs_0_), channel_id=1, source_target_pairs={{0,8},{4,124},{8,16},{12,4},{16,24},{20,12},{24,32},{28,20},{32,40... | collective-permute-start | bytes 792584 | tf_op jit(solution)/shard_map/ppermute | solution.py:559
  59.4 0.7 copy-start.6
  60.2 5.9 %collective-permute-start.5 = (bf16[1032,128]{1,0:T(8,128)(2,1)}, bf16[1032,128]{1,0:T(8,128)(2,1)}, u32[]{:S(2)}, u32[]{:S(2)}) collective-permute-start(bf16[1032,128]{1,0:T(8,128)(2,1)} %collective-permute-done.4.refs_1_), channel_id=1, source_target_pairs={{0,8},{4,124},{8,16},{12,4},{16,24},{20,12},{24,32},{28,20},{32,40... | collective-permute-start | bytes 792584 | tf_op jit(solution)/shard_map/ppermute | solution.py:559
  62.7 11.8 %collective-permute-start.14 = (bf16[1032,128]{1,0:T(8,128)(2,1)}, bf16[1032,128]{1,0:T(8,128)(2,1)}, u32[]{:S(2)}, u32[]{:S(2)}) collective-permute-start(bf16[1032,128]{1,0:T(8,128)(2,1)} %collective-permute-done.13.refs_0_), channel_id=1, source_target_pairs={{0,8},{4,124},{8,16},{12,4},{16,24},{20,12},{24,32},{28,20},{32,40... | collective-permute-start | bytes 792584 | tf_op jit(solution)/shard_map/ppermute | solution.py:559
  66.0 10.5 %collective-permute-start.6 = (bf16[1032,128]{1,0:T(8,128)(2,1)}, bf16[1032,128]{1,0:T(8,128)(2,1)S(1)}, u32[]{:S(2)}, u32[]{:S(2)}) collective-permute-start(bf16[1032,128]{1,0:T(8,128)(2,1)} %collective-permute-done.5.refs_1_), channel_id=1, source_target_pairs={{0,8},{4,124},{8,16},{12,4},{16,24},{20,12},{24,32},{28,20},{32,40... | collective-permute-start | bytes 792584 | tf_op jit(solution)/shard_map/ppermute | solution.py:559
  74.6 8.3 %collective-permute-start.15 = (bf16[1032,128]{1,0:T(8,128)(2,1)}, bf16[1032,128]{1,0:T(8,128)(2,1)S(1)}, u32[]{:S(2)}, u32[]{:S(2)}) collective-permute-start(bf16[1032,128]{1,0:T(8,128)(2,1)} %collective-permute-done.14.refs_0_), channel_id=1, source_target_pairs={{0,8},{4,124},{8,16},{12,4},{16,24},{20,12},{24,32},{28,20},{32,40... | collective-permute-start | bytes 792584 | tf_op jit(solution)/shard_map/ppermute | solution.py:559
  74.7 6.0 %copy-start.3 = (bf16[1032,128]{1,0:T(8,128)(2,1)S(1)}, bf16[1032,128]{1,0:T(8,128)(2,1)}, u32[]{:S(2)}) copy-start(bf16[1032,128]{1,0:T(8,128)(2,1)} %copy-done.2) | copy-start | bytes 792580
  74.7 6.0 %copy-start.5 = (bf16[1032,128]{1,0:T(8,128)(2,1)S(1)}, bf16[1032,128]{1,0:T(8,128)(2,1)}, u32[]{:S(2)}) copy-start(bf16[1032,128]{1,0:T(8,128)(2,1)} %copy-done.4) | copy-start | bytes 792580
  76.5 10.8 %collective-permute-start.7 = (bf16[1032,128]{1,0:T(8,128)(2,1)S(1)}, bf16[1032,128]{1,0:T(8,128)(2,1)S(1)}, u32[]{:S(2)}, u32[]{:S(2)}) collective-permute-start(bf16[1032,128]{1,0:T(8,128)(2,1)S(1)} %collective-permute-done.6.refs_1_), channel_id=1, source_target_pairs={{0,8},{4,124},{8,16},{12,4},{16,24},{20,12},{24,32},{28,20},{32,40... | collective-permute-start | bytes 792584 | tf_op jit(solution)/shard_map/ppermute | solution.py:559
  76.6 8.2 %copy-start.7 = (bf16[1032,128]{1,0:T(8,128)(2,1)S(1)}, bf16[1032,128]{1,0:T(8,128)(2,1)}, u32[]{:S(2)}) copy-start(bf16[1032,128]{1,0:T(8,128)(2,1)} %copy-done.6) | copy-start | bytes 792580
  82.8 15.3 %collective-permute-start.16 = (bf16[1032,128]{1,0:T(8,128)(2,1)S(1)}, bf16[1032,128]{1,0:T(8,128)(2,1)S(1)}, u32[]{:S(2)}, u32[]{:S(2)}) collective-permute-start(bf16[1032,128]{1,0:T(8,128)(2,1)S(1)} %collective-permute-done.15.refs_0_), channel_id=1, source_target_pairs={{4,124},{12,4},{20,12},{28,20},{36,28},{44,36},{52,44},{60,52},{68... | collective-permute-start | bytes 792584 | tf_op jit(solution)/shard_map/ppermute | solution.py:559
  87.3 14.5 %collective-permute-start.8 = (bf16[1032,128]{1,0:T(8,128)(2,1)S(1)}, bf16[1032,128]{1,0:T(8,128)(2,1)S(1)}, u32[]{:S(2)}, u32[]{:S(2)}) collective-permute-start(bf16[1032,128]{1,0:T(8,128)(2,1)S(1)} %collective-permute-done.7.refs_1_), channel_id=1, source_target_pairs={{4,124},{12,4},{20,12},{28,20},{36,28},{44,36},{52,44},{60,52},{68... | collective-permute-start | bytes 792584 | tf_op jit(solution)/shard_map/ppermute | solution.py:559
  96.1 10.3 %copy-start.11 = (f32[512,2]{0,1:T(2,128)S(1)}, f32[512,2]{0,1:T(2,128)}, u32[]{:S(2)}) copy-start(f32[512,2]{0,1:T(2,128)} %param.26) | copy-start | bytes 12292
  96.1 10.3 %copy-start.12 = (f32[2]{0:T(128)S(1)}, f32[2]{0:T(128)}, u32[]{:S(2)}) copy-start(f32[2]{0:T(128)} %rate_ref.15) | copy-start | bytes 28
  96.1 10.3 %copy-start.13 = (f32[128]{0:T(128)S(1)}, f32[128]{0:T(128)}, u32[]{:S(2)}) copy-start(f32[128]{0:T(128)} %param.27) | copy-start | bytes 1540
  99.8 8.9 %collective-permute-start.17 = (bf16[8,136,128]{2,1,0:T(8,128)(2,1)S(1)}, bf16[8,136,128]{2,1,0:T(8,128)(2,1)S(1)}, u32[]{:S(2)}, u32[]{:S(2)}) collective-permute-start(bf16[8,136,128]{2,1,0:T(8,128)(2,1)S(1)} %far.2.after_ref), channel_id=1, source_target_pairs={{124,4},{4,12},{12,20},{20,28},{28,36},{36,44},{44,52},{52,60},{60... | collective-permute-start | bytes 835592 | tf_op jit(solution)/shard_map/ppermute | solution.py:559
  103.4 8.5 %collective-permute-start.18 = (bf16[8,136,128]{2,1,0:T(8,128)(2,1)S(1)}, bf16[8,136,128]{2,1,0:T(8,128)(2,1)S(1)}, u32[]{:S(2)}, u32[]{:S(2)}) collective-permute-start(bf16[8,136,128]{2,1,0:T(8,128)(2,1)S(1)} %far.3.after_ref), channel_id=1, source_target_pairs={{124,4},{4,12},{12,20},{20,28},{28,36},{36,44},{44,52},{52,60},{60... | collective-permute-start | bytes 835592 | tf_op jit(solution)/shard_map/ppermute | solution.py:559
  109.4 7.2 %collective-permute-start.19 = (bf16[8,136,128]{2,1,0:T(8,128)(2,1)S(1)}, bf16[8,136,128]{2,1,0:T(8,128)(2,1)S(1)}, u32[]{:S(2)}, u32[]{:S(2)}) collective-permute-start(bf16[8,136,128]{2,1,0:T(8,128)(2,1)S(1)} %merge.15.after_ref), channel_id=1, source_target_pairs={{8,0},{124,4},{16,8},{4,12},{24,16},{12,20},{32,24},{20,28},{40,32... | collective-permute-start | bytes 835592 | tf_op jit(solution)/shard_map/ppermute | solution.py:559
  112.6 6.7 %collective-permute-start.20 = (bf16[8,136,128]{2,1,0:T(8,128)(2,1)S(1)}, bf16[8,136,128]{2,1,0:T(8,128)(2,1)S(1)}, u32[]{:S(2)}, u32[]{:S(2)}) collective-permute-start(bf16[8,136,128]{2,1,0:T(8,128)(2,1)S(1)} %merge.16.after_ref), channel_id=1, source_target_pairs={{8,0},{124,4},{16,8},{4,12},{24,16},{12,20},{32,24},{20,28},{40,32... | collective-permute-start | bytes 835592 | tf_op jit(solution)/shard_map/ppermute | solution.py:559
  117.3 6.7 %collective-permute-start.21 = (bf16[8,136,128]{2,1,0:T(8,128)(2,1)S(1)}, bf16[8,136,128]{2,1,0:T(8,128)(2,1)S(1)}, u32[]{:S(2)}, u32[]{:S(2)}) collective-permute-start(bf16[8,136,128]{2,1,0:T(8,128)(2,1)S(1)} %merge.17.after_ref), channel_id=1, source_target_pairs={{8,0},{124,4},{16,8},{4,12},{24,16},{12,20},{32,24},{20,28},{40,32... | collective-permute-start | bytes 835592 | tf_op jit(solution)/shard_map/ppermute | solution.py:559
  119.9 7.0 %collective-permute-start.22 = (bf16[8,136,128]{2,1,0:T(8,128)(2,1)S(1)}, bf16[8,136,128]{2,1,0:T(8,128)(2,1)S(1)}, u32[]{:S(2)}, u32[]{:S(2)}) collective-permute-start(bf16[8,136,128]{2,1,0:T(8,128)(2,1)S(1)} %merge.18.after_ref), channel_id=1, source_target_pairs={{8,0},{124,4},{16,8},{4,12},{24,16},{12,20},{32,24},{20,28},{40,32... | collective-permute-start | bytes 835592 | tf_op jit(solution)/shard_map/ppermute | solution.py:559
  124.6 6.9 %collective-permute-start.23 = (bf16[8,136,128]{2,1,0:T(8,128)(2,1)S(1)}, bf16[8,136,128]{2,1,0:T(8,128)(2,1)S(1)}, u32[]{:S(2)}, u32[]{:S(2)}) collective-permute-start(bf16[8,136,128]{2,1,0:T(8,128)(2,1)S(1)} %merge.19.after_ref), channel_id=1, source_target_pairs={{8,0},{124,4},{16,8},{4,12},{24,16},{12,20},{32,24},{20,28},{40,32... | collective-permute-start | bytes 835592 | tf_op jit(solution)/shard_map/ppermute | solution.py:559
  127.6 6.9 %collective-permute-start.24 = (bf16[8,136,128]{2,1,0:T(8,128)(2,1)S(1)}, bf16[8,136,128]{2,1,0:T(8,128)(2,1)S(1)}, u32[]{:S(2)}, u32[]{:S(2)}) collective-permute-start(bf16[8,136,128]{2,1,0:T(8,128)(2,1)S(1)} %merge.20.after_ref), channel_id=1, source_target_pairs={{8,0},{124,4},{16,8},{4,12},{24,16},{12,20},{32,24},{20,28},{40,32... | collective-permute-start | bytes 835592 | tf_op jit(solution)/shard_map/ppermute | solution.py:559
  132.2 6.7 %collective-permute-start.25 = (bf16[8,136,128]{2,1,0:T(8,128)(2,1)S(1)}, bf16[8,136,128]{2,1,0:T(8,128)(2,1)S(1)}, u32[]{:S(2)}, u32[]{:S(2)}) collective-permute-start(bf16[8,136,128]{2,1,0:T(8,128)(2,1)S(1)} %merge.21.after_ref), channel_id=1, source_target_pairs={{8,0},{124,4},{16,8},{4,12},{24,16},{12,20},{32,24},{20,28},{40,32... | collective-permute-start | bytes 835592 | tf_op jit(solution)/shard_map/ppermute | solution.py:559
  135.2 6.7 %collective-permute-start.26 = (bf16[8,136,128]{2,1,0:T(8,128)(2,1)S(1)}, bf16[8,136,128]{2,1,0:T(8,128)(2,1)S(1)}, u32[]{:S(2)}, u32[]{:S(2)}) collective-permute-start(bf16[8,136,128]{2,1,0:T(8,128)(2,1)S(1)} %merge.22.after_ref), channel_id=1, source_target_pairs={{8,0},{124,4},{16,8},{4,12},{24,16},{12,20},{32,24},{20,28},{40,32... | collective-permute-start | bytes 835592 | tf_op jit(solution)/shard_map/ppermute | solution.py:559
  139.6 6.7 %collective-permute-start.27 = (bf16[8,136,128]{2,1,0:T(8,128)(2,1)S(1)}, bf16[8,136,128]{2,1,0:T(8,128)(2,1)S(1)}, u32[]{:S(2)}, u32[]{:S(2)}) collective-permute-start(bf16[8,136,128]{2,1,0:T(8,128)(2,1)S(1)} %merge.23.after_ref), channel_id=1, source_target_pairs={{8,0},{124,4},{16,8},{4,12},{24,16},{12,20},{32,24},{20,28},{40,32... | collective-permute-start | bytes 835592 | tf_op jit(solution)/shard_map/ppermute | solution.py:559
  142.6 6.7 %collective-permute-start.28 = (bf16[8,136,128]{2,1,0:T(8,128)(2,1)S(1)}, bf16[8,136,128]{2,1,0:T(8,128)(2,1)S(1)}, u32[]{:S(2)}, u32[]{:S(2)}) collective-permute-start(bf16[8,136,128]{2,1,0:T(8,128)(2,1)S(1)} %merge.24.after_ref), channel_id=1, source_target_pairs={{8,0},{124,4},{16,8},{4,12},{24,16},{12,20},{32,24},{20,28},{40,32... | collective-permute-start | bytes 835592 | tf_op jit(solution)/shard_map/ppermute | solution.py:559
  147.0 6.7 %collective-permute-start.29 = (bf16[8,136,128]{2,1,0:T(8,128)(2,1)S(1)}, bf16[8,136,128]{2,1,0:T(8,128)(2,1)S(1)}, u32[]{:S(2)}, u32[]{:S(2)}) collective-permute-start(bf16[8,136,128]{2,1,0:T(8,128)(2,1)S(1)} %merge.25.after_ref), channel_id=1, source_target_pairs={{8,0},{124,4},{16,8},{4,12},{24,16},{12,20},{32,24},{20,28},{40,32... | collective-permute-start | bytes 835592 | tf_op jit(solution)/shard_map/ppermute | solution.py:559
  150.0 6.7 %collective-permute-start.30 = (bf16[8,136,128]{2,1,0:T(8,128)(2,1)S(1)}, bf16[8,136,128]{2,1,0:T(8,128)(2,1)S(1)}, u32[]{:S(2)}, u32[]{:S(2)}) collective-permute-start(bf16[8,136,128]{2,1,0:T(8,128)(2,1)S(1)} %merge.26.after_ref), channel_id=1, source_target_pairs={{8,0},{124,4},{16,8},{4,12},{24,16},{12,20},{32,24},{20,28},{40,32... | collective-permute-start | bytes 835592 | tf_op jit(solution)/shard_map/ppermute | solution.py:559
  154.3 6.7 %collective-permute-start.31 = (bf16[8,136,128]{2,1,0:T(8,128)(2,1)S(1)}, bf16[8,136,128]{2,1,0:T(8,128)(2,1)S(1)}, u32[]{:S(2)}, u32[]{:S(2)}) collective-permute-start(bf16[8,136,128]{2,1,0:T(8,128)(2,1)S(1)} %merge.27.after_ref), channel_id=1, source_target_pairs={{8,0},{124,4},{16,8},{4,12},{24,16},{12,20},{32,24},{20,28},{40,32... | collective-permute-start | bytes 835592 | tf_op jit(solution)/shard_map/ppermute | solution.py:559
  157.3 6.4 %collective-permute-start.32 = (bf16[8,136,128]{2,1,0:T(8,128)(2,1)S(1)}, bf16[8,136,128]{2,1,0:T(8,128)(2,1)S(1)}, u32[]{:S(2)}, u32[]{:S(2)}) collective-permute-start(bf16[8,136,128]{2,1,0:T(8,128)(2,1)S(1)} %merge.28.after_ref), channel_id=1, source_target_pairs={{8,4},{124,0},{16,12},{4,8},{24,20},{12,16},{32,28},{20,24},{40,36... | collective-permute-start | bytes 835592 | tf_op jit(solution)/shard_map/ppermute | solution.py:559

commit v2 on v1

--- a/solution.py
+++ b/solution.py
@@ -262,6 +262,7 @@
         within = (nt(q.astype(BF16), k16) * damping).astype(BF16)
         inverse = jnp.where(diag, 1.0, 0.0) - power
         p16 = power.astype(BF16)
+
         for _ in range(5):
             p16 = nn(p16, p16).astype(BF16)
             inverse = inverse + nn(inverse.astype(BF16), p16)
@@ -372,7 +373,9 @@
             split = jnp.concatenate(
                 [jnp.where(left, expo, 0.0), jnp.where(left, 0.0, expo)], axis=0
             ).astype(BF16)
-            weighed.append((i, nn(values, split), jnp.where(row == 0, peak, denom)))
+            stats = jnp.where(row == 0, peak, denom)
+            stats = jnp.where(row == 2, codes_ref[i].astype(F32), stats)
+            weighed.append((i, nn(values, split), stats))
         for i, sums, stats in weighed:
             sums_ref[i], stats_ref[i] = sums, stats
         return 0
@@ -388,12 +391,12 @@
     return pl.pallas_call(
         functools.partial(find_parts, count),
         in_specs=[scalars] + [whole] * (count + 2) + [pl.BlockSpec(memory_space=pl.ANY)],
-        out_specs=[whole, whole, scalars],
+        out_specs=[whole, whole],
         out_shape=[
             jax.ShapeDtypeStruct((total, 128, 128), F32),
             jax.ShapeDtypeStruct((total, 8, 128), F32),
-            jax.ShapeDtypeStruct((total,), jnp.int32),
-        ],
+        ],
+        scratch_shapes=[pltpu.SMEM((total,), jnp.int32)],
         compiler_params=params(12),
         cost_estimate=cost(count * 400 * MIB, count * 500 * 1024),
         name="parts",
@@ -416,14 +419,18 @@
         out_ref[b, 128:136, :] = none
 
 
-def merge_into(first, codes_ref, sums_ref, stats_ref, out_ref):
+def merge_into(first, sums_ref, stats_ref, out_ref, codes_ref):
     for r in range(SLOTS):
-        code = codes_ref[first + r]
+        codes_ref[r] = jnp.max(stats_ref[first + r, 2:3, :]).astype(jnp.int32)
+
+    def one(slot, _):
+        r = first + slot
+        code = codes_ref[slot]
 
         @pl.when(code > 0)
         def _():
             b = (code - 1) >> 5
-            peak, denom = stats_ref[first + r, 0:1, :], stats_ref[first + r, 1:2, :]
+            peak, denom = stats_ref[r, 0:1, :], stats_ref[r, 1:2, :]
             stats = out_ref[b, 128:136, :].astype(F32)
             m_old = stats[0:1] + stats[1:2] + stats[2:3]
             l_old = stats[3:4] + stats[4:5] + stats[5:6]
@@ -434,17 +441,20 @@
             zero = jnp.zeros((2, 128), F32)
             fresh = jnp.concatenate(split3(m_new) + split3(l_new) + (zero,), axis=0)
             out_ref[b, 128:136, :] = fresh.astype(BF16)
-            mixed = out_ref[b, 0:128, :].astype(F32) * keep + sums_ref[first + r] * gain
+            mixed = out_ref[b, 0:128, :].astype(F32) * keep + sums_ref[r] * gain
             out_ref[b, 0:128, :] = mixed.astype(BF16)
 
-
-def merge_body(first, start, own_ref, codes_ref, sums_ref, stats_ref, after_ref, *refs):
-    out_ref = refs[-1]
-    if start == "all":
-        begin(out_ref)
-    elif start == "core_0":
+        return 0
+
+    lax.fori_loop(0, SLOTS, one, 0)
+
+
+def merge_body(first, start, sums_ref, stats_ref, after_ref, *refs):
+    out_ref, codes_ref = refs[-2:]
+    if start:
+        own_ref = refs[-3]
         pl.when(own_ref[1] == 0)(lambda: begin(out_ref))
-    merge_into(first, codes_ref, sums_ref, stats_ref, out_ref)
+    merge_into(first, sums_ref, stats_ref, out_ref, codes_ref)
 
 
 def far_body(own_ref, q_ref, kv_ref, mate_ref, after_ref, out_ref, sums_ref, stats_ref, codes_ref):
@@ -452,7 +462,7 @@
     def _():
         find_parts(1, own_ref, q_ref, kv_ref, mate_ref, after_ref, sums_ref, stats_ref, codes_ref)
         begin(out_ref)
-        merge_into(0, codes_ref, sums_ref, stats_ref, out_ref)
+        merge_into(0, sums_ref, stats_ref, out_ref, codes_ref)
 
 
 def far_message(own, q, kv, kv_mate, blocks, after):
@@ -474,22 +484,22 @@
     )(own, q, kv, kv_mate, after)
 
 
-def merge(own, part, blocks, after, msg=None, start="none"):
-    (sums, stats, codes), n = part
+def merge(part, blocks, after, msg, start=None):
+    (sums, stats), n = part
     whole = pl.BlockSpec(memory_space=VMEM)
-    scalars = pl.BlockSpec(memory_space=pltpu.SMEM)
-    more = () if msg is None else (msg,)
-    return pl.pallas_call(
-        functools.partial(merge_body, n * SLOTS, start),
-        in_specs=[scalars, scalars, whole, whole, pl.BlockSpec(memory_space=pl.ANY)]
-        + [whole] * len(more),
+    more = () if start is None else (start,)
+    return pl.pallas_call(
+        functools.partial(merge_body, n * SLOTS, start is not None),
+        in_specs=[whole, whole, pl.BlockSpec(memory_space=pl.ANY), whole]
+        + [pl.BlockSpec(memory_space=pltpu.SMEM)] * len(more),
         out_specs=whole,
         out_shape=jax.ShapeDtypeStruct((blocks, 136, 128), BF16),
-        input_output_aliases={5: 0} if more else {},
+        input_output_aliases={3: 0},
+        scratch_shapes=[pltpu.SMEM((SLOTS,), jnp.int32)],
         compiler_params=params(8),
         cost_estimate=cost(100 * MIB, 900 * 1024),
         name="merge",
-    )(own, codes, sums, stats, after, *more)
+    )(sums, stats, after, msg, *more)
 
 
 def finish_body(count, lg_ref, *refs):
@@ -622,14 +632,14 @@
             if h == reach:
                 last = far_message(where_own, lane[h], kv_own, kv_mate, blocks, last)
             else:
-                start = "core_0" if h == reach - 1 else "none"
-                last = merge(where_own, part[(name, h)], blocks, last, came[name], start)
+                start = where_own if h == reach - 1 else None
+                last = merge(part[(name, h)], blocks, last, came[name], start)
             came[name] = send(last, reverse(pairs(name, h)))
-        if len(normed) < blocks:
+        if h < reach:
             last = mixer_step(last)
     while len(normed) < blocks:
         last = mixer_step(last)
-    came["own"] = merge(where_own, part[("own", 0)], blocks, last, came["own"])
+    came["own"] = merge(part[("own", 0)], blocks, last, came["own"])
     return finish((came["own"], came["other"]), logits, normed)
 
 

time: 165 us -> 160 us (0.970)
  Pallas kernels: 63.9 us -> 55.9 us
  waiting for transfers between devices: 27.8 us -> 33.7 us
  starting transfers between devices: 69.2 us -> 66.1 us
    ppermute x33, waiting for transfers between devices: 27.8 us -> 33.7 us  [send(): return lax.ppermute(x, 'st', pairs)]
    pallas_call x15, Pallas kernels: 9.61 us -> 4.75 us  [merge(): pl.pallas_call(functools.partial(merge_body, n * SLOTS, start is not None...]
    pallas_call x8, Pallas kernels: 17.4 us -> 14.2 us  [parts(): pl.pallas_call(functools.partial(find_parts, count), in_specs=[scalars] +...]
    ppermute x33, starting transfers between devices: 69.2 us -> 66.1 us  [send(): return lax.ppermute(x, 'st', pairs)]
  transfers between devices with their start and end apart: 33 -> 33, of which waited for: 19 -> 19; matrix products, arithmetic and copies ran while one was open for 0% -> 0% of each run, Pallas kernels for 36% -> 32%
where the time goes in v2:
time: 160 us
  starting transfers between devices  66.1 us (41%)
  Pallas kernels  55.9 us (35%)
  waiting for transfers between devices  33.7 us (21%)
  local copies, waits for them, and re-layouts  3.54 us (2%)
    ppermute x33, starting transfers between devices, send(): return lax.ppermute(x, 'st', pairs)  66.1 us
    ppermute x33, waiting for transfers between devices, send(): return lax.ppermute(x, 'st', pairs)  33.7 us
    pallas_call x8, Pallas kernels, mixer(): pl.pallas_call(functools.partial(mixer_body, first), grid=(1,), in_specs=...  18.7 us
    pallas_call x8, Pallas kernels, parts(): pl.pallas_call(functools.partial(find_parts, count), in_specs=[scalars] +...  14.2 us
    pallas_call x1, Pallas kernels, mixer_inputs(): pl.pallas_call(mixed_body, in_specs=[hbm] * 4 + [whole] * 3 + [pl.BlockSp...  5.38 us
    pallas_call x1, Pallas kernels, project_passages(): pl.pallas_call(passages_body, in_specs=[hbm, hbm, hbm, pl.BlockSpec(memor...  5.23 us
    pallas_call x15, Pallas kernels, merge(): pl.pallas_call(functools.partial(merge_body, n * SLOTS, start is not None...  4.75 us
    unnamed x28, local copies, waits for them, and re-layouts  3.53 us
  transfers between devices with their start and end apart: 33, of which 19 were waited for; matrix products, arithmetic and copies ran while one was open for 0% of the time, Pallas kernels for 32%

profile of v2, /device:TPU:33, one launch (start us, length us, event | category | flops | bytes accessed | tf_op | source)
XLA Modules:
  0.0 159.8 jit_solution(4567750676710089604)
XLA Ops:
  1.4 3.0 %query.1.after_ref.refs_0_ = bf16[1032,128]{1,0:T(8,128)(2,1)S(1)} custom-call(bf16[512,2048]{1,0:T(8,128)(2,1)} %x_hbm.3, bf16[2048,256]{1,0:T(8,128)(2,1)} %w_hbm.1, s32[4,8]{1,0:T(4,128)S(1)} %bitcast.10, s32[4,8]{1,0:T(4,128)S(1)} %bitcast.11), custom_call_target="tpu_custom_call" | custom-call | flops 536870912 | bytes 3145728 | tf_op jit(solution)/shard_map/query/pallas_call | solution.py:91
  4.4 23.0 %collective-permute-start.2 = (bf16[1032,128]{1,0:T(8,128)(2,1)S(1)}, bf16[1032,128]{1,0:T(8,128)(2,1)S(1)}, u32[]{:S(2)}, u32[]{:S(2)}) collective-permute-start(bf16[1032,128]{1,0:T(8,128)(2,1)S(1)} %query.1.after_ref.refs_0_), channel_id=1, source_target_pairs={{0,8},{4,124},{8,16},{12,4},{16,24},{20,12},{24,32},{28,20},{32,40... | collective-permute-start | bytes 792584 | tf_op jit(solution)/shard_map/ppermute | solution.py:569
  27.4 5.4 %collective-permute-done.2.refs_0_ = bf16[1032,128]{1,0:T(8,128)(2,1)S(1)} collective-permute-done((bf16[1032,128]{1,0:T(8,128)(2,1)S(1)}, bf16[1032,128]{1,0:T(8,128)(2,1)S(1)}, u32[]{:S(2)}, u32[]{:S(2)}) %collective-permute-start.2) | collective-permute-done | bytes 264224 | tf_op jit(solution)/shard_map/ppermute | solution.py:569
  32.9 3.1 %collective-permute-start.3 = (bf16[1032,128]{1,0:T(8,128)(2,1)S(1)}, bf16[1032,128]{1,0:T(8,128)(2,1)S(1)}, u32[]{:S(2)}, u32[]{:S(2)}) collective-permute-start(bf16[1032,128]{1,0:T(8,128)(2,1)S(1)} %collective-permute-done.2.refs_0_), channel_id=1, source_target_pairs={{0,8},{4,124},{8,16},{12,4},{16,24},{20,12},{24,32},{28,20},{32,40... | collective-permute-start | bytes 792584 | tf_op jit(solution)/shard_map/ppermute | solution.py:569
  36.7 2.6 %collective-permute-done.3.refs_0_ = bf16[1032,128]{1,0:T(8,128)(2,1)S(1)} collective-permute-done((bf16[1032,128]{1,0:T(8,128)(2,1)S(1)}, bf16[1032,128]{1,0:T(8,128)(2,1)S(1)}, u32[]{:S(2)}, u32[]{:S(2)}) %collective-permute-start.3) | collective-permute-done | bytes 264224 | tf_op jit(solution)/shard_map/ppermute | solution.py:569
  39.3 3.1 %collective-permute-start.4 = (bf16[1032,128]{1,0:T(8,128)(2,1)S(1)}, bf16[1032,128]{1,0:T(8,128)(2,1)S(1)}, u32[]{:S(2)}, u32[]{:S(2)}) collective-permute-start(bf16[1032,128]{1,0:T(8,128)(2,1)S(1)} %collective-permute-done.3.refs_0_), channel_id=1, source_target_pairs={{0,8},{4,124},{8,16},{12,4},{16,24},{20,12},{24,32},{28,20},{32,40... | collective-permute-start | bytes 792584 | tf_op jit(solution)/shard_map/ppermute | solution.py:569
  42.5 2.8 %collective-permute-start.10 = (bf16[1032,128]{1,0:T(8,128)(2,1)S(1)}, bf16[1032,128]{1,0:T(8,128)(2,1)S(1)}, u32[]{:S(2)}, u32[]{:S(2)}) collective-permute-start(bf16[1032,128]{1,0:T(8,128)(2,1)S(1)} %collective-permute-done.9.refs_1_), channel_id=1, source_target_pairs={{0,8},{4,124},{8,16},{12,4},{16,24},{20,12},{24,32},{28,20},{32,40... | collective-permute-start | bytes 792584 | tf_op jit(solution)/shard_map/ppermute | solution.py:569
  45.3 5.2 %passages.1.refs_1_.refs_2_.kv_ref = bf16[16,256,128]{2,1,0:T(8,128)(2,1)S(1)} custom-call(bf16[1024,2048]{1,0:T(8,128)(2,1)} %bitcast.31, bf16[2048,256]{1,0:T(8,128)(2,1)} %wk_hbm.3, bf16[2048,256]{1,0:T(8,128)(2,1)} %wv_hbm.3, bf16[1032,128]{1,0:T(8,128)(2,1)S(1)} %query.1.after_ref.refs_0_), custom_call_target="tpu_custom_call" | custom-call | flops 2147483648 | bytes 4194304 | tf_op jit(solution)/shard_map/passages/pallas_call | solution.py:210
  50.8 3.0 %collective-permute-start.5 = (bf16[1032,128]{1,0:T(8,128)(2,1)S(1)}, bf16[1032,128]{1,0:T(8,128)(2,1)S(1)}, u32[]{:S(2)}, u32[]{:S(2)}) collective-permute-start(bf16[1032,128]{1,0:T(8,128)(2,1)S(1)} %collective-permute-done.4.refs_0_), channel_id=1, source_target_pairs={{0,8},{4,124},{8,16},{12,4},{16,24},{20,12},{24,32},{28,20},{32,40... | collective-permute-start | bytes 792584 | tf_op jit(solution)/shard_map/ppermute | solution.py:569
  55.1 1.9 %collective-permute-done.5.refs_0_ = bf16[1032,128]{1,0:T(8,128)(2,1)S(1)} collective-permute-done((bf16[1032,128]{1,0:T(8,128)(2,1)S(1)}, bf16[1032,128]{1,0:T(8,128)(2,1)S(1)}, u32[]{:S(2)}, u32[]{:S(2)}) %collective-permute-start.5) | collective-permute-done | bytes 264224 | tf_op jit(solution)/shard_map/ppermute | solution.py:569
  57.0 3.1 %collective-permute-start.6 = (bf16[1032,128]{1,0:T(8,128)(2,1)S(1)}, bf16[1032,128]{1,0:T(8,128)(2,1)}, u32[]{:S(2)}, u32[]{:S(2)}) collective-permute-start(bf16[1032,128]{1,0:T(8,128)(2,1)S(1)} %collective-permute-done.5.refs_0_), channel_id=1, source_target_pairs={{0,8},{4,124},{8,16},{12,4},{16,24},{20,12},{24,32},{28,20},{32,40... | collective-permute-start | bytes 792584 | tf_op jit(solution)/shard_map/ppermute | solution.py:569
  60.9 2.2 %collective-permute-start.12 = (bf16[1032,128]{1,0:T(8,128)(2,1)}, bf16[1032,128]{1,0:T(8,128)(2,1)}, u32[]{:S(2)}, u32[]{:S(2)}) collective-permute-start(bf16[1032,128]{1,0:T(8,128)(2,1)} %collective-permute-done.11.refs_1_), channel_id=1, source_target_pairs={{0,8},{4,124},{8,16},{12,4},{16,24},{20,12},{24,32},{28,20},{32,40... | collective-permute-start | bytes 792584 | tf_op jit(solution)/shard_map/ppermute | solution.py:569
  63.5 3.2 %collective-permute-start.7 = (bf16[1032,128]{1,0:T(8,128)(2,1)}, bf16[1032,128]{1,0:T(8,128)(2,1)}, u32[]{:S(2)}, u32[]{:S(2)}) collective-permute-start(bf16[1032,128]{1,0:T(8,128)(2,1)} %collective-permute-done.6.refs_0_), channel_id=1, source_target_pairs={{0,8},{4,124},{8,16},{12,4},{16,24},{20,12},{24,32},{28,20},{32,40... | collective-permute-start | bytes 792584 | tf_op jit(solution)/shard_map/ppermute | solution.py:569
  66.8 3.1 %collective-permute-start.13 = (bf16[1032,128]{1,0:T(8,128)(2,1)}, bf16[1032,128]{1,0:T(8,128)(2,1)S(1)}, u32[]{:S(2)}, u32[]{:S(2)}) collective-permute-start(bf16[1032,128]{1,0:T(8,128)(2,1)} %collective-permute-done.12.refs_1_), channel_id=1, source_target_pairs={{0,8},{4,124},{8,16},{12,4},{16,24},{20,12},{24,32},{28,20},{32,40... | collective-permute-start | bytes 792584 | tf_op jit(solution)/shard_map/ppermute | solution.py:569
  70.0 5.4 %mixer_inputs.1 = (bf16[3,8,128,128]{3,2,1,0:T(8,128)(2,1)S(1)}, f32[512,8]{1,0:T(8,128)S(1)}) custom-call(bf16[512,2048]{1,0:T(8,128)(2,1)} %x_hbm.3, bf16[2048,256]{1,0:T(8,128)(2,1)} %wq_hbm.1, bf16[2048,256]{1,0:T(8,128)(2,1)} %wk_hbm.2, bf16[2048,256]{1,0:T(8,128)(2,1)} %wv_hbm.2, bf16[2,2048]{1,0:T(2,128)(2,1)S(1)} %bitcast.12, ...), custom_call_target="tpu_custom_call" | custom-call | flops 1610612736 | bytes 5242880 | tf_op jit(solution)/shard_map/mixer_inputs/pallas_call | solution.py:153
  75.5 1.5 parts.8
  77.2 1.6 %parts.9 = (f32[8,128,128]{2,1,0:T(8,128)S(1)}, f32[8,8,128]{2,1,0:T(8,128)S(1)}) custom-call(s32[2]{0:T(128)S(1)} %pad_add_fusion.own_ref.refs_1_, bf16[1032,128]{1,0:T(8,128)(2,1)S(1)} %collective-permute-done.2.refs_0_, bf16[1032,128]{1,0:T(8,128)(2,1)S(1)} %collective-permute-done.after_ref.refs_1_, ...), custom_call_target="tpu_custom_call" | custom-call | flops 838860800 | bytes 1024000 | tf_op jit(solution)/shard_map/parts/pallas_call | solution.py:391
  78.8 1.6 %parts.10 = (f32[8,128,128]{2,1,0:T(8,128)S(1)}, f32[8,8,128]{2,1,0:T(8,128)S(1)}) custom-call(s32[2]{0:T(128)S(1)} %pad_add_fusion.own_ref.refs_1_, bf16[1032,128]{1,0:T(8,128)(2,1)S(1)} %collective-permute-done.3.refs_0_, bf16[1032,128]{1,0:T(8,128)(2,1)S(1)} %collective-permute-done.9.refs_1_, bf16[16,256,128]{2,1,0:T(8,128)(2,1)S(1)} %passages.1.refs_1_.refs_2_.kv_ref, ...), custom_call_target="tpu_custom_call" | custom-call | flops 838860800 | bytes 1024000 | tf_op jit(solution)/shard_map/parts/pallas_call | solution.py:391
  80.5 1.6 %parts.11 = (f32[8,128,128]{2,1,0:T(8,128)S(1)}, f32[8,8,128]{2,1,0:T(8,128)S(1)}) custom-call(s32[2]{0:T(128)S(1)} %pad_add_fusion.own_ref.refs_1_, bf16[1032,128]{1,0:T(8,128)(2,1)S(1)} %copy-done.3, bf16[1032,128]{1,0:T(8,128)(2,1)S(1)} %copy-done.5, bf16[16,256,128]{2,1,0:T(8,128)(2,1)S(1)} %passages.1.refs_1_.refs_2_.kv_ref, ...), custom_call_target="tpu_custom_call" | custom-call | flops 838860800 | bytes 1024000 | tf_op jit(solution)/shard_map/parts/pallas_call | solution.py:391
  82.1 2.0 %collective-permute-start.16 = (bf16[1032,128]{1,0:T(8,128)(2,1)S(1)}, bf16[1032,128]{1,0:T(8,128)(2,1)S(1)}, u32[]{:S(2)}, u32[]{:S(2)}) collective-permute-start(bf16[1032,128]{1,0:T(8,128)(2,1)S(1)} %collective-permute-done.8.refs_0_), channel_id=1, source_target_pairs={{4,124},{12,4},{20,12},{28,20},{36,28},{44,36},{52,44},{60,52},{68... | collective-permute-start | bytes 792584 | tf_op jit(solution)/shard_map/ppermute | solution.py:569
  84.1 2.0 %parts.12 = (f32[8,128,128]{2,1,0:T(8,128)S(1)}, f32[8,8,128]{2,1,0:T(8,128)S(1)}) custom-call(s32[2]{0:T(128)S(1)} %pad_add_fusion.own_ref.refs_1_, bf16[1032,128]{1,0:T(8,128)(2,1)S(1)} %copy-done.7, bf16[1032,128]{1,0:T(8,128)(2,1)} %collective-permute-done.11.refs_1_, bf16[16,256,128]{2,1,0:T(8,128)(2,1)S(1)} %passages.1.refs_1_.refs_2_.kv_ref, ...), custom_call_target="tpu_custom_call" | custom-call | flops 838860800 | bytes 1024000 | tf_op jit(solution)/shard_map/parts/pallas_call | solution.py:391
  86.1 3.6 %collective-permute-start.15 = (bf16[1032,128]{1,0:T(8,128)(2,1)S(1)}, bf16[1032,128]{1,0:T(8,128)(2,1)S(1)}, u32[]{:S(2)}, u32[]{:S(2)}) collective-permute-start(bf16[1032,128]{1,0:T(8,128)(2,1)S(1)} %collective-permute-done.14.refs_1_), channel_id=1, source_target_pairs={{4,124},{12,4},{20,12},{28,20},{36,28},{44,36},{52,44},{60,52},{68... | collective-permute-start | bytes 792584 | tf_op jit(solution)/shard_map/ppermute | solution.py:569
  89.8 2.1 %parts.13 = (f32[8,128,128]{2,1,0:T(8,128)S(1)}, f32[8,8,128]{2,1,0:T(8,128)S(1)}) custom-call(s32[2]{0:T(128)S(1)} %pad_add_fusion.own_ref.refs_1_, bf16[1032,128]{1,0:T(8,128)(2,1)} %collective-permute-done.6.refs_0_, bf16[1032,128]{1,0:T(8,128)(2,1)} %collective-permute-done.12.refs_1_, bf16[16,256,128]{2,1,0:T(8,128)(2,1)S(1)} %passages.1.refs_1_.refs_2_.kv_ref, ...), custom_call_target="tpu_custom_call" | custom-call | flops 838860800 | bytes 1024000 | tf_op jit(solution)/shard_map/parts/pallas_call | solution.py:391
  91.9 2.0 %parts.14 = (f32[8,128,128]{2,1,0:T(8,128)S(1)}, f32[8,8,128]{2,1,0:T(8,128)S(1)}) custom-call(s32[2]{0:T(128)S(1)} %pad_add_fusion.own_ref.refs_1_, bf16[1032,128]{1,0:T(8,128)(2,1)} %collective-permute-done.7.refs_0_, bf16[1032,128]{1,0:T(8,128)(2,1)S(1)} %collective-permute-done.13.refs_1_, bf16[16,256,128]{2,1,0:T(8,128)(2,1)S(1)} %passages.1.refs_1_.refs_2_.kv_ref, ...), custom_call_target="tpu_custom_call" | custom-call | flops 838860800 | bytes 1024000 | tf_op jit(solution)/shard_map/parts/pallas_call | solution.py:391
  93.9 1.6 %parts.15 = (f32[8,128,128]{2,1,0:T(8,128)S(1)}, f32[8,8,128]{2,1,0:T(8,128)S(1)}) custom-call(s32[2]{0:T(128)S(1)} %pad_add_fusion.own_ref.refs_1_, bf16[1032,128]{1,0:T(8,128)(2,1)S(1)} %collective-permute-done.8.refs_0_, bf16[1032,128]{1,0:T(8,128)(2,1)S(1)} %collective-permute-done.14.refs_1_, bf16[16,256,128]{2,1,0:T(8,128)(2,1)S(1)} %passages.1.refs_1_.refs_2_.kv_ref, ...), custom_call_target="tpu_custom_call" | custom-call | flops 838860800 | bytes 1024000 | tf_op jit(solution)/shard_map/parts/pallas_call | solution.py:391
  95.6 1.7 %far.2.after_ref = bf16[8,136,128]{2,1,0:T(8,128)(2,1)S(1)} custom-call(s32[2]{0:T(128)S(1)} %pad_add_fusion.own_ref.refs_1_, bf16[1032,128]{1,0:T(8,128)(2,1)S(1)} %collective-permute-done.16.q_ref, bf16[16,256,128]{2,1,0:T(8,128)(2,1)S(1)} %passages.1.refs_1_.refs_2_.kv_ref, bf16[16,256,128]{2,1,0:T(8,128)(2,1)S(1)} %collective-permute-done.1.refs_2_.refs_3_.mate_ref, ...), custom_call_target="tpu_custom_call" | custom-call | flops 524288000 | bytes 512000 | tf_op jit(solution)/shard_map/far/pallas_call | solution.py:470
  97.3 2.0 %collective-permute-start.17 = (bf16[8,136,128]{2,1,0:T(8,128)(2,1)S(1)}, bf16[8,136,128]{2,1,0:T(8,128)(2,1)S(1)}, u32[]{:S(2)}, u32[]{:S(2)}) collective-permute-start(bf16[8,136,128]{2,1,0:T(8,128)(2,1)S(1)} %far.2.after_ref), channel_id=1, source_target_pairs={{124,4},{4,12},{12,20},{20,28},{28,36},{36,44},{44,52},{52,60},{60... | collective-permute-start | bytes 835592 | tf_op jit(solution)/shard_map/ppermute | solution.py:569
  99.2 1.7 %far.3.after_ref = bf16[8,136,128]{2,1,0:T(8,128)(2,1)S(1)} custom-call(s32[2]{0:T(128)S(1)} %pad_add_fusion.own_ref.refs_1_, bf16[1032,128]{1,0:T(8,128)(2,1)S(1)} %collective-permute-done.15.q_ref, bf16[16,256,128]{2,1,0:T(8,128)(2,1)S(1)} %passages.1.refs_1_.refs_2_.kv_ref, bf16[16,256,128]{2,1,0:T(8,128)(2,1)S(1)} %collective-permute-done.1.refs_2_.refs_3_.mate_ref, ...), custom_call_target="tpu_custom_call" | custom-call | flops 524288000 | bytes 512000 | tf_op jit(solution)/shard_map/far/pallas_call | solution.py:470
  100.9 3.1 %collective-permute-start.18 = (bf16[8,136,128]{2,1,0:T(8,128)(2,1)S(1)}, bf16[8,136,128]{2,1,0:T(8,128)(2,1)S(1)}, u32[]{:S(2)}, u32[]{:S(2)}) collective-permute-start(bf16[8,136,128]{2,1,0:T(8,128)(2,1)S(1)} %far.3.after_ref), channel_id=1, source_target_pairs={{124,4},{4,12},{12,20},{20,28},{28,36},{36,44},{44,52},{52,60},{60... | collective-permute-start | bytes 835592 | tf_op jit(solution)/shard_map/ppermute | solution.py:569
  104.0 1.8 %collective-permute-done.17.refs_0_ = bf16[8,136,128]{2,1,0:T(8,128)(2,1)S(1)} collective-permute-done((bf16[8,136,128]{2,1,0:T(8,128)(2,1)S(1)}, bf16[8,136,128]{2,1,0:T(8,128)(2,1)S(1)}, u32[]{:S(2)}, u32[]{:S(2)}) %collective-permute-start.17) | collective-permute-done | bytes 278560 | tf_op jit(solution)/shard_map/ppermute | solution.py:569
  106.7 2.7 %collective-permute-done.18.refs_0_ = bf16[8,136,128]{2,1,0:T(8,128)(2,1)S(1)} collective-permute-done((bf16[8,136,128]{2,1,0:T(8,128)(2,1)S(1)}, bf16[8,136,128]{2,1,0:T(8,128)(2,1)S(1)}, u32[]{:S(2)}, u32[]{:S(2)}) %collective-permute-start.18) | collective-permute-done | bytes 278560 | tf_op jit(solution)/shard_map/ppermute | solution.py:569
  110.6 2.3 %mixer.8 = (f32[1,128,128]{2,1,0:T(8,128)S(1)}, f32[2,128,128]{2,1,0:T(8,128)S(1)}) custom-call(bf16[3,8,128,128]{3,2,1,0:T(8,128)(2,1)S(1)} %get-tuple-element.42.qkv_ref, f32[512,8]{1,0:T(8,128)S(1)} %get-tuple-element.39.refs_3_.lg_ref, f32[2,512]{1,0:T(2,128)S(1)} %bitcast.15, f32[2]{0:T(128)S(1)} %copy-done.12, f32[1,128]{1,0:T(1,128)S(1)} %bitcast.23, ...), custom_call_target="tpu_custom_call" | custom-call | flops 524288000 | bytes 307200 | tf_op jit(solution)/shard_map/mixer/pallas_call | solution.py:296
  113.6 1.5 collective-permute-start.21
  115.1 1.8 %collective-permute-done.20.refs_0_ = bf16[8,136,128]{2,1,0:T(8,128)(2,1)S(1)} collective-permute-done((bf16[8,136,128]{2,1,0:T(8,128)(2,1)S(1)}, bf16[8,136,128]{2,1,0:T(8,128)(2,1)S(1)}, u32[]{:S(2)}, u32[]{:S(2)}) %collective-permute-start.20) | collective-permute-done | bytes 278560 | tf_op jit(solution)/shard_map/ppermute | solution.py:569
  117.4 2.3 %mixer.9 = (f32[1,128,128]{2,1,0:T(8,128)S(1)}, f32[2,128,128]{2,1,0:T(8,128)S(1)}) custom-call(bf16[3,8,128,128]{3,2,1,0:T(8,128)(2,1)S(1)} %get-tuple-element.42.qkv_ref, f32[512,8]{1,0:T(8,128)S(1)} %get-tuple-element.39.refs_3_.lg_ref, f32[2,512]{1,0:T(2,128)S(1)} %bitcast.16, f32[2]{0:T(128)S(1)} %copy-done.12, f32[1,128]{1,0:T(1,128)S(1)} %bitcast.24, ...), custom_call_target="tpu_custom_call" | custom-call | flops 524288000 | bytes 307200 | tf_op jit(solution)/shard_map/mixer/pallas_call | solution.py:296
  121.3 2.7 %collective-permute-done.22.refs_0_ = bf16[8,136,128]{2,1,0:T(8,128)(2,1)S(1)} collective-permute-done((bf16[8,136,128]{2,1,0:T(8,128)(2,1)S(1)}, bf16[8,136,128]{2,1,0:T(8,128)(2,1)S(1)}, u32[]{:S(2)}, u32[]{:S(2)}) %collective-permute-start.22) | collective-permute-done | bytes 278560 | tf_op jit(solution)/shard_map/ppermute | solution.py:569
  124.5 2.3 %mixer.10 = (f32[1,128,128]{2,1,0:T(8,128)S(1)}, f32[2,128,128]{2,1,0:T(8,128)S(1)}) custom-call(bf16[3,8,128,128]{3,2,1,0:T(8,128)(2,1)S(1)} %get-tuple-element.42.qkv_ref, f32[512,8]{1,0:T(8,128)S(1)} %get-tuple-element.39.refs_3_.lg_ref, f32[2,512]{1,0:T(2,128)S(1)} %bitcast.17, f32[2]{0:T(128)S(1)} %copy-done.12, f32[1,128]{1,0:T(1,128)S(1)} %bitcast.25, ...), custom_call_target="tpu_custom_call" | custom-call | flops 524288000 | bytes 307200 | tf_op jit(solution)/shard_map/mixer/pallas_call | solution.py:296
  127.5 1.4 collective-permute-start.25
  128.9 2.2 %collective-permute-done.24.refs_0_ = bf16[8,136,128]{2,1,0:T(8,128)(2,1)S(1)} collective-permute-done((bf16[8,136,128]{2,1,0:T(8,128)(2,1)S(1)}, bf16[8,136,128]{2,1,0:T(8,128)(2,1)S(1)}, u32[]{:S(2)}, u32[]{:S(2)}) %collective-permute-start.24) | collective-permute-done | bytes 278560 | tf_op jit(solution)/shard_map/ppermute | solution.py:569
  131.5 2.3 %mixer.11 = (f32[1,128,128]{2,1,0:T(8,128)S(1)}, f32[2,128,128]{2,1,0:T(8,128)S(1)}) custom-call(bf16[3,8,128,128]{3,2,1,0:T(8,128)(2,1)S(1)} %get-tuple-element.42.qkv_ref, f32[512,8]{1,0:T(8,128)S(1)} %get-tuple-element.39.refs_3_.lg_ref, f32[2,512]{1,0:T(2,128)S(1)} %bitcast.18, f32[2]{0:T(128)S(1)} %copy-done.12, f32[1,128]{1,0:T(1,128)S(1)} %bitcast.26, ...), custom_call_target="tpu_custom_call" | custom-call | flops 524288000 | bytes 307200 | tf_op jit(solution)/shard_map/mixer/pallas_call | solution.py:296
  135.3 2.8 %collective-permute-done.26.refs_0_ = bf16[8,136,128]{2,1,0:T(8,128)(2,1)S(1)} collective-permute-done((bf16[8,136,128]{2,1,0:T(8,128)(2,1)S(1)}, bf16[8,136,128]{2,1,0:T(8,128)(2,1)S(1)}, u32[]{:S(2)}, u32[]{:S(2)}) %collective-permute-start.26) | collective-permute-done | bytes 278560 | tf_op jit(solution)/shard_map/ppermute | solution.py:569
  138.5 2.3 %mixer.12 = (f32[1,128,128]{2,1,0:T(8,128)S(1)}, f32[2,128,128]{2,1,0:T(8,128)S(1)}) custom-call(bf16[3,8,128,128]{3,2,1,0:T(8,128)(2,1)S(1)} %get-tuple-element.42.qkv_ref, f32[512,8]{1,0:T(8,128)S(1)} %get-tuple-element.39.refs_3_.lg_ref, f32[2,512]{1,0:T(2,128)S(1)} %bitcast.19, f32[2]{0:T(128)S(1)} %copy-done.12, f32[1,128]{1,0:T(1,128)S(1)} %bitcast.27, ...), custom_call_target="tpu_custom_call" | custom-call | flops 524288000 | bytes 307200 | tf_op jit(solution)/shard_map/mixer/pallas_call | solution.py:296
  142.3 2.8 %collective-permute-done.28.refs_0_ = bf16[8,136,128]{2,1,0:T(8,128)(2,1)S(1)} collective-permute-done((bf16[8,136,128]{2,1,0:T(8,128)(2,1)S(1)}, bf16[8,136,128]{2,1,0:T(8,128)(2,1)S(1)}, u32[]{:S(2)}, u32[]{:S(2)}) %collective-permute-start.28) | collective-permute-done | bytes 278560 | tf_op jit(solution)/shard_map/ppermute | solution.py:569
  145.5 2.3 %mixer.13 = (f32[1,128,128]{2,1,0:T(8,128)S(1)}, f32[2,128,128]{2,1,0:T(8,128)S(1)}) custom-call(bf16[3,8,128,128]{3,2,1,0:T(8,128)(2,1)S(1)} %get-tuple-element.42.qkv_ref, f32[512,8]{1,0:T(8,128)S(1)} %get-tuple-element.39.refs_3_.lg_ref, f32[2,512]{1,0:T(2,128)S(1)} %bitcast.20, f32[2]{0:T(128)S(1)} %copy-done.12, f32[1,128]{1,0:T(1,128)S(1)} %bitcast.28, ...), custom_call_target="tpu_custom_call" | custom-call | flops 524288000 | bytes 307200 | tf_op jit(solution)/shard_map/mixer/pallas_call | solution.py:296
  149.2 2.8 %collective-permute-done.30.refs_0_ = bf16[8,136,128]{2,1,0:T(8,128)(2,1)S(1)} collective-permute-done((bf16[8,136,128]{2,1,0:T(8,128)(2,1)S(1)}, bf16[8,136,128]{2,1,0:T(8,128)(2,1)S(1)}, u32[]{:S(2)}, u32[]{:S(2)}) %collective-permute-start.30) | collective-permute-done | bytes 278560 | tf_op jit(solution)/shard_map/ppermute | solution.py:569
  152.5 2.3 %mixer.14 = (f32[1,128,128]{2,1,0:T(8,128)S(1)}, f32[2,128,128]{2,1,0:T(8,128)S(1)}) custom-call(bf16[3,8,128,128]{3,2,1,0:T(8,128)(2,1)S(1)} %get-tuple-element.42.qkv_ref, f32[512,8]{1,0:T(8,128)S(1)} %get-tuple-element.39.refs_3_.lg_ref, f32[2,512]{1,0:T(2,128)S(1)} %bitcast.21, f32[2]{0:T(128)S(1)} %copy-done.12, f32[1,128]{1,0:T(1,128)S(1)} %bitcast.29, ...), custom_call_target="tpu_custom_call" | custom-call | flops 524288000 | bytes 307200 | tf_op jit(solution)/shard_map/mixer/pallas_call | solution.py:296
  154.8 2.3 %mixer.15 = (f32[1,128,128]{2,1,0:T(8,128)S(1)}, f32[2,128,128]{2,1,0:T(8,128)S(1)}) custom-call(bf16[3,8,128,128]{3,2,1,0:T(8,128)(2,1)S(1)} %get-tuple-element.42.qkv_ref, f32[512,8]{1,0:T(8,128)S(1)} %get-tuple-element.39.refs_3_.lg_ref, f32[2,512]{1,0:T(2,128)S(1)} %bitcast.22, f32[2]{0:T(128)S(1)} %copy-done.12, f32[1,128]{1,0:T(1,128)S(1)} %bitcast.30, ...), custom_call_target="tpu_custom_call" | custom-call | flops 524288000 | bytes 307200 | tf_op jit(solution)/shard_map/mixer/pallas_call | solution.py:296
  158.5 1.4 finish.1
  (85 shorter events, 18.2 us)
Async XLA Ops:
  0.0 0.7 copy-start
  0.7 0.7 copy-start.1
  4.4 65.6 %copy-start.8 = (bf16[2048,2]{0,1:T(2,128)(2,1)S(1)}, bf16[2048,2]{0,1:T(2,128)(2,1)}, u32[]{:S(2)}) copy-start(bf16[2048,2]{0,1:T(2,128)(2,1)} %param.23) | copy-start | bytes 24580
  4.4 65.6 %copy-start.9 = (bf16[2048,2]{0,1:T(2,128)(2,1)S(1)}, bf16[2048,2]{0,1:T(2,128)(2,1)}, u32[]{:S(2)}) copy-start(bf16[2048,2]{0,1:T(2,128)(2,1)} %param.24) | copy-start | bytes 24580
  4.4 65.6 %copy-start.10 = (bf16[2048,2]{0,1:T(2,128)(2,1)S(1)}, bf16[2048,2]{0,1:T(2,128)(2,1)}, u32[]{:S(2)}) copy-start(bf16[2048,2]{0,1:T(2,128)(2,1)} %param.31) | copy-start | bytes 24580
  4.4 28.5 %collective-permute-start.2 = (bf16[1032,128]{1,0:T(8,128)(2,1)S(1)}, bf16[1032,128]{1,0:T(8,128)(2,1)S(1)}, u32[]{:S(2)}, u32[]{:S(2)}) collective-permute-start(bf16[1032,128]{1,0:T(8,128)(2,1)S(1)} %query.1.after_ref.refs_0_), channel_id=1, source_target_pairs={{0,8},{4,124},{8,16},{12,4},{16,24},{20,12},{24,32},{28,20},{32,40... | collective-permute-start | bytes 792584 | tf_op jit(solution)/shard_map/ppermute | solution.py:569
  27.4 8.6 %collective-permute-start = (bf16[1032,128]{1,0:T(8,128)(2,1)S(1)}, bf16[1032,128]{1,0:T(8,128)(2,1)S(1)}, u32[]{:S(2)}, u32[]{:S(2)}) collective-permute-start(bf16[1032,128]{1,0:T(8,128)(2,1)S(1)} %query.1.after_ref.refs_0_), channel_id=1, source_target_pairs={{4,8},{0,124},{12,16},{8,4},{20,24},{16,12},{28,32},{24,20},{36,40... | collective-permute-start | bytes 792584 | tf_op jit(solution)/shard_map/ppermute | solution.py:569
  32.9 6.5 %collective-permute-start.3 = (bf16[1032,128]{1,0:T(8,128)(2,1)S(1)}, bf16[1032,128]{1,0:T(8,128)(2,1)S(1)}, u32[]{:S(2)}, u32[]{:S(2)}) collective-permute-start(bf16[1032,128]{1,0:T(8,128)(2,1)S(1)} %collective-permute-done.2.refs_0_), channel_id=1, source_target_pairs={{0,8},{4,124},{8,16},{12,4},{16,24},{20,12},{24,32},{28,20},{32,40... | collective-permute-start | bytes 792584 | tf_op jit(solution)/shard_map/ppermute | solution.py:569
  36.0 6.5 %collective-permute-start.9 = (bf16[1032,128]{1,0:T(8,128)(2,1)S(1)}, bf16[1032,128]{1,0:T(8,128)(2,1)S(1)}, u32[]{:S(2)}, u32[]{:S(2)}) collective-permute-start(bf16[1032,128]{1,0:T(8,128)(2,1)S(1)} %collective-permute-done.after_ref.refs_1_), channel_id=1, source_target_pairs={{0,8},{4,124},{8,16},{12,4},{16,24},{20,12},{24,32},{28,20},{32,40... | collective-permute-start | bytes 792584 | tf_op jit(solution)/shard_map/ppermute | solution.py:569
  39.3 11.4 %collective-permute-start.4 = (bf16[1032,128]{1,0:T(8,128)(2,1)S(1)}, bf16[1032,128]{1,0:T(8,128)(2,1)S(1)}, u32[]{:S(2)}, u32[]{:S(2)}) collective-permute-start(bf16[1032,128]{1,0:T(8,128)(2,1)S(1)} %collective-permute-done.3.refs_0_), channel_id=1, source_target_pairs={{0,8},{4,124},{8,16},{12,4},{16,24},{20,12},{24,32},{28,20},{32,40... | collective-permute-start | bytes 792584 | tf_op jit(solution)/shard_map/ppermute | solution.py:569
  42.5 12.0 %collective-permute-start.10 = (bf16[1032,128]{1,0:T(8,128)(2,1)S(1)}, bf16[1032,128]{1,0:T(8,128)(2,1)S(1)}, u32[]{:S(2)}, u32[]{:S(2)}) collective-permute-start(bf16[1032,128]{1,0:T(8,128)(2,1)S(1)} %collective-permute-done.9.refs_1_), channel_id=1, source_target_pairs={{0,8},{4,124},{8,16},{12,4},{16,24},{20,12},{24,32},{28,20},{32,40... | collective-permute-start | bytes 792584 | tf_op jit(solution)/shard_map/ppermute | solution.py:569
  50.5 25.0 %collective-permute-start.1 = (bf16[16,256,128]{2,1,0:T(8,128)(2,1)S(1)}, bf16[16,256,128]{2,1,0:T(8,128)(2,1)S(1)}, u32[]{:S(2)}, u32[]{:S(2)}) collective-permute-start(bf16[16,256,128]{2,1,0:T(8,128)(2,1)S(1)} %passages.1.refs_1_.refs_2_.kv_ref), channel_id=1, source_target_pairs={{0,4},{4,0},{8,12},{12,8},{16,20},{20,16},{24,28},{28,24},{32,36},... | collective-permute-start | bytes 3145736 | tf_op jit(solution)/shard_map/ppermute | solution.py:569
  50.8 6.3 %collective-permute-start.5 = (bf16[1032,128]{1,0:T(8,128)(2,1)S(1)}, bf16[1032,128]{1,0:T(8,128)(2,1)S(1)}, u32[]{:S(2)}, u32[]{:S(2)}) collective-permute-start(bf16[1032,128]{1,0:T(8,128)(2,1)S(1)} %collective-permute-done.4.refs_0_), channel_id=1, source_target_pairs={{0,8},{4,124},{8,16},{12,4},{16,24},{20,12},{24,32},{28,20},{32,40... | collective-permute-start | bytes 792584 | tf_op jit(solution)/shard_map/ppermute | solution.py:569
  53.7 0.7 copy-start.2
  54.4 6.4 %collective-permute-start.11 = (bf16[1032,128]{1,0:T(8,128)(2,1)S(1)}, bf16[1032,128]{1,0:T(8,128)(2,1)}, u32[]{:S(2)}, u32[]{:S(2)}) collective-permute-start(bf16[1032,128]{1,0:T(8,128)(2,1)S(1)} %collective-permute-done.10.refs_1_), channel_id=1, source_target_pairs={{0,8},{4,124},{8,16},{12,4},{16,24},{20,12},{24,32},{28,20},{32,40... | collective-permute-start | bytes 792584 | tf_op jit(solution)/shard_map/ppermute | solution.py:569
  54.4 0.7 copy-start.4
  57.0 6.5 %collective-permute-start.6 = (bf16[1032,128]{1,0:T(8,128)(2,1)S(1)}, bf16[1032,128]{1,0:T(8,128)(2,1)}, u32[]{:S(2)}, u32[]{:S(2)}) collective-permute-start(bf16[1032,128]{1,0:T(8,128)(2,1)S(1)} %collective-permute-done.5.refs_0_), channel_id=1, source_target_pairs={{0,8},{4,124},{8,16},{12,4},{16,24},{20,12},{24,32},{28,20},{32,40... | collective-permute-start | bytes 792584 | tf_op jit(solution)/shard_map/ppermute | solution.py:569
  60.2 0.7 copy-start.6
  60.9 5.9 %collective-permute-start.12 = (bf16[1032,128]{1,0:T(8,128)(2,1)}, bf16[1032,128]{1,0:T(8,128)(2,1)}, u32[]{:S(2)}, u32[]{:S(2)}) collective-permute-start(bf16[1032,128]{1,0:T(8,128)(2,1)} %collective-permute-done.11.refs_1_), channel_id=1, source_target_pairs={{0,8},{4,124},{8,16},{12,4},{16,24},{20,12},{24,32},{28,20},{32,40... | collective-permute-start | bytes 792584 | tf_op jit(solution)/shard_map/ppermute | solution.py:569
  63.5 11.8 %collective-permute-start.7 = (bf16[1032,128]{1,0:T(8,128)(2,1)}, bf16[1032,128]{1,0:T(8,128)(2,1)}, u32[]{:S(2)}, u32[]{:S(2)}) collective-permute-start(bf16[1032,128]{1,0:T(8,128)(2,1)} %collective-permute-done.6.refs_0_), channel_id=1, source_target_pairs={{0,8},{4,124},{8,16},{12,4},{16,24},{20,12},{24,32},{28,20},{32,40... | collective-permute-start | bytes 792584 | tf_op jit(solution)/shard_map/ppermute | solution.py:569
  66.8 10.3 %collective-permute-start.13 = (bf16[1032,128]{1,0:T(8,128)(2,1)}, bf16[1032,128]{1,0:T(8,128)(2,1)S(1)}, u32[]{:S(2)}, u32[]{:S(2)}) collective-permute-start(bf16[1032,128]{1,0:T(8,128)(2,1)} %collective-permute-done.12.refs_1_), channel_id=1, source_target_pairs={{0,8},{4,124},{8,16},{12,4},{16,24},{20,12},{24,32},{28,20},{32,40... | collective-permute-start | bytes 792584 | tf_op jit(solution)/shard_map/ppermute | solution.py:569
  75.4 6.7 %collective-permute-start.8 = (bf16[1032,128]{1,0:T(8,128)(2,1)}, bf16[1032,128]{1,0:T(8,128)(2,1)S(1)}, u32[]{:S(2)}, u32[]{:S(2)}) collective-permute-start(bf16[1032,128]{1,0:T(8,128)(2,1)} %collective-permute-done.7.refs_0_), channel_id=1, source_target_pairs={{0,8},{4,124},{8,16},{12,4},{16,24},{20,12},{24,32},{28,20},{32,40... | collective-permute-start | bytes 792584 | tf_op jit(solution)/shard_map/ppermute | solution.py:569
  75.5 4.9 %copy-start.3 = (bf16[1032,128]{1,0:T(8,128)(2,1)S(1)}, bf16[1032,128]{1,0:T(8,128)(2,1)}, u32[]{:S(2)}) copy-start(bf16[1032,128]{1,0:T(8,128)(2,1)} %copy-done.2) | copy-start | bytes 792580
  75.5 4.9 %copy-start.5 = (bf16[1032,128]{1,0:T(8,128)(2,1)S(1)}, bf16[1032,128]{1,0:T(8,128)(2,1)}, u32[]{:S(2)}) copy-start(bf16[1032,128]{1,0:T(8,128)(2,1)} %copy-done.4) | copy-start | bytes 792580
  77.0 9.1 %collective-permute-start.14 = (bf16[1032,128]{1,0:T(8,128)(2,1)S(1)}, bf16[1032,128]{1,0:T(8,128)(2,1)S(1)}, u32[]{:S(2)}, u32[]{:S(2)}) collective-permute-start(bf16[1032,128]{1,0:T(8,128)(2,1)S(1)} %collective-permute-done.13.refs_1_), channel_id=1, source_target_pairs={{0,8},{4,124},{8,16},{12,4},{16,24},{20,12},{24,32},{28,20},{32,40... | collective-permute-start | bytes 792584 | tf_op jit(solution)/shard_map/ppermute | solution.py:569
  77.2 6.9 %copy-start.7 = (bf16[1032,128]{1,0:T(8,128)(2,1)S(1)}, bf16[1032,128]{1,0:T(8,128)(2,1)}, u32[]{:S(2)}) copy-start(bf16[1032,128]{1,0:T(8,128)(2,1)} %copy-done.6) | copy-start | bytes 792580
  82.1 13.5 %collective-permute-start.16 = (bf16[1032,128]{1,0:T(8,128)(2,1)S(1)}, bf16[1032,128]{1,0:T(8,128)(2,1)S(1)}, u32[]{:S(2)}, u32[]{:S(2)}) collective-permute-start(bf16[1032,128]{1,0:T(8,128)(2,1)S(1)} %collective-permute-done.8.refs_0_), channel_id=1, source_target_pairs={{4,124},{12,4},{20,12},{28,20},{36,28},{44,36},{52,44},{60,52},{68... | collective-permute-start | bytes 792584 | tf_op jit(solution)/shard_map/ppermute | solution.py:569
  86.1 13.1 %collective-permute-start.15 = (bf16[1032,128]{1,0:T(8,128)(2,1)S(1)}, bf16[1032,128]{1,0:T(8,128)(2,1)S(1)}, u32[]{:S(2)}, u32[]{:S(2)}) collective-permute-start(bf16[1032,128]{1,0:T(8,128)(2,1)S(1)} %collective-permute-done.14.refs_1_), channel_id=1, source_target_pairs={{4,124},{12,4},{20,12},{28,20},{36,28},{44,36},{52,44},{60,52},{68... | collective-permute-start | bytes 792584 | tf_op jit(solution)/shard_map/ppermute | solution.py:569
  95.6 15.0 %copy-start.11 = (f32[512,2]{0,1:T(2,128)S(1)}, f32[512,2]{0,1:T(2,128)}, u32[]{:S(2)}) copy-start(f32[512,2]{0,1:T(2,128)} %param.26) | copy-start | bytes 12292
  95.6 15.0 %copy-start.12 = (f32[2]{0:T(128)S(1)}, f32[2]{0:T(128)}, u32[]{:S(2)}) copy-start(f32[2]{0:T(128)} %rate_ref.15) | copy-start | bytes 28
  95.6 15.0 %copy-start.13 = (f32[128]{0:T(128)S(1)}, f32[128]{0:T(128)}, u32[]{:S(2)}) copy-start(f32[128]{0:T(128)} %param.27) | copy-start | bytes 1540
  97.3 8.5 %collective-permute-start.17 = (bf16[8,136,128]{2,1,0:T(8,128)(2,1)S(1)}, bf16[8,136,128]{2,1,0:T(8,128)(2,1)S(1)}, u32[]{:S(2)}, u32[]{:S(2)}) collective-permute-start(bf16[8,136,128]{2,1,0:T(8,128)(2,1)S(1)} %far.2.after_ref), channel_id=1, source_target_pairs={{124,4},{4,12},{12,20},{20,28},{28,36},{36,44},{44,52},{52,60},{60... | collective-permute-start | bytes 835592 | tf_op jit(solution)/shard_map/ppermute | solution.py:569
  100.9 8.5 %collective-permute-start.18 = (bf16[8,136,128]{2,1,0:T(8,128)(2,1)S(1)}, bf16[8,136,128]{2,1,0:T(8,128)(2,1)S(1)}, u32[]{:S(2)}, u32[]{:S(2)}) collective-permute-start(bf16[8,136,128]{2,1,0:T(8,128)(2,1)S(1)} %far.3.after_ref), channel_id=1, source_target_pairs={{124,4},{4,12},{12,20},{20,28},{28,36},{36,44},{44,52},{52,60},{60... | collective-permute-start | bytes 835592 | tf_op jit(solution)/shard_map/ppermute | solution.py:569
  106.6 6.7 %collective-permute-start.19 = (bf16[8,136,128]{2,1,0:T(8,128)(2,1)S(1)}, bf16[8,136,128]{2,1,0:T(8,128)(2,1)S(1)}, u32[]{:S(2)}, u32[]{:S(2)}) collective-permute-start(bf16[8,136,128]{2,1,0:T(8,128)(2,1)S(1)} %merge.15.after_ref), channel_id=1, source_target_pairs={{8,0},{124,4},{16,8},{4,12},{24,16},{12,20},{32,24},{20,28},{40,32... | collective-permute-start | bytes 835592 | tf_op jit(solution)/shard_map/ppermute | solution.py:569
  110.2 6.7 %collective-permute-start.20 = (bf16[8,136,128]{2,1,0:T(8,128)(2,1)S(1)}, bf16[8,136,128]{2,1,0:T(8,128)(2,1)S(1)}, u32[]{:S(2)}, u32[]{:S(2)}) collective-permute-start(bf16[8,136,128]{2,1,0:T(8,128)(2,1)S(1)} %merge.16.after_ref), channel_id=1, source_target_pairs={{8,0},{124,4},{16,8},{4,12},{24,16},{12,20},{32,24},{20,28},{40,32... | collective-permute-start | bytes 835592 | tf_op jit(solution)/shard_map/ppermute | solution.py:569
  113.6 6.7 %collective-permute-start.21 = (bf16[8,136,128]{2,1,0:T(8,128)(2,1)S(1)}, bf16[8,136,128]{2,1,0:T(8,128)(2,1)S(1)}, u32[]{:S(2)}, u32[]{:S(2)}) collective-permute-start(bf16[8,136,128]{2,1,0:T(8,128)(2,1)S(1)} %merge.17.after_ref), channel_id=1, source_target_pairs={{8,0},{124,4},{16,8},{4,12},{24,16},{12,20},{32,24},{20,28},{40,32... | collective-permute-start | bytes 835592 | tf_op jit(solution)/shard_map/ppermute | solution.py:569
  117.2 6.7 %collective-permute-start.22 = (bf16[8,136,128]{2,1,0:T(8,128)(2,1)S(1)}, bf16[8,136,128]{2,1,0:T(8,128)(2,1)S(1)}, u32[]{:S(2)}, u32[]{:S(2)}) collective-permute-start(bf16[8,136,128]{2,1,0:T(8,128)(2,1)S(1)} %merge.18.after_ref), channel_id=1, source_target_pairs={{8,0},{124,4},{16,8},{4,12},{24,16},{12,20},{32,24},{20,28},{40,32... | collective-permute-start | bytes 835592 | tf_op jit(solution)/shard_map/ppermute | solution.py:569
  120.6 6.7 %collective-permute-start.23 = (bf16[8,136,128]{2,1,0:T(8,128)(2,1)S(1)}, bf16[8,136,128]{2,1,0:T(8,128)(2,1)S(1)}, u32[]{:S(2)}, u32[]{:S(2)}) collective-permute-start(bf16[8,136,128]{2,1,0:T(8,128)(2,1)S(1)} %merge.19.after_ref), channel_id=1, source_target_pairs={{8,0},{124,4},{16,8},{4,12},{24,16},{12,20},{32,24},{20,28},{40,32... | collective-permute-start | bytes 835592 | tf_op jit(solution)/shard_map/ppermute | solution.py:569
  124.2 6.9 %collective-permute-start.24 = (bf16[8,136,128]{2,1,0:T(8,128)(2,1)S(1)}, bf16[8,136,128]{2,1,0:T(8,128)(2,1)S(1)}, u32[]{:S(2)}, u32[]{:S(2)}) collective-permute-start(bf16[8,136,128]{2,1,0:T(8,128)(2,1)S(1)} %merge.20.after_ref), channel_id=1, source_target_pairs={{8,0},{124,4},{16,8},{4,12},{24,16},{12,20},{32,24},{20,28},{40,32... | collective-permute-start | bytes 835592 | tf_op jit(solution)/shard_map/ppermute | solution.py:569
  127.5 6.7 %collective-permute-start.25 = (bf16[8,136,128]{2,1,0:T(8,128)(2,1)S(1)}, bf16[8,136,128]{2,1,0:T(8,128)(2,1)S(1)}, u32[]{:S(2)}, u32[]{:S(2)}) collective-permute-start(bf16[8,136,128]{2,1,0:T(8,128)(2,1)S(1)} %merge.21.after_ref), channel_id=1, source_target_pairs={{8,0},{124,4},{16,8},{4,12},{24,16},{12,20},{32,24},{20,28},{40,32... | collective-permute-start | bytes 835592 | tf_op jit(solution)/shard_map/ppermute | solution.py:569
  131.4 6.7 %collective-permute-start.26 = (bf16[8,136,128]{2,1,0:T(8,128)(2,1)S(1)}, bf16[8,136,128]{2,1,0:T(8,128)(2,1)S(1)}, u32[]{:S(2)}, u32[]{:S(2)}) collective-permute-start(bf16[8,136,128]{2,1,0:T(8,128)(2,1)S(1)} %merge.22.after_ref), channel_id=1, source_target_pairs={{8,0},{124,4},{16,8},{4,12},{24,16},{12,20},{32,24},{20,28},{40,32... | collective-permute-start | bytes 835592 | tf_op jit(solution)/shard_map/ppermute | solution.py:569
  134.5 6.7 %collective-permute-start.27 = (bf16[8,136,128]{2,1,0:T(8,128)(2,1)S(1)}, bf16[8,136,128]{2,1,0:T(8,128)(2,1)S(1)}, u32[]{:S(2)}, u32[]{:S(2)}) collective-permute-start(bf16[8,136,128]{2,1,0:T(8,128)(2,1)S(1)} %merge.23.after_ref), channel_id=1, source_target_pairs={{8,0},{124,4},{16,8},{4,12},{24,16},{12,20},{32,24},{20,28},{40,32... | collective-permute-start | bytes 835592 | tf_op jit(solution)/shard_map/ppermute | solution.py:569
  138.4 6.7 %collective-permute-start.28 = (bf16[8,136,128]{2,1,0:T(8,128)(2,1)S(1)}, bf16[8,136,128]{2,1,0:T(8,128)(2,1)S(1)}, u32[]{:S(2)}, u32[]{:S(2)}) collective-permute-start(bf16[8,136,128]{2,1,0:T(8,128)(2,1)S(1)} %merge.24.after_ref), channel_id=1, source_target_pairs={{8,0},{124,4},{16,8},{4,12},{24,16},{12,20},{32,24},{20,28},{40,32... | collective-permute-start | bytes 835592 | tf_op jit(solution)/shard_map/ppermute | solution.py:569
  141.5 6.7 %collective-permute-start.29 = (bf16[8,136,128]{2,1,0:T(8,128)(2,1)S(1)}, bf16[8,136,128]{2,1,0:T(8,128)(2,1)S(1)}, u32[]{:S(2)}, u32[]{:S(2)}) collective-permute-start(bf16[8,136,128]{2,1,0:T(8,128)(2,1)S(1)} %merge.25.after_ref), channel_id=1, source_target_pairs={{8,0},{124,4},{16,8},{4,12},{24,16},{12,20},{32,24},{20,28},{40,32... | collective-permute-start | bytes 835592 | tf_op jit(solution)/shard_map/ppermute | solution.py:569
  145.3 6.7 %collective-permute-start.30 = (bf16[8,136,128]{2,1,0:T(8,128)(2,1)S(1)}, bf16[8,136,128]{2,1,0:T(8,128)(2,1)S(1)}, u32[]{:S(2)}, u32[]{:S(2)}) collective-permute-start(bf16[8,136,128]{2,1,0:T(8,128)(2,1)S(1)} %merge.26.after_ref), channel_id=1, source_target_pairs={{8,0},{124,4},{16,8},{4,12},{24,16},{12,20},{32,24},{20,28},{40,32... | collective-permute-start | bytes 835592 | tf_op jit(solution)/shard_map/ppermute | solution.py:569
  148.5 8.7 %collective-permute-start.31 = (bf16[8,136,128]{2,1,0:T(8,128)(2,1)S(1)}, bf16[8,136,128]{2,1,0:T(8,128)(2,1)S(1)}, u32[]{:S(2)}, u32[]{:S(2)}) collective-permute-start(bf16[8,136,128]{2,1,0:T(8,128)(2,1)S(1)} %merge.27.after_ref), channel_id=1, source_target_pairs={{8,0},{124,4},{16,8},{4,12},{24,16},{12,20},{32,24},{20,28},{40,32... | collective-permute-start | bytes 835592 | tf_op jit(solution)/shard_map/ppermute | solution.py:569
  152.3 6.2 %collective-permute-start.32 = (bf16[8,136,128]{2,1,0:T(8,128)(2,1)S(1)}, bf16[8,136,128]{2,1,0:T(8,128)(2,1)S(1)}, u32[]{:S(2)}, u32[]{:S(2)}) collective-permute-start(bf16[8,136,128]{2,1,0:T(8,128)(2,1)S(1)} %merge.28.after_ref), channel_id=1, source_target_pairs={{8,4},{124,0},{16,12},{4,8},{24,20},{12,16},{32,28},{20,24},{40,36... | collective-permute-start | bytes 835592 | tf_op jit(solution)/shard_map/ppermute | solution.py:569
